TPU v7x, 256 devices: a whole 4x4x8 slice. The times are simulated.
256 devices in a mesh: sp: 16 (over y, x), tp: 16 (over z, core).
Axes of the slice: x: 4, y: 4, z: 8, core: 2. Of those that a mesh axis runs over, the one named last changes fastest.
Arguments:
- moe_input: bfloat16 [4096, 4096], P('sp', 'tp'), may hold values from -6 to 6
- out_gate: bfloat16 [4096, 4096], P('sp', 'tp'), may hold values from -6 to 6
- in_gate: bfloat16 [4096, 4096], P('sp', 'tp'), may hold values from -6 to 6
- values: bfloat16 [4096, 4096], P('sp', 'tp'), may hold values from -6 to 6
- conv_taps: float32 [3, 4096], P(None, 'tp'), may hold values from -3 to 3
- out_proj: bfloat16 [4096, 4096], P(None, 'tp'), may hold values from -0.09375 to 0.09375
- route_ids: int32 [4096, 2], P('sp'), may hold values from 0 to 15, all different within a row; in each aligned block of 256 rows (0 to 255, 256 to 511, ...) at most 48 rows name the same one
- route_gates: float32 [4096, 2], P('sp'), may hold values from 0.1 to 0.9
- expert_gate: bfloat16 [16, 4096, 2048], P('sp', None, 'tp'), may hold values from -0.09375 to 0.09375
- expert_up: bfloat16 [16, 4096, 2048], P('sp', None, 'tp'), may hold values from -0.09375 to 0.09375
- expert_down: bfloat16 [16, 2048, 4096], P('sp', 'tp'), may hold values from -0.125 to 0.125
- cotangent: bfloat16 [4096, 4096], P('sp', 'tp'), may hold values from -6 to 6
Outputs:
- grad_out_gate: bfloat16 [4096, 4096], P('sp', 'tp')
- grad_in_gate: bfloat16 [4096, 4096], P('sp', 'tp')
- grad_values: bfloat16 [4096, 4096], P('sp', 'tp')
- grad_out_proj: float32 [4096, 4096], P('sp', 'tp')
- grad_expert_gate: float32 [16, 4096, 2048], P('sp', None, 'tp')
- grad_expert_up: float32 [16, 4096, 2048], P('sp', None, 'tp')
- grad_expert_down: float32 [16, 2048, 4096], P('sp', 'tp')
Inputs may be any that keep to these rules, and one draw needn't show every extreme that they name: `route_ids`: the 2 experts of a token differ. In the rows of one device no expert is named by more than 48 assignments, and in some device's rows some expert is named by exactly 48.
All inputs are finite; a program needn't handle non-finite values.
Results may differ from a plain program's by a relative error of at most 0.014.
Values may be sent and summed in bfloat16 or wider, within the bound.
A program may use at most 128 MiB of HBM per device.

v0:
```python
import jax
import jax.numpy as jnp
from jax import lax
from jax.sharding import Mesh
from jax.sharding import PartitionSpec as P

TP = ("tp_0", "tp_1")


def side_by_side(arrays, axis, split_dim, concat_dim, along):
    ends, at = ([], 0)
    for a in arrays[:-1]:
        at += a.shape[along]
        ends.append(at)
    both = jnp.concatenate(arrays, axis=along)
    return tuple(
        jnp.split(
            lax.all_to_all(both, axis, split_axis=split_dim, concat_axis=concat_dim, tiled=True),
            ends,
            axis=along,
        )
    )


def side_by_side_2(arrays, axis, dim, along):
    widths = [a.shape[along] for a in arrays]
    both = jnp.concatenate(arrays, axis=along)
    out = lax.all_gather(both, axis, axis=dim, tiled=True)
    return tuple(jnp.split(out, [sum(widths[:k]) for k in range(1, len(widths))], axis=along))


def padded(array, sides, width):
    for axis, dim in sides:
        size, length = (lax.axis_size(axis), array.shape[dim])
        up = [(i, (i + 1) % size) for i in range(size - 1)]
        down = [(j, i) for i, j in up]
        last = lax.slice_in_dim(array, length - width, length, axis=dim)
        initial = lax.slice_in_dim(array, 0, width, axis=dim)
        before = lax.ppermute(last, axis, up)
        after = lax.ppermute(initial, axis, down)
        array = jnp.concatenate([before, array, after], axis=dim)
    return array


def gather_axes(array, axes, dim):
    if not axes:
        return array
    nearer = lax.all_gather(array, axes[-1], axis=dim, tiled=True)
    return gather_axes(nearer, axes[:-1], dim)


def from_everyone(array, axis):
    size = lax.axis_size(axis)
    return lax.all_to_all(
        jnp.broadcast_to(array[None], (size, *array.shape)), axis, 0, 0, tiled=True
    )


def laid_out(parts, dim):
    shape = list(parts.shape[1:])
    shape[dim] *= parts.shape[0]
    return jnp.moveaxis(parts, 0, dim).reshape(shape)


def gathered_copies(array, axis, dim):
    parts = from_everyone(array, axis)
    return laid_out(parts, dim)


def body(
    moe_input,
    out_gate,
    in_gate,
    values,
    conv_taps,
    out_proj,
    route_ids,
    route_gates,
    expert_gate,
    expert_up,
    expert_down,
    cotangent,
):
    token_count = moe_input.shape[0]
    part_width = moe_input.shape[1]
    pick_count = route_ids.shape[1]
    group_count = lax.axis_size("sp")
    local_count = expert_gate.shape[0]
    expert_count = group_count * local_count
    capacity = 3 * token_count // expert_count
    contract_rows = (((0,), (0,)), ((), ()))
    flat_ids = route_ids.reshape(-1)
    owner = jnp.arange(token_count * pick_count, dtype=jnp.int32) // pick_count
    one_hot = (flat_ids[:, None] == jnp.arange(expert_count, dtype=jnp.int32)[None, :]).astype(
        jnp.int32
    )
    earlier = jnp.cumsum(one_hot, axis=0) - one_hot
    position = jnp.sum(earlier * one_hot, axis=1)
    slot_index = flat_ids * capacity + position
    slot_token = (
        jnp.full((expert_count * capacity,), token_count, jnp.int32).at[slot_index].set(owner)
    )
    slot_weight = (
        jnp.zeros((expert_count * capacity,), jnp.float32)
        .at[slot_index]
        .set(route_gates.reshape(-1))
    )
    padded_input = jnp.concatenate([moe_input, jnp.zeros((1, part_width), moe_input.dtype)], axis=0)
    padded_cot = jnp.concatenate([cotangent, jnp.zeros((1, part_width), cotangent.dtype)], axis=0)
    send_rows = padded_input[slot_token].reshape(expert_count, capacity, part_width)
    send_cot = (slot_weight[:, None] * padded_cot[slot_token].astype(jnp.float32)).astype(
        jnp.bfloat16
    )
    send_cot = send_cot.reshape(expert_count, capacity, part_width)
    recv_rows, recv_cot = side_by_side((send_rows, send_cot), "sp", 0, 1, 2)
    full_rows, full_cot = side_by_side_2((recv_rows, recv_cot), TP, 2, 0)
    pre_gate = jnp.einsum(
        "prd,pdf->prf", full_rows, expert_gate, preferred_element_type=jnp.float32
    )
    pre_up = jnp.einsum("prd,pdf->prf", full_rows, expert_up, preferred_element_type=jnp.float32)
    gate_sig = jax.nn.sigmoid(pre_gate)
    activated = pre_gate * gate_sig
    hidden_act = (activated * pre_up).astype(jnp.bfloat16)
    grad_expert_down = jnp.einsum(
        "prf,prd->pfd", hidden_act, full_cot, preferred_element_type=jnp.float32
    )
    grad_hidden = jnp.einsum(
        "prd,pfd->prf", full_cot, expert_down, preferred_element_type=jnp.float32
    )
    grad_pre_gate = (grad_hidden * pre_up * gate_sig * (1.0 + pre_gate * (1.0 - gate_sig))).astype(
        jnp.bfloat16
    )
    grad_pre_up = (grad_hidden * activated).astype(jnp.bfloat16)
    grad_expert_gate = jnp.einsum(
        "prd,prf->pdf", full_rows, grad_pre_gate, preferred_element_type=jnp.float32
    )
    grad_expert_up = jnp.einsum(
        "prd,prf->pdf", full_rows, grad_pre_up, preferred_element_type=jnp.float32
    )
    partial_grad = jnp.einsum(
        "prf,pdf->prd", grad_pre_gate, expert_gate, preferred_element_type=jnp.float32
    ) + jnp.einsum("prf,pdf->prd", grad_pre_up, expert_up, preferred_element_type=jnp.float32)
    slot_grad = lax.psum_scatter(partial_grad, TP, scatter_dimension=2, tiled=True)
    returned = lax.all_to_all(slot_grad, "sp", split_axis=1, concat_axis=0, tiled=True)
    flat_returned = returned.reshape(expert_count * capacity, part_width)
    moe_grad = jnp.sum(
        flat_returned[slot_index].reshape(token_count, pick_count, part_width), axis=1
    )
    mixer_cot = (cotangent.astype(jnp.float32) + moe_grad).astype(jnp.bfloat16)
    conv_in = in_gate.astype(jnp.float32) * values.astype(jnp.float32)
    rimmed = padded(conv_in, (("sp", 0),), 1)
    conv_out = rimmed[:-2] * conv_taps[0] + rimmed[1:-1] * conv_taps[1] + rimmed[2:] * conv_taps[2]
    mixed = (out_gate.astype(jnp.float32) * conv_out).astype(jnp.bfloat16)
    full_mixer_cot = gather_axes(mixer_cot, TP, 1)
    grad_mixed = jnp.dot(full_mixer_cot, out_proj, preferred_element_type=jnp.float32)
    grad_out_gate = (grad_mixed * conv_out).astype(jnp.bfloat16)
    grad_conv_out = grad_mixed * out_gate.astype(jnp.float32)
    rim_grad = padded(grad_conv_out, (("sp", 0),), 1)
    grad_conv_in = (
        rim_grad[2:] * conv_taps[0] + rim_grad[1:-1] * conv_taps[1] + rim_grad[:-2] * conv_taps[2]
    )
    grad_in_gate = (grad_conv_in * values.astype(jnp.float32)).astype(jnp.bfloat16)
    grad_values = (grad_conv_in * in_gate.astype(jnp.float32)).astype(jnp.bfloat16)
    columns = lax.all_to_all(full_mixer_cot, "sp", split_axis=1, concat_axis=0, tiled=True)
    grad_out_proj = lax.dot_general(
        columns, gathered_copies(mixed, "sp", 0), contract_rows, preferred_element_type=jnp.float32
    )
    return (
        grad_out_gate,
        grad_in_gate,
        grad_values,
        grad_out_proj,
        grad_expert_gate,
        grad_expert_up,
        grad_expert_down,
    )


def solution(mesh):
    finer = Mesh(mesh.devices.reshape(mesh.shape["sp"], 8, 2), ("sp", "tp_0", "tp_1"))
    in_specs = (
        P("sp", TP),
        P("sp", TP),
        P("sp", TP),
        P("sp", TP),
        P(None, TP),
        P(None, TP),
        P("sp", None),
        P("sp", None),
        P("sp", None, TP),
        P("sp", None, TP),
        P("sp", TP, None),
        P("sp", TP),
    )
    out_specs = (
        P("sp", TP),
        P("sp", TP),
        P("sp", TP),
        P("sp", TP),
        P("sp", None, TP),
        P("sp", None, TP),
        P("sp", TP, None),
    )
    return jax.shard_map(body, mesh=finer, in_specs=in_specs, out_specs=out_specs, check_vma=False)
```

profile of v0, /device:TPU:17, one launch (start us, length us, event | category | flops | bytes accessed | tf_op | source)
XLA Modules:
  0.0 367.3 jit_solution(3472268219430080457)
XLA Ops:
  18.8 2.7 gather_fusion.1
  24.4 17.7 %all_to_all.42 = bf16[16,48,512]{2,1,0:T(8,128)(2,1)S(1)} all-to-all(bf16[16,48,512]{2,1,0:T(8,128)(2,1)S(1)} %pad_maximum_fusion), channel_id=1, replica_groups=mesh['sp'=16,'tp_0'=8,'tp_1'=2] {'sp'}, dimensions={0} | all-to-all | bytes 1572864 | tf_op jit(solution)/shard_map/all_to_all | solution.py:18
  43.4 84.2 %all-gather.3.cloned.1.call-done = bf16[2,768,4096]{2,1,0:T(8,128)(2,1)} async-done(((bf16[2,768,256]{2,1,0:T(8,128)(2,1)}), bf16[2,768,4096]{2,1,0:T(8,128)(2,1)}) %all-gather.3.cloned.1.call-update) | async-done | bytes 12582928 | tf_op jit(solution)/shard_map/all_gather | solution.py:28
  127.6 5.0 %fusion.3 = f32[768,128]{1,0:T(8,128)S(1)} fusion(bf16[2,768,4096]{2,1,0:T(8,128)(2,1)} %all-gather.3.cloned.1.call-done, bf16[1,4096,128]{2,1,0:T(8,128)(2,1)} %param.20), kind=kOutput, calls=%fused_computation.13 | convolution fusion | flops 805306368 | bytes 7733248 | tf_op jit(solution)/shard_map/prd,pdf->prf/dot_general | solution.py:117
  132.6 5.4 %fusion.4 = f32[768,128]{1,0:T(8,128)S(1)} fusion(bf16[2,768,4096]{2,1,0:T(8,128)(2,1)} %all-gather.3.cloned.1.call-done, bf16[1,4096,128]{2,1,0:T(8,128)(2,1)S(1)} %copy-done.2), kind=kOutput, calls=%fused_computation.14 | convolution fusion | flops 805306368 | bytes 7733248 | tf_op jit(solution)/shard_map/prd,pdf->prf/dot_general | solution.py:120
  141.7 6.4 %add_bitcast_fusion = f32[1,768,4096]{2,1,0:T(8,128)} fusion(f32[768,4096]{1,0:T(8,128)S(1)} %fusion.10, bf16[768,128]{1,0:T(8,128)(2,1)S(1)} %get-tuple-element.7, bf16[1,4096,128]{2,1,0:T(8,128)(2,1)S(1)} %copy-done.2), kind=kOutput, calls=%fused_computation.5 | convolution fusion | flops 808452096 | bytes 26411008 | tf_op jit(solution)/shard_map/prf,pdf->prd/dot_general | solution.py:142
  148.1 76.2 %reduce-scatter.2.cloned.1.call-done = f32[1,768,256]{2,1,0:T(8,128)} async-done(((f32[1,768,4096]{2,1,0:T(8,128)}), f32[1,768,256]{2,1,0:T(8,128)}) %reduce-scatter.2.cloned.1.call-update) | async-done | bytes 786448 | tf_op jit(solution)/shard_map/reduce_scatter | solution.py:143
  224.4 2.8 copy.31
  227.2 6.7 %all-to-all-start.1 = ((f32[1,768,256]{2,0,1:T(1,128)}), f32[1,768,256]{2,0,1:T(1,128)}, u32[]{:S(2)}, u32[]{:S(2)}) async-start(f32[1,768,256]{2,0,1:T(1,128)} %copy.31), calls=%async_computation.2 | async-start | bytes 1572864 | tf_op jit(solution)/shard_map/all_to_all | solution.py:144
  233.9 10.7 %all-to-all-done.1 = f32[1,768,256]{2,0,1:T(1,128)} async-done(((f32[1,768,256]{2,0,1:T(1,128)}), f32[1,768,256]{2,0,1:T(1,128)}, u32[]{:S(2)}, u32[]{:S(2)}) %all-to-all-start.1) | async-done | bytes 786464 | tf_op jit(solution)/shard_map/all_to_all | solution.py:144
  248.4 4.1 %all_gather.10 = bf16[256,512]{1,0:T(8,128)(2,1)} all-gather(bf16[256,256]{1,0:T(8,128)(2,1)S(1)} %add_convert_fusion), channel_id=1, replica_groups=mesh['sp'=16,'tp_0'=8,'tp_1'=2] {'tp_1'}, dimensions={1}, use_global_device_ids=true | all-gather | bytes 393216 | tf_op jit(solution)/shard_map/all_gather | solution.py:48
  252.6 35.4 %all-gather.5.cloned.1.call-done = bf16[256,4096]{1,0:T(8,128)(2,1)} async-done(((bf16[256,512]{1,0:T(8,128)(2,1)}), bf16[256,4096]{1,0:T(8,128)(2,1)}) %all-gather.5.cloned.1.call-update) | async-done | bytes 2097168 | tf_op jit(solution)/shard_map/all_gather | solution.py:48
  288.0 4.1 %copy.32 = bf16[256,4096]{0,1:T(8,128)(2,1)} copy(bf16[256,4096]{1,0:T(8,128)(2,1)} %all-gather.5.cloned.1.call-done) | data formatting | bytes 4194304 | tf_op jit(solution)/shard_map/all_gather | solution.py:48
  292.1 6.7 %all-to-all-start.2 = ((bf16[256,16,256]{0,2,1:T(8,128)(2,1)}), bf16[256,16,256]{0,2,1:T(8,128)(2,1)}, u32[]{:S(2)}, u32[]{:S(2)}) async-start(bf16[256,16,256]{0,2,1:T(8,128)(2,1)} %bitcast.86), calls=%async_computation.3 | async-start | bytes 4194304 | tf_op jit(solution)/shard_map/all_to_all | solution.py:164
  298.9 3.2 collective-permute-start
  302.1 4.5 %collective-permute-start.1 = (f32[1,256]{1,0:T(1,128)S(1)}, f32[1,256]{1,0:T(1,128)S(1)}, u32[]{:S(2)}, u32[]{:S(2)}) collective-permute-start(f32[1,256]{1,0:T(1,128)S(1)} %get-tuple-element.19), channel_id=1, source_target_pairs={{16,0},{32,16},{48,32},{64,48},{80,64},{96,80},{112,96},{128,112},... | collective-permute-start | bytes 3080 | tf_op jit(solution)/shard_map/ppermute | solution.py:40
  306.6 16.0 %collective-permute-done = f32[1,256]{1,0:T(1,128)S(1)} collective-permute-done((f32[1,256]{1,0:T(1,128)S(1)}, f32[1,256]{1,0:T(1,128)S(1)}, u32[]{:S(2)}, u32[]{:S(2)}) %collective-permute-start) | collective-permute-done | bytes 1056 | tf_op jit(solution)/shard_map/ppermute | solution.py:39
  322.6 3.0 fusion.20
  327.1 5.2 %all-to-all-start.3 = ((bf16[16,256,256]{2,1,0:T(8,128)(2,1)}), bf16[16,256,256]{2,1,0:T(8,128)(2,1)}, u32[]{:S(2)}, u32[]{:S(2)}) async-start(bf16[16,256,256]{2,1,0:T(8,128)(2,1)} %broadcast_in_dim.11), calls=%async_computation.4 | async-start | bytes 4194304 | tf_op jit(solution)/shard_map/all_to_all | solution.py:54
  332.3 6.1 %convolution_bitcast_fusion = f32[1,4096,128]{2,1,0:T(8,128)} fusion(bf16[768,128]{1,0:T(8,128)(2,1)S(1)} %copy-done.5, bf16[2,768,4096]{2,1,0:T(8,128)(2,1)} %all-gather.3.cloned.1.call-done), kind=kOutput, calls=%fused_computation.11 | convolution fusion | flops 805306368 | bytes 8585216 | tf_op jit(solution)/shard_map/prd,prf->pdf/dot_general | solution.py:137
  338.5 6.1 %convolution_bitcast_fusion.1 = f32[1,4096,128]{2,1,0:T(8,128)} fusion(bf16[768,128]{1,0:T(8,128)(2,1)S(1)} %copy-done.14, bf16[2,768,4096]{2,1,0:T(8,128)(2,1)} %all-gather.3.cloned.1.call-done), kind=kOutput, calls=%fused_computation.12 | convolution fusion | flops 805306368 | bytes 8585216 | tf_op jit(solution)/shard_map/prd,prf->pdf/dot_general | solution.py:134
  344.6 4.3 %collective-permute-start.2 = (f32[1,256]{1,0:T(1,128)S(1)}, f32[1,256]{1,0:T(1,128)S(1)}, u32[]{:S(2)}, u32[]{:S(2)}) collective-permute-start(f32[1,256]{1,0:T(1,128)S(1)} %get-tuple-element.16), channel_id=1, source_target_pairs={{16,0},{32,16},{48,32},{64,48},{80,64},{96,80},{112,96},{128,112},... | collective-permute-start | bytes 3080 | tf_op jit(solution)/shard_map/ppermute | solution.py:40
  353.4 2.9 collective-permute-done.3
  357.1 3.6 fusion.7
  (97 shorter events, 30.1 us)
Async XLA Ops:
  7.2 315.5 %copy-start = (bf16[4096,256]{1,0:T(8,128)(2,1)S(1)}, bf16[4096,256]{1,0:T(8,128)(2,1)}, u32[]{:S(2)}) copy-start(bf16[4096,256]{1,0:T(8,128)(2,1)} %param.17) | copy-start | bytes 6291460
  7.2 120.4 %all-gather.3.cloned.1.call-start = ((), (), s32[]{:S(2)}) async-start(), calls=%async_computation.5 | async-start | bytes 13369344 | tf_op jit(solution)/shard_map/all_gather | solution.py:28
  42.2 90.4 %copy-start.2 = (bf16[1,4096,128]{2,1,0:T(8,128)(2,1)S(1)}, bf16[1,4096,128]{2,1,0:T(8,128)(2,1)}, u32[]{:S(2)}) copy-start(bf16[1,4096,128]{2,1,0:T(8,128)(2,1)} %param.21) | copy-start | bytes 3145732
  43.2 181.2 %reduce-scatter.2.cloned.1.call-start = ((), (), s32[]{:S(2)}) async-start(), calls=%async_computation.6 | async-start | bytes 13369344 | tf_op jit(solution)/shard_map/reduce_scatter | solution.py:143
  127.6 10.4 %copy-start.1 = (bf16[2,768,4096]{2,1,0:T(8,128)(2,1)S(1)}, bf16[2,768,4096]{2,1,0:T(8,128)(2,1)}, u32[]{:S(2)}) copy-start(bf16[2,768,4096]{2,1,0:T(8,128)(2,1)} %all-gather.3.cloned.1.call-done) | copy-start | bytes 37748740
  148.1 100.2 %copy-start.6 = (bf16[256,256]{1,0:T(8,128)(2,1)S(1)}, bf16[256,256]{1,0:T(8,128)(2,1)}, u32[]{:S(2)}) copy-start(bf16[256,256]{1,0:T(8,128)(2,1)} %param.23) | copy-start | bytes 393220
  227.2 17.4 %all-to-all-start.1 = ((f32[1,768,256]{2,0,1:T(1,128)}), f32[1,768,256]{2,0,1:T(1,128)}, u32[]{:S(2)}, u32[]{:S(2)}) async-start(f32[1,768,256]{2,0,1:T(1,128)} %copy.31), calls=%async_computation.2 | async-start | bytes 1572864 | tf_op jit(solution)/shard_map/all_to_all | solution.py:144
  233.9 54.2 %all-gather.5.cloned.1.call-start = ((), (), s32[]{:S(2)}) async-start(), calls=%async_computation.7 | async-start | bytes 2359296 | tf_op jit(solution)/shard_map/all_gather | solution.py:48
  247.4 59.2 %copy-start.15 = (f32[3,256]{1,0:T(4,128)S(1)}, f32[3,256]{1,0:T(4,128)}, u32[]{:S(2)}) copy-start(f32[3,256]{1,0:T(4,128)} %param.16) | copy-start | bytes 9220
  247.7 51.1 %copy-start.7 = (bf16[256,256]{1,0:T(8,128)(2,1)S(1)}, bf16[256,256]{1,0:T(8,128)(2,1)}, u32[]{:S(2)}) copy-start(bf16[256,256]{1,0:T(8,128)(2,1)} %param.15) | copy-start | bytes 393220
  247.7 51.1 %copy-start.8 = (bf16[256,256]{1,0:T(8,128)(2,1)S(1)}, bf16[256,256]{1,0:T(8,128)(2,1)}, u32[]{:S(2)}) copy-start(bf16[256,256]{1,0:T(8,128)(2,1)} %param.14) | copy-start | bytes 393220
  247.7 74.9 %copy-start.17 = (bf16[256,256]{1,0:T(8,128)(2,1)S(1)}, bf16[256,256]{1,0:T(8,128)(2,1)}, u32[]{:S(2)}) copy-start(bf16[256,256]{1,0:T(8,128)(2,1)} %param.13) | copy-start | bytes 393220
  292.1 33.5 %all-to-all-start.2 = ((bf16[256,16,256]{0,2,1:T(8,128)(2,1)}), bf16[256,16,256]{0,2,1:T(8,128)(2,1)}, u32[]{:S(2)}, u32[]{:S(2)}) async-start(bf16[256,16,256]{0,2,1:T(8,128)(2,1)} %bitcast.86), calls=%async_computation.3 | async-start | bytes 4194304 | tf_op jit(solution)/shard_map/all_to_all | solution.py:164
  298.8 33.5 %copy-start.5 = (bf16[768,128]{1,0:T(8,128)(2,1)S(1)}, bf16[768,128]{1,0:T(8,128)(2,1)}, u32[]{:S(2)}) copy-start(bf16[768,128]{1,0:T(8,128)(2,1)} %copy-done.4) | copy-start | bytes 589828
  298.9 23.8 %collective-permute-start = (f32[1,256]{1,0:T(1,128)S(1)}, f32[1,256]{1,0:T(1,128)S(1)}, u32[]{:S(2)}, u32[]{:S(2)}) collective-permute-start(f32[1,256]{1,0:T(1,128)S(1)} %get-tuple-element.18), channel_id=1, source_target_pairs={{0,16},{16,32},{32,48},{48,64},{64,80},{80,96},{96,112},{112,128},... | collective-permute-start | bytes 3080 | tf_op jit(solution)/shard_map/ppermute | solution.py:39
  302.1 20.5 %collective-permute-start.1 = (f32[1,256]{1,0:T(1,128)S(1)}, f32[1,256]{1,0:T(1,128)S(1)}, u32[]{:S(2)}, u32[]{:S(2)}) collective-permute-start(f32[1,256]{1,0:T(1,128)S(1)} %get-tuple-element.19), channel_id=1, source_target_pairs={{16,0},{32,16},{48,32},{64,48},{80,64},{96,80},{112,96},{128,112},... | collective-permute-start | bytes 3080 | tf_op jit(solution)/shard_map/ppermute | solution.py:40
  327.1 30.0 %all-to-all-start.3 = ((bf16[16,256,256]{2,1,0:T(8,128)(2,1)}), bf16[16,256,256]{2,1,0:T(8,128)(2,1)}, u32[]{:S(2)}, u32[]{:S(2)}) async-start(bf16[16,256,256]{2,1,0:T(8,128)(2,1)} %broadcast_in_dim.11), calls=%async_computation.4 | async-start | bytes 4194304 | tf_op jit(solution)/shard_map/all_to_all | solution.py:54
  332.3 18.5 %slice-start = ((s8[12582912]{0:T(1024)(128)(4,1)}), s8[4194304]{0:T(1024)(128)(4,1)S(1)}, s32[]{:S(2)}) async-start(s8[12582912]{0:T(1024)(128)(4,1)} %bitcast.87), calls=%async_computation.8 | async-start | bytes 8388608
  332.3 18.5 %slice-start.1 = ((s8[12582912]{0:T(1024)(128)(4,1)}), s8[4194304]{0:T(1024)(128)(4,1)S(1)}, s32[]{:S(2)}) async-start(s8[12582912]{0:T(1024)(128)(4,1)} %bitcast.87), calls=%async_computation.9 | async-start | bytes 8388608
  338.4 12.4 %slice-start.2 = ((s8[12582912]{0:T(1024)(128)(4,1)}), s8[4194304]{0:T(1024)(128)(4,1)S(1)}, s32[]{:S(2)}) async-start(s8[12582912]{0:T(1024)(128)(4,1)} %bitcast.87), calls=%async_computation.10 | async-start | bytes 8388608
  338.4 12.4 %copy-start.10 = (f32[768,128]{1,0:T(8,128)S(1)}, f32[768,128]{1,0:T(8,128)}, u32[]{:S(2)}) copy-start(f32[768,128]{1,0:T(8,128)} %copy-done.9) | copy-start | bytes 1179652
  338.4 12.4 %copy-start.12 = (f32[768,128]{1,0:T(8,128)S(1)}, f32[768,128]{1,0:T(8,128)}, u32[]{:S(2)}) copy-start(f32[768,128]{1,0:T(8,128)} %copy-done.11) | copy-start | bytes 1179652
  344.6 8.8 %collective-permute-start.2 = (f32[1,256]{1,0:T(1,128)S(1)}, f32[1,256]{1,0:T(1,128)S(1)}, u32[]{:S(2)}, u32[]{:S(2)}) collective-permute-start(f32[1,256]{1,0:T(1,128)S(1)} %get-tuple-element.16), channel_id=1, source_target_pairs={{16,0},{32,16},{48,32},{64,48},{80,64},{96,80},{112,96},{128,112},... | collective-permute-start | bytes 3080 | tf_op jit(solution)/shard_map/ppermute | solution.py:40
  348.8 7.5 %collective-permute-start.3 = (f32[1,256]{1,0:T(1,128)S(1)}, f32[1,256]{1,0:T(1,128)S(1)}, u32[]{:S(2)}, u32[]{:S(2)}) collective-permute-start(f32[1,256]{1,0:T(1,128)S(1)} %get-tuple-element.17), channel_id=1, source_target_pairs={{0,16},{16,32},{32,48},{48,64},{64,80},{80,96},{96,112},{112,128},... | collective-permute-start | bytes 3080 | tf_op jit(solution)/shard_map/ppermute | solution.py:39
  (7 other events, 26.3 us)
Sparse Core Ops, SparseCore 0:
  43.3 84.2 all-gather.2
  148.3 76.0 reduce-scatter.1
  252.7 35.2 all-gather.4
where the time goes:
time: 374 us; the launch traced here: 367 us
  waiting for transfers between devices  226 us (60%)
  matrix products  41.5 us (11%)
  starting transfers between devices  32.8 us (9%)
  local copies, waits for them, and re-layouts  26.3 us (7%)
  blocking collectives  21.9 us (6%)
  between operations  14.3 us (4%)
  other arithmetic  4.83 us (1%)
    all_gather x1, waiting for transfers between devices, side_by_side_2(): out = lax.all_gather(both, axis, axis=dim, tiled=True)  84.2 us
    reduce_scatter x1, waiting for transfers between devices, body(): lax.psum_scatter(partial_grad, TP, scatter_dimension=2, tiled=True)  76.2 us
    all_gather x1, waiting for transfers between devices, gather_axes(): nearer = lax.all_gather(array, axes[-1], axis=dim, tiled=True)  35.4 us
    ppermute x2, waiting for transfers between devices, padded(): before = lax.ppermute(last, axis, up)  18.9 us
    all_to_all x1, blocking collectives, side_by_side(): lax.all_to_all(both, axis, split_axis=split_dim, concat_axis=concat_dim,...  17.7 us
    all_to_all x1, waiting for transfers between devices, body(): lax.all_to_all(slot_grad, 'sp', split_axis=1, concat_axis=0, tiled=True)  10.7 us
    ppermute x2, starting transfers between devices, padded(): after = lax.ppermute(initial, axis, down)  8.81 us
  transfers between devices with their start and end apart: 10, of which 7 were waited for; matrix products, arithmetic and copies ran while one was open for 5% of the time, Pallas kernels for 0%

commit v1 on v0

v1 whole, which is shorter than its diff:
```python
import functools
import jax
import jax.numpy as jnp
from jax import lax
from jax.experimental import pallas as pl
from jax.experimental.pallas import tpu as pltpu
from jax.sharding import PartitionSpec as P

F32 = jnp.float32
BF16 = jnp.bfloat16
MESH = pl.DeviceIdType.MESH
NT = (((1,), (1,)), ((), ()))
TN = (((0,), (0,)), ((), ()))


def dot(a, b, dims):
    return lax.dot_general(a, b, dims, preferred_element_type=F32)


def moe_kernel(
    send_ref, wg_ref, wu_ref, wd_ref,
    ret_ref, gg_ref, gu_ref, gd_ref,
    rows, wgu, wd, acc, g2, hid, q, r, in_f, in_b, out_f, out_b, fin, grad_gu, grad_d,
    w_sem, disp_send, disp_recv,
    af_send, af_recv, ab_send, ab_recv, ap_send, ap_recv,
    rp_send, rp_recv, rf_send, rf_recv, rb_send, rb_recv,
    ret_send, ret_recv, out_sem,
):
    s = lax.axis_index("sp")
    t = lax.axis_index("tp")
    z, c = t // 2, t % 2
    y = s // 4
    up, down, mate = ((z + 1) % 8) * 2 + c, ((z + 7) % 8) * 2 + c, z * 2 + (1 - c)

    weights = [
        pltpu.make_async_copy(wg_ref, wgu.at[:, :, pl.ds(0, 128)], w_sem.at[0]),
        pltpu.make_async_copy(wu_ref, wgu.at[:, :, pl.ds(128, 128)], w_sem.at[1]),
        pltpu.make_async_copy(wd_ref, wd, w_sem.at[2]),
    ]
    for w in weights:
        w.start()

    barrier = pltpu.get_barrier_semaphore()

    @pl.loop(1, 16)
    def _(i):
        pl.semaphore_signal(barrier, inc=1, device_id={"sp": (s + i) % 16}, device_id_type=MESH)

    for other in (up, down, mate):
        pl.semaphore_signal(barrier, inc=1, device_id={"tp": other}, device_id_type=MESH)
    pl.semaphore_wait(barrier, 18)

    def remote(src, dst, send_sem, recv_sem, **where):
        return pltpu.make_async_remote_copy(
            src_ref=src, dst_ref=dst, send_sem=send_sem, recv_sem=recv_sem,
            device_id=where, device_id_type=MESH,
        )

    def dispatch(peer, source):
        return remote(
            send_ref.at[peer], rows.at[t, source], disp_send.at[peer], disp_recv.at[source], sp=peer
        )

    own = pltpu.make_async_copy(send_ref.at[s], rows.at[t, s], disp_recv.at[s])
    own.start()

    @pl.loop(1, 16)
    def _(i):
        dispatch((s + i) % 16, s).start()

    acc[...] = jnp.zeros_like(acc)
    for w in weights:
        w.wait()

    def part(k):
        return pl.ds(4 * ((y + 4 - k) % 4), 4)

    def slice_of(zz, core, k):
        return rows.at[zz * 2 + core, part(k)]

    def along_f(d, k):
        at = slice_of((z + 8 - d) % 8, c, k)
        return remote(at, at, af_send.at[d, k], af_recv.at[d, k], tp=up)

    def along_b(d, k):
        at = slice_of((z + d) % 8, c, k)
        return remote(at, at, ab_send.at[d, k], ab_recv.at[d, k], tp=down)

    def to_mate(zz, core, k):
        at = slice_of(zz, core, k)
        return remote(at, at, ap_send.at[zz, k], ap_recv.at[zz, k], tp=mate)

    def multiply(tt, k):
        block = rows[tt, part(k)].reshape(192, 512)
        pre = dot(block[:, :256], wgu[tt], (((1,), (0,)), ((), ())))
        columns = pl.ds(pl.multiple_of(tt * 256, 256), 256)
        hidden = dot(block[:, 256:], wd[:, columns], NT)
        acc[part(k), :, pl.ds(0, 256)] += pre.reshape(4, 48, 256)
        acc[part(k), :, pl.ds(256, 128)] += hidden.reshape(4, 48, 128)

    @pl.loop(0, 4)
    def _(k):
        for x in range(4):
            source = 4 * ((y + 4 - k) % 4) + x

            @pl.when(source == s)
            def _():
                own.wait()

            @pl.when(source != s)
            def _():
                dispatch(source, source).wait_recv()

        along_f(0, k).start()
        along_b(0, k).start()
        to_mate(z, c, k).start()
        multiply(t, k)

    def mate_part(zz, k):
        to_mate(zz, 1 - c, k).wait_recv()
        multiply(zz * 2 + 1 - c, k)

    @pl.loop(0, 16)
    def _(i):
        d, k = i // 4 + 1, i % 4
        even = (k % 2) == 0
        zf, zb = (z + 8 - d) % 8, (z + d) % 8

        @pl.when((d < 4) | even)
        def _():
            at = slice_of(zf, c, k)
            remote(at, at, af_send.at[d - 1, k], af_recv.at[d - 1, k], tp=up).wait_recv()

            @pl.when((d < 3) | ((d == 3) & even))
            def _():
                along_f(d, k).start()

            to_mate(zf, c, k).start()

        @pl.when((d < 4) | (~even))
        def _():
            at = slice_of(zb, c, k)
            remote(at, at, ab_send.at[d - 1, k], ab_recv.at[d - 1, k], tp=down).wait_recv()

            @pl.when((d < 3) | ((d == 3) & (~even)))
            def _():
                along_b(d, k).start()

        @pl.when((d < 4) | (~even))
        def _():
            to_mate(zb, c, k).start()

        @pl.when((d < 4) | even)
        def _():
            multiply(zf * 2 + c, k)

        @pl.when((d < 4) | (~even))
        def _():
            multiply(zb * 2 + c, k)

        e = i // 4

        @pl.when(e == 0)
        def _():
            mate_part(z, k)

        @pl.when(e > 0)
        def _():
            mate_part((z + 8 - e) % 8, k)
            mate_part((z + e) % 8, k)

    @pl.loop(0, 4)
    def _(k):
        mate_part((z + 4) % 8, k)

    def dots_of(tt, k):
        return dot(g2[part(k)].reshape(192, 256), wgu[tt], NT)

    def prepare(zz, k):
        value = dots_of(zz * 2 + 1 - c, k)
        q[zz, part(k)] = value.astype(BF16).reshape(4, 48, 256)
        remote(
            q.at[zz, part(k)], r.at[zz, part(k)], rp_send.at[zz, k], rp_recv.at[zz, k], tp=mate
        ).start()

    @pl.loop(0, 4)
    def _(k):
        block = acc[part(k)].reshape(192, 384)
        pre_gate, pre_up, grad_hidden = block[:, :128], block[:, 128:256], block[:, 256:]
        sig = jax.nn.sigmoid(pre_gate)
        activated = pre_gate * sig
        hid[part(k)] = (activated * pre_up).astype(BF16).reshape(4, 48, 128)
        grad_gate = (grad_hidden * pre_up * sig * (1.0 + pre_gate * (1.0 - sig))).astype(BF16)
        grad_up = (grad_hidden * activated).astype(BF16)
        g2[part(k), :, pl.ds(0, 128)] = grad_gate.reshape(4, 48, 128)
        g2[part(k), :, pl.ds(128, 128)] = grad_up.reshape(4, 48, 128)
        prepare((z + 4) % 8, k)

    def summed(zz, k):
        at = r.at[zz, part(k)]
        remote(at, at, rp_send.at[zz, k], rp_recv.at[zz, k], tp=mate).wait_recv()
        return dots_of(zz * 2 + c, k) + r[zz, part(k)].reshape(192, 256).astype(F32)

    def ring_step(d, k, zz, incoming, outgoing, send_sem, recv_sem, to, starts):
        value = summed(zz, k)

        @pl.when(starts)
        def _():
            outgoing[d - 1, part(k)] = value.astype(BF16).reshape(4, 48, 256)

        @pl.when(jnp.logical_not(starts))
        def _():
            at = incoming.at[d, part(k)]
            remote(at, at, send_sem.at[d, k], recv_sem.at[d, k], tp=to).wait_recv()
            both = value + incoming[d, part(k)].reshape(192, 256).astype(F32)
            outgoing[d - 1, part(k)] = both.astype(BF16).reshape(4, 48, 256)

        remote(
            outgoing.at[d - 1, part(k)], incoming.at[d - 1, part(k)],
            send_sem.at[d - 1, k], recv_sem.at[d - 1, k], tp=to,
        ).start()

    def grads(tt):
        x = rows[tt, :, :, pl.ds(0, 256)].reshape(768, 256)
        cot = rows[tt, :, :, pl.ds(256, 256)].reshape(768, 256)
        grad_gu[tt] = dot(x, g2[...].reshape(768, 256), TN)
        columns = pl.ds(pl.multiple_of(tt * 256, 256), 256)
        grad_d[:, columns] = dot(hid[...].reshape(768, 128), cot, TN)
        for copy in outputs(tt):
            copy.start()

    def outputs(tt):
        columns = pl.ds(pl.multiple_of(tt * 256, 256), 256)
        return [
            pltpu.make_async_copy(grad_gu.at[tt, :, pl.ds(0, 128)], gg_ref.at[tt], out_sem.at[0, tt]),
            pltpu.make_async_copy(grad_gu.at[tt, :, pl.ds(128, 128)], gu_ref.at[tt], out_sem.at[1, tt]),
            pltpu.make_async_copy(grad_d.at[:, columns], gd_ref.at[:, columns], out_sem.at[2, tt]),
        ]

    @pl.loop(0, 16)
    def _(i):
        d, k = 4 - i // 4, i % 4
        even = (k % 2) == 0
        zf, zb = (z + d) % 8, (z + 8 - d) % 8

        @pl.when((d < 4) | even)
        def _():
            ring_step(d, k, zf, in_f, out_f, rf_send, rf_recv, up, (d == 4) | ((d == 3) & (~even)))

        @pl.when((d < 4) | (~even))
        def _():
            ring_step(d, k, zb, in_b, out_b, rb_send, rb_recv, down, (d == 4) | ((d == 3) & even))

        prepare((z + d - 1) % 8, k)

        @pl.when(d > 1)
        def _():
            prepare((z + 9 - d) % 8, k)

        grads(i)

    def giving_back(peer, source):
        return remote(fin.at[peer], ret_ref.at[source], ret_send.at[peer], ret_recv.at[source], sp=peer)

    mine = pltpu.make_async_copy(fin.at[s], ret_ref.at[s], ret_recv.at[s])

    @pl.loop(0, 4)
    def _(k):
        value = summed(z, k)
        for incoming, send_sem, recv_sem, to in ((in_f, rf_send, rf_recv, up), (in_b, rb_send, rb_recv, down)):
            at = incoming.at[0, part(k)]
            remote(at, at, send_sem.at[0, k], recv_sem.at[0, k], tp=to).wait_recv()
            value = value + incoming[0, part(k)].reshape(192, 256).astype(F32)
        fin[part(k)] = value.astype(BF16).reshape(4, 48, 256)
        for x in range(4):
            peer = 4 * ((y + 4 - k) % 4) + x

            @pl.when(peer == s)
            def _():
                mine.start()

            @pl.when(peer != s)
            def _():
                giving_back(peer, s).start()

    @pl.loop(1, 16)
    def _(i):
        giving_back((s + i) % 16, (s + i) % 16).wait_recv()

    mine.wait()

    @pl.loop(1, 16)
    def _(i):
        dispatch((s + i) % 16, s).wait_send()
        giving_back((s + i) % 16, s).wait_send()

    @pl.loop(0, 16)
    def _(i):
        d, k = i // 4, i % 4
        even = (k % 2) == 0

        @pl.when((d < 3) | even)
        def _():
            along_f(d, k).wait_send()
            at = out_f.at[d, part(k)]
            remote(at, at, rf_send.at[d, k], rf_recv.at[d, k], tp=up).wait_send()

        @pl.when((d < 3) | (~even))
        def _():
            along_b(d, k).wait_send()
            at = out_b.at[d, part(k)]
            remote(at, at, rb_send.at[d, k], rb_recv.at[d, k], tp=down).wait_send()

        for half in range(2):
            zz = d * 2 + half
            to_mate(zz, c, k).wait_send()
            at = q.at[zz, part(k)]
            remote(at, at, rp_send.at[zz, k], rp_recv.at[zz, k], tp=mate).wait_send()
        for copy in outputs(i):
            copy.wait()


def moe(send, wg, wu, wd):
    vm = lambda shape, dtype: pltpu.VMEM(shape, dtype)
    dma = lambda *shape: pltpu.SemaphoreType.DMA(shape)
    any_ = pl.BlockSpec(memory_space=pl.ANY)
    vmem = pl.BlockSpec(memory_space=pltpu.VMEM)
    return pl.pallas_call(
        moe_kernel,
        out_shape=(
            jax.ShapeDtypeStruct((16, 48, 256), BF16),
            jax.ShapeDtypeStruct((16, 256, 128), F32),
            jax.ShapeDtypeStruct((16, 256, 128), F32),
            jax.ShapeDtypeStruct((128, 4096), F32),
        ),
        in_specs=[vmem, any_, any_, any_],
        out_specs=(vmem, any_, any_, any_),
        scratch_shapes=[
            vm((16, 16, 48, 512), BF16),
            vm((16, 256, 256), BF16),
            vm((128, 4096), BF16),
            vm((16, 48, 384), F32),
            vm((16, 48, 256), BF16),
            vm((16, 48, 128), BF16),
            vm((8, 16, 48, 256), BF16),
            vm((8, 16, 48, 256), BF16),
            vm((4, 16, 48, 256), BF16),
            vm((4, 16, 48, 256), BF16),
            vm((4, 16, 48, 256), BF16),
            vm((4, 16, 48, 256), BF16),
            vm((16, 48, 256), BF16),
            vm((16, 256, 256), F32),
            vm((128, 4096), F32),
            dma(3), dma(16), dma(16),
            dma(4, 4), dma(4, 4), dma(4, 4), dma(4, 4), dma(8, 4), dma(8, 4),
            dma(8, 4), dma(8, 4), dma(4, 4), dma(4, 4), dma(4, 4), dma(4, 4),
            dma(16), dma(16), dma(3, 16),
        ],
        compiler_params=pltpu.CompilerParams(
            collective_id=1, has_side_effects=True, vmem_limit_bytes=60 * 1024 * 1024
        ),
        cost_estimate=pl.CostEstimate(flops=8_000_000_000, bytes_accessed=20_000_000, transcendentals=100_000),
        name="moe",
    )(send, wg, wu, wd)


def padded(array):
    size = 16
    up = [(i, i + 1) for i in range(size - 1)]
    before = lax.ppermute(array[-1:], "sp", up)
    after = lax.ppermute(array[:1], "sp", [(j, i) for i, j in up])
    return jnp.concatenate([before, array, after], axis=0)


def body(moe_input, out_gate, in_gate, values, conv_taps, out_proj, route_ids, route_gates, expert_gate, expert_up, expert_down, cotangent):
    experts = jnp.arange(16, dtype=jnp.int32)
    chosen = route_ids[:, :, None] == experts[None, None, :]
    member = jnp.sum(chosen.astype(F32), axis=1)
    weight = jnp.sum(jnp.where(chosen, route_gates[:, :, None], 0.0), axis=1)
    tokens = jnp.arange(256, dtype=jnp.int32)
    earlier = (tokens[:, None] > tokens[None, :]).astype(BF16)
    place = jnp.dot(earlier, member.astype(BF16), preferred_element_type=F32)
    place = jnp.where(member > 0, place, -1.0)
    pick = place.T[:, None, :] == jnp.arange(48, dtype=F32)[None, :, None]
    slot_weight = jnp.sum(jnp.where(pick, weight.T[:, None, :], 0.0), axis=2)
    pick = pick.astype(BF16).reshape(768, 256)
    both = jnp.dot(pick, jnp.concatenate([moe_input, cotangent], axis=1), preferred_element_type=F32)
    scale = slot_weight.reshape(768, 1)
    send = jnp.concatenate([both[:, :256], both[:, 256:] * scale], axis=1).astype(BF16).reshape(16, 48, 512)

    ret, gg, gu, gd = moe(
        send,
        expert_gate.reshape(16, 256, 128),
        expert_up.reshape(16, 256, 128),
        expert_down.reshape(128, 4096),
    )
    grad_expert_gate = gg.reshape(1, 4096, 128)
    grad_expert_up = gu.reshape(1, 4096, 128)
    grad_expert_down = gd.reshape(1, 128, 4096)
    moe_grad = lax.dot_general(pick, ret.reshape(768, 256), TN, preferred_element_type=F32)
    mixer_cot = (cotangent.astype(F32) + moe_grad).astype(BF16)

    conv_in = in_gate.astype(F32) * values.astype(F32)
    rimmed = padded(conv_in)
    conv_out = rimmed[:-2] * conv_taps[0] + rimmed[1:-1] * conv_taps[1] + rimmed[2:] * conv_taps[2]
    mixed = (out_gate.astype(F32) * conv_out).astype(BF16)
    all_mixed = lax.all_gather(mixed, "sp", axis=0, tiled=True)
    full_mixer_cot = lax.all_gather(mixer_cot, "tp", axis=1, tiled=True)
    grad_mixed = jnp.dot(full_mixer_cot, out_proj, preferred_element_type=F32)
    grad_out_gate = (grad_mixed * conv_out).astype(BF16)
    grad_conv_out = grad_mixed * out_gate.astype(F32)
    rim_grad = padded(grad_conv_out)
    grad_conv_in = rim_grad[2:] * conv_taps[0] + rim_grad[1:-1] * conv_taps[1] + rim_grad[:-2] * conv_taps[2]
    grad_in_gate = (grad_conv_in * values.astype(F32)).astype(BF16)
    grad_values = (grad_conv_in * in_gate.astype(F32)).astype(BF16)
    columns = lax.all_to_all(full_mixer_cot, "sp", split_axis=1, concat_axis=0, tiled=True)
    grad_out_proj = lax.dot_general(columns, all_mixed, TN, preferred_element_type=F32)
    return (grad_out_gate, grad_in_gate, grad_values, grad_out_proj, grad_expert_gate, grad_expert_up, grad_expert_down)


def solution(mesh):
    in_specs = (
        P("sp", "tp"), P("sp", "tp"), P("sp", "tp"), P("sp", "tp"), P(None, "tp"), P(None, "tp"),
        P("sp", None), P("sp", None),
        P("sp", None, "tp"), P("sp", None, "tp"), P("sp", "tp", None), P("sp", "tp"),
    )
    out_specs = (
        P("sp", "tp"), P("sp", "tp"), P("sp", "tp"), P("sp", "tp"),
        P("sp", None, "tp"), P("sp", None, "tp"), P("sp", "tp", None),
    )
    return jax.shard_map(body, mesh=mesh, in_specs=in_specs, out_specs=out_specs, check_vma=False)
```

time: 374 us -> 261 us (0.70)
  waiting for transfers between devices: 226 us -> 75.9 us
  Pallas kernels: 0 us -> 124 us
  matrix products: 41.5 us -> 10.5 us
  blocking collectives: 21.9 us -> 0 us
  local copies, waits for them, and re-layouts: 26.3 us -> 9.4 us
  starting transfers between devices: 32.8 us -> 20.4 us
    pallas_call x0 -> x1, Pallas kernels: none -> 124 us  [moe(): pl.pallas_call(moe_kernel, out_shape=(jax.ShapeDtypeStruct((16, 48, 256),...]
    reduce_scatter x1 -> x0, waiting for transfers between devices: 76.2 us -> none  [body(): lax.psum_scatter(partial_grad, TP, scatter_dimension=2, tiled=True)]
    all_gather x2, waiting for transfers between devices: 120 us -> 47.8 us  [the longest x1 29 us: body(): full_mixer_cot = lax.all_gather(mixer_cot, 'tp', axis=1, tiled=True)]
    dot_general x10 -> x5, matrix products: 41.5 us -> 10.5 us  [the longest x1 3.81 us: body(): lax.dot_general(columns, all_mixed, TN, preferred_element_type=F32)]
    all_to_all x1 -> x0, blocking collectives: 17.7 us -> none  [side_by_side(): lax.all_to_all(both, axis, split_axis=split_dim, concat_axis=concat_dim,...]
    all_to_all x2 -> x0, starting transfers between devices: 11.8 us -> none  [the longest x1 6.67 us: body(): lax.all_to_all(slot_grad, 'sp', split_axis=1, concat_axis=0, tiled=True)]
    all_to_all x2 -> x0, waiting for transfers between devices: 10.7 us -> none  [the longest x1 10.7 us: body(): lax.all_to_all(slot_grad, 'sp', split_axis=1, concat_axis=0, tiled=True)]
    ppermute x4, waiting for transfers between devices: 19.1 us -> 26.9 us  [the longest x2 24.7 us: padded(): before = lax.ppermute(array[-1:], 'sp', up)]
  transfers between devices with their start and end apart: 10 -> 7, of which waited for: 7 -> 6; matrix products, arithmetic and copies ran while one was open for 5% -> 2% of each run, Pallas kernels for 0% -> 0%
where the time goes in v1:
time: 261 us; the launch traced here: 257 us
  Pallas kernels  124 us (48%)
  waiting for transfers between devices  75.9 us (29%)
  starting transfers between devices  20.4 us (8%)
  between operations  14.2 us (5%)
  matrix products  10.5 us (4%)
  local copies, waits for them, and re-layouts  9.4 us (4%)
  other arithmetic  3.21 us (1%)
    pallas_call x1, Pallas kernels, moe(): pl.pallas_call(moe_kernel, out_shape=(jax.ShapeDtypeStruct((16, 48, 256),...  124 us
    all_gather x1, waiting for transfers between devices, body(): full_mixer_cot = lax.all_gather(mixer_cot, 'tp', axis=1, tiled=True)  29 us
    ppermute x2, waiting for transfers between devices, padded(): before = lax.ppermute(array[-1:], 'sp', up)  24.7 us
    all_gather x1, waiting for transfers between devices, body(): all_mixed = lax.all_gather(mixed, 'sp', axis=0, tiled=True)  18.8 us
    ppermute x2, starting transfers between devices, padded(): after = lax.ppermute(array[:1], 'sp', [(j, i) for i, j in up])  8.66 us
    all_to_all x1, starting transfers between devices, body(): lax.all_to_all(full_mixer_cot, 'sp', split_axis=1, concat_axis=0, tiled=T...  6.68 us
    unnamed x21, local copies, waits for them, and re-layouts  6.05 us
  transfers between devices with their start and end apart: 7, of which 6 were waited for; matrix products, arithmetic and copies ran while one was open for 2% of the time, Pallas kernels for 0%

profile of v1, /device:TPU:17, one launch (start us, length us, event | category | flops | bytes accessed | tf_op | source)
XLA Modules:
  0.0 257.3 jit_solution(2518897074634618040)
XLA Ops:
  7.3 0.8 select_reduce_fusion.1
  8.8 1.3 fusion.15
  10.4 1.0 pad_maximum_fusion.send_ref
  11.3 123.6 %moe.1 = (bf16[16,48,256]{2,1,0:T(8,128)(2,1)}, f32[16,256,128]{2,1,0:T(8,128)}, f32[16,256,128]{2,1,0:T(8,128)}, f32[128,4096]{1,0:T(8,128)}) custom-call(bf16[16,48,512]{2,1,0:T(8,128)(2,1)} %pad_maximum_fusion.send_ref, bf16[16,256,128]{2,1,0:T(8,128)(2,1)} %bitcast.49, bf16[16,256,128]{2,1,0:T(8,128)(2,1)} %bitcast.50, bf16[128,4096]{1,0:T(8,128)(2,1)} %bitcast.51), custom_call_target="tpu_custom_call" | custom-call | flops 8000000000 | bytes 20000000 | tf_op jit(solution)/shard_map/moe/pallas_call | solution.py:328
  135.0 2.2 fusion.1
  137.3 4.4 %collective-permute-start.1 = (f32[1,256]{1,0:T(1,128)S(1)}, f32[1,256]{1,0:T(1,128)S(1)}, u32[]{:S(2)}, u32[]{:S(2)}) collective-permute-start(f32[1,256]{1,0:T(1,128)S(1)} %get-tuple-element.25), channel_id=1, source_target_pairs={{16,0},{32,16},{48,32},{64,48},{80,64},{96,80},{112,96},{128,112},... | collective-permute-start | bytes 3080 | tf_op jit(solution)/shard_map/ppermute | solution.py:371
  141.7 1.9 collective-permute-start
  143.6 4.5 %collective-permute-done = f32[1,256]{1,0:T(1,128)S(1)} collective-permute-done((f32[1,256]{1,0:T(1,128)S(1)}, f32[1,256]{1,0:T(1,128)S(1)}, u32[]{:S(2)}, u32[]{:S(2)}) %collective-permute-start) | collective-permute-done | bytes 1056 | tf_op jit(solution)/shard_map/ppermute | solution.py:370
  148.1 29.0 %all-gather.3.cloned.1.call-done = bf16[256,4096]{1,0:T(8,128)(2,1)} async-done(((bf16[256,256]{1,0:T(8,128)(2,1)}), bf16[256,4096]{1,0:T(8,128)(2,1)}) %all-gather.3.cloned.1.call-update) | async-done | bytes 2097168 | tf_op jit(solution)/shard_map/all_gather | solution.py:408
  177.1 3.0 %fusion.6 = (bf16[256,256]{1,0:T(8,128)(2,1)}, bf16[256,256]{1,0:T(8,128)(2,1)}, f32[256,256]{1,0:T(8,128)S(1)}) fusion(bf16[256,256]{1,0:T(8,128)(2,1)S(1)} %copy-done.8, f32[256]{0:T(256)S(1)} %bitcast.45, f32[1,256]{1,0:T(1,128)S(1)} %collective-permute-done.1, f32[256,256]{1,0:T(8,128)S(1)} %convert_multiply_fusion.3, f32[256]{0:T(256)S(1)} %bitcast.47, ...), kind=kOutput, calls=%fused_computation.20 | convolution fusion | flops 537722880 | bytes 5116928 | tf_op jit(solution)/shard_map/dot_general | solution.py:409
  180.1 3.1 %copy.27 = bf16[32,16,8,256]{3,2,0,1:T(8,128)(2,1)} copy(bf16[32,16,8,256]{3,2,1,0:T(8,128)(2,1)} %bitcast.39) | data formatting | bytes 4194304 | tf_op jit(solution)/shard_map/all_to_all | solution.py:416
  183.2 6.7 %all-to-all-start = ((bf16[256,16,256]{2,0,1:T(8,128)(2,1)}), bf16[256,16,256]{2,0,1:T(8,128)(2,1)}, u32[]{:S(2)}, u32[]{:S(2)}) async-start(bf16[256,16,256]{2,0,1:T(8,128)(2,1)} %bitcast.35), calls=%async_computation | async-start | bytes 4194304 | tf_op jit(solution)/shard_map/all_to_all | solution.py:416
  189.9 3.1 %collective-permute-start.3 = (f32[1,256]{1,0:T(1,128)S(1)}, f32[1,256]{1,0:T(1,128)S(1)}, u32[]{:S(2)}, u32[]{:S(2)}) collective-permute-start(f32[1,256]{1,0:T(1,128)S(1)} %get-tuple-element.23), channel_id=1, source_target_pairs={{0,16},{16,32},{32,48},{48,64},{64,80},{80,96},{96,112},{112,128},... | collective-permute-start | bytes 3080 | tf_op jit(solution)/shard_map/ppermute | solution.py:370
  193.0 4.3 %collective-permute-start.2 = (f32[1,256]{1,0:T(1,128)S(1)}, f32[1,256]{1,0:T(1,128)S(1)}, u32[]{:S(2)}, u32[]{:S(2)}) collective-permute-start(f32[1,256]{1,0:T(1,128)S(1)} %get-tuple-element.22), channel_id=1, source_target_pairs={{16,0},{32,16},{48,32},{64,48},{80,64},{96,80},{112,96},{128,112},... | collective-permute-start | bytes 3080 | tf_op jit(solution)/shard_map/ppermute | solution.py:371
  197.3 20.3 %collective-permute-done.3 = f32[1,256]{1,0:T(1,128)S(1)} collective-permute-done((f32[1,256]{1,0:T(1,128)S(1)}, f32[1,256]{1,0:T(1,128)S(1)}, u32[]{:S(2)}, u32[]{:S(2)}) %collective-permute-start.3) | collective-permute-done | bytes 1056 | tf_op jit(solution)/shard_map/ppermute | solution.py:370
  217.6 2.2 collective-permute-done.2
  220.6 1.2 all-to-all-done
  221.8 18.8 %all-gather.5.cloned.1.call-done = bf16[4096,256]{1,0:T(8,128)(2,1)} async-done(((bf16[256,256]{1,0:T(8,128)(2,1)}), bf16[4096,256]{1,0:T(8,128)(2,1)}) %all-gather.5.cloned.1.call-update) | async-done | bytes 2097168 | tf_op jit(solution)/shard_map/all_gather | solution.py:407
  240.6 3.8 %fusion.24 = f32[256,256]{1,0:T(8,128)} fusion(bf16[4096,256]{1,0:T(8,128)(2,1)} %bitcast.13, bf16[4096,256]{1,0:T(8,128)(2,1)} %all-gather.5.cloned.1.call-done), kind=kOutput, calls=%fused_computation.47 | convolution fusion | flops 536870912 | bytes 4456448 | tf_op jit(solution)/shard_map/dot_general | solution.py:417
  244.4 1.3 copy.33
  245.7 1.0 copy-done.2
  246.8 1.3 copy.34
  248.1 1.0 copy-done.1
  249.1 1.3 copy.35
  (34 shorter events, 2.0 us)
Async XLA Ops:
  7.2 169.9 %copy-start = (bf16[4096,256]{1,0:T(8,128)(2,1)S(1)}, bf16[4096,256]{1,0:T(8,128)(2,1)}, u32[]{:S(2)}) copy-start(bf16[4096,256]{1,0:T(8,128)(2,1)} %param.17) | copy-start | bytes 6291460
  7.2 169.9 %all-gather.3.cloned.1.call-start = ((), (), s32[]{:S(2)}) async-start(), calls=%async_computation.1 | async-start | bytes 2228224 | tf_op jit(solution)/shard_map/all_gather | solution.py:408
  11.3 123.6 %copy-start.6 = (bf16[256,256]{1,0:T(8,128)(2,1)S(1)}, bf16[256,256]{1,0:T(8,128)(2,1)}, u32[]{:S(2)}) copy-start(bf16[256,256]{1,0:T(8,128)(2,1)} %param.23) | copy-start | bytes 393220
  134.9 2.3 copy-start.4
  134.9 2.3 copy-start.5
  134.9 8.7 %copy-start.7 = (f32[3,256]{1,0:T(4,128)S(1)}, f32[3,256]{1,0:T(4,128)}, u32[]{:S(2)}) copy-start(f32[3,256]{1,0:T(4,128)} %param.16) | copy-start | bytes 9220
  135.0 42.1 %copy-start.8 = (bf16[256,256]{1,0:T(8,128)(2,1)S(1)}, bf16[256,256]{1,0:T(8,128)(2,1)}, u32[]{:S(2)}) copy-start(bf16[256,256]{1,0:T(8,128)(2,1)} %param.13) | copy-start | bytes 393220
  137.2 103.4 %all-gather.5.cloned.1.call-start = ((), (), s32[]{:S(2)}) async-start(), calls=%async_computation.2 | async-start | bytes 2228224 | tf_op jit(solution)/shard_map/all_gather | solution.py:407
  137.3 6.3 %collective-permute-start.1 = (f32[1,256]{1,0:T(1,128)S(1)}, f32[1,256]{1,0:T(1,128)S(1)}, u32[]{:S(2)}, u32[]{:S(2)}) collective-permute-start(f32[1,256]{1,0:T(1,128)S(1)} %get-tuple-element.25), channel_id=1, source_target_pairs={{16,0},{32,16},{48,32},{64,48},{80,64},{96,80},{112,96},{128,112},... | collective-permute-start | bytes 3080 | tf_op jit(solution)/shard_map/ppermute | solution.py:371
  141.7 6.4 %collective-permute-start = (f32[1,256]{1,0:T(1,128)S(1)}, f32[1,256]{1,0:T(1,128)S(1)}, u32[]{:S(2)}, u32[]{:S(2)}) collective-permute-start(f32[1,256]{1,0:T(1,128)S(1)} %get-tuple-element.24), channel_id=1, source_target_pairs={{0,16},{16,32},{32,48},{48,64},{64,80},{80,96},{96,112},{112,128},... | collective-permute-start | bytes 3080 | tf_op jit(solution)/shard_map/ppermute | solution.py:370
  183.2 38.6 %all-to-all-start = ((bf16[256,16,256]{2,0,1:T(8,128)(2,1)}), bf16[256,16,256]{2,0,1:T(8,128)(2,1)}, u32[]{:S(2)}, u32[]{:S(2)}) async-start(bf16[256,16,256]{2,0,1:T(8,128)(2,1)} %bitcast.35), calls=%async_computation | async-start | bytes 4194304 | tf_op jit(solution)/shard_map/all_to_all | solution.py:416
  189.9 27.7 %collective-permute-start.3 = (f32[1,256]{1,0:T(1,128)S(1)}, f32[1,256]{1,0:T(1,128)S(1)}, u32[]{:S(2)}, u32[]{:S(2)}) collective-permute-start(f32[1,256]{1,0:T(1,128)S(1)} %get-tuple-element.23), channel_id=1, source_target_pairs={{0,16},{16,32},{32,48},{48,64},{64,80},{80,96},{96,112},{112,128},... | collective-permute-start | bytes 3080 | tf_op jit(solution)/shard_map/ppermute | solution.py:370
  193.0 26.8 %collective-permute-start.2 = (f32[1,256]{1,0:T(1,128)S(1)}, f32[1,256]{1,0:T(1,128)S(1)}, u32[]{:S(2)}, u32[]{:S(2)}) collective-permute-start(f32[1,256]{1,0:T(1,128)S(1)} %get-tuple-element.22), channel_id=1, source_target_pairs={{16,0},{32,16},{48,32},{64,48},{80,64},{96,80},{112,96},{128,112},... | collective-permute-start | bytes 3080 | tf_op jit(solution)/shard_map/ppermute | solution.py:371
  240.6 3.8 %copy-start.3 = (f32[16,256,128]{2,1,0:T(8,128)S(1)}, f32[16,256,128]{2,1,0:T(8,128)}, u32[]{:S(2)}) copy-start(f32[16,256,128]{2,1,0:T(8,128)} %get-tuple-element.12) | copy-start | bytes 6291460
  244.4 2.3 copy-start.2
  246.8 2.3 copy-start.1
Sparse Core Ops, SparseCore 0:
  137.3 39.7 all-gather.2
  180.2 60.3 all-gather.4

commit v2 on v1

--- a/solution.py
+++ b/solution.py
@@ -18,13 +18,17 @@
 
 
 def moe_kernel(
-    send_ref, wg_ref, wu_ref, wd_ref,
-    ret_ref, gg_ref, gu_ref, gd_ref,
+    send_ref, pick_ref, cot_ref, og_ref, ig_ref, val_ref, taps_ref, wg_ref, wu_ref, wd_ref, op_ref,
+    gog_ref, gig_ref, gval_ref, gop_ref, gg_ref, gu_ref, gd_ref,
     rows, wgu, wd, acc, g2, hid, q, r, in_f, in_b, out_f, out_b, fin, grad_gu, grad_d,
+    ret_ref, op, cin, cout, halo, mix, mcf, col, acc2,
     w_sem, disp_send, disp_recv,
     af_send, af_recv, ab_send, ab_recv, ap_send, ap_recv,
     rp_send, rp_recv, rf_send, rf_recv, rb_send, rb_recv,
     ret_send, ret_recv, out_sem,
+    halo_send, halo_recv, mix_send, mix_recv,
+    mf_send, mf_recv, mb_send, mb_recv, mp_send, mp_recv,
+    col_send, col_recv, colp_send, colp_recv,
 ):
     s = lax.axis_index("sp")
     t = lax.axis_index("tp")
@@ -36,9 +40,12 @@
         pltpu.make_async_copy(wg_ref, wgu.at[:, :, pl.ds(0, 128)], w_sem.at[0]),
         pltpu.make_async_copy(wu_ref, wgu.at[:, :, pl.ds(128, 128)], w_sem.at[1]),
         pltpu.make_async_copy(wd_ref, wd, w_sem.at[2]),
+        pltpu.make_async_copy(op_ref, op, w_sem.at[3]),
     ]
     for w in weights:
         w.start()
+
+    cin[...] = ig_ref[...].astype(F32) * val_ref[...].astype(F32)
 
     barrier = pltpu.get_barrier_semaphore()
 
@@ -64,9 +71,38 @@
     own = pltpu.make_async_copy(send_ref.at[s], rows.at[t, s], disp_recv.at[s])
     own.start()
 
+    def halo_copies(h):
+        return [
+            remote(cin.at[pl.ds(248, 8)], halo.at[h, 0], halo_send.at[h, 0], halo_recv.at[h, 0], sp=(s + 1) % 16),
+            remote(cin.at[pl.ds(0, 8)], halo.at[h, 1], halo_send.at[h, 1], halo_recv.at[h, 1], sp=(s + 15) % 16),
+        ]
+
+    row = lax.broadcasted_iota(jnp.int32, (256, 256), 0)
+
+    def neighbours(h):
+        for copy in halo_copies(h):
+            copy.wait()
+        array = cin[...]
+        first = jnp.where(s > 0, halo[h, 0, 7:8, :], 0.0)
+        last = jnp.where(s < 15, halo[h, 1, 0:1, :], 0.0)
+        before = jnp.where(row == 0, first, pltpu.roll(array, 1, 0))
+        after = jnp.where(row == 255, last, pltpu.roll(array, 255, 0))
+        return before, array, after
+
+    for copy in halo_copies(0):
+        copy.start()
+
     @pl.loop(1, 16)
     def _(i):
         dispatch((s + i) % 16, s).start()
+
+    before, here, after = neighbours(0)
+    conv = before * taps_ref[0:1, :] + here * taps_ref[1:2, :] + after * taps_ref[2:3, :]
+    cout[...] = conv
+    mix[s] = (og_ref[...].astype(F32) * conv).astype(BF16)
+
+    def mix_copy(peer, source):
+        return remote(mix.at[source], mix.at[source], mix_send.at[peer], mix_recv.at[source], sp=peer)
 
     acc[...] = jnp.zeros_like(acc)
     for w in weights:
@@ -115,6 +151,10 @@
         along_b(0, k).start()
         to_mate(z, c, k).start()
         multiply(t, k)
+
+    @pl.loop(1, 16)
+    def _(i):
+        mix_copy((s + i) % 16, s).start()
 
     def mate_part(zz, k):
         to_mate(zz, 1 - c, k).wait_recv()
@@ -289,10 +329,164 @@
 
     mine.wait()
 
+    moe_grad = dot(pick_ref[...], ret_ref[...].reshape(768, 256), TN)
+    mixer = (cot_ref[...].astype(F32) + moe_grad).astype(BF16)
+    mcf[t] = mixer.reshape(2, 128, 256)
+    acc2[...] = jnp.zeros_like(acc2)
+
+    def mc_f(d, k):
+        at = mcf.at[((z + 8 - d) % 8) * 2 + c, k]
+        return remote(at, at, mf_send.at[d, k], mf_recv.at[d, k], tp=up)
+
+    def mc_b(d, k):
+        at = mcf.at[((z + d) % 8) * 2 + c, k]
+        return remote(at, at, mb_send.at[d, k], mb_recv.at[d, k], tp=down)
+
+    def mc_mate(zz, core, k):
+        at = mcf.at[zz * 2 + core, k]
+        return remote(at, at, mp_send.at[zz, k], mp_recv.at[zz, k], tp=mate)
+
+    def column(peer, source):
+        return remote(mcf.at[peer, c], col.at[source, c], col_send.at[peer], col_recv.at[source], sp=peer)
+
+    def column_mate(source, core):
+        at = col.at[source, core]
+        return remote(at, at, colp_send.at[source], colp_recv.at[source], tp=mate)
+
+    kept = pltpu.make_async_copy(mcf.at[s, c], col.at[s, c], col_recv.at[s])
+
+    def use(tt, k):
+        @pl.when((k == c) & (tt == s))
+        def _():
+            kept.start()
+
+        @pl.when((k == c) & (tt != s))
+        def _():
+            column(tt, s).start()
+
+        acc2[k] += dot(mcf[tt, k], op[tt], (((1,), (0,)), ((), ())))
+
+    for k in range(2):
+        mc_f(0, k).start()
+        mc_b(0, k).start()
+        mc_mate(z, c, k).start()
+    for k in range(2):
+        use(t, k)
+
+    def mc_mate_part(zz, k):
+        mc_mate(zz, 1 - c, k).wait_recv()
+        use(zz * 2 + 1 - c, k)
+
+    @pl.loop(0, 8)
+    def _(i):
+        d, k = i // 2 + 1, i % 2
+        zf, zb = (z + 8 - d) % 8, (z + d) % 8
+        goes_f = (d < 4) | (k == 0)
+        goes_b = (d < 4) | (k == 1)
+
+        @pl.when(goes_f)
+        def _():
+            at = mcf.at[zf * 2 + c, k]
+            remote(at, at, mf_send.at[d - 1, k], mf_recv.at[d - 1, k], tp=up).wait_recv()
+
+            @pl.when((d < 3) | ((d == 3) & (k == 0)))
+            def _():
+                mc_f(d, k).start()
+
+            mc_mate(zf, c, k).start()
+
+        @pl.when(goes_b)
+        def _():
+            at = mcf.at[zb * 2 + c, k]
+            remote(at, at, mb_send.at[d - 1, k], mb_recv.at[d - 1, k], tp=down).wait_recv()
+
+            @pl.when((d < 3) | ((d == 3) & (k == 1)))
+            def _():
+                mc_b(d, k).start()
+
+        @pl.when(goes_b)
+        def _():
+            mc_mate(zb, c, k).start()
+
+        @pl.when(goes_f)
+        def _():
+            use(zf * 2 + c, k)
+
+        @pl.when(goes_b)
+        def _():
+            use(zb * 2 + c, k)
+
+        e = i // 2
+
+        @pl.when(e == 0)
+        def _():
+            mc_mate_part(z, k)
+
+        @pl.when(e > 0)
+        def _():
+            mc_mate_part((z + 8 - e) % 8, k)
+            mc_mate_part((z + e) % 8, k)
+
+    @pl.loop(0, 2)
+    def _(k):
+        mc_mate_part((z + 4) % 8, k)
+
+    grad_mixed = acc2[...].reshape(256, 256)
+    gog_ref[...] = (grad_mixed * cout[...]).astype(BF16)
+    cin[...] = grad_mixed * og_ref[...].astype(F32)
+    for copy in halo_copies(1):
+        copy.start()
+
+    kept.wait()
+    column_mate(s, c).start()
+
+    @pl.loop(1, 16)
+    def _(i):
+        source = (s + i) % 16
+        column(source, source).wait_recv()
+        column_mate(source, c).start()
+
+    gop_ref[...] = jnp.zeros_like(gop_ref)
+
+    @pl.loop(0, 16)
+    def _(i):
+        source = (s + i) % 16
+
+        @pl.when(i > 0)
+        def _():
+            mix_copy(source, source).wait_recv()
+
+        column_mate(source, 1 - c).wait_recv()
+        gop_ref[...] += dot(col[source].reshape(256, 256), mix[source], TN)
+
+    before, here, after = neighbours(1)
+    grad_in = after * taps_ref[0:1, :] + here * taps_ref[1:2, :] + before * taps_ref[2:3, :]
+    gig_ref[...] = (grad_in * val_ref[...].astype(F32)).astype(BF16)
+    gval_ref[...] = (grad_in * ig_ref[...].astype(F32)).astype(BF16)
+
     @pl.loop(1, 16)
     def _(i):
         dispatch((s + i) % 16, s).wait_send()
         giving_back((s + i) % 16, s).wait_send()
+        mix_copy((s + i) % 16, s).wait_send()
+        column((s + i) % 16, s).wait_send()
+
+    @pl.loop(0, 16)
+    def _(i):
+        column_mate(i, c).wait_send()
+        mc_mate(i // 2, c, i % 2).wait_send()
+
+    @pl.loop(0, 8)
+    def _(i):
+        d, k = i // 2, i % 2
+
+        @pl.when((d < 3) | (k == 0))
+        def _():
+            mc_f(d, k).wait_send()
+
+        @pl.when((d < 3) | (k == 1))
+        def _():
+            mc_b(d, k).wait_send()
 
     @pl.loop(0, 16)
     def _(i):
@@ -320,21 +514,23 @@
             copy.wait()
 
 
-def moe(send, wg, wu, wd):
+def mixer_and_experts(*operands):
     vm = lambda shape, dtype: pltpu.VMEM(shape, dtype)
     dma = lambda *shape: pltpu.SemaphoreType.DMA(shape)
     any_ = pl.BlockSpec(memory_space=pl.ANY)
     vmem = pl.BlockSpec(memory_space=pltpu.VMEM)
+    tile = jax.ShapeDtypeStruct((256, 256), BF16)
     return pl.pallas_call(
         moe_kernel,
         out_shape=(
-            jax.ShapeDtypeStruct((16, 48, 256), BF16),
+            tile, tile, tile,
+            jax.ShapeDtypeStruct((256, 256), F32),
             jax.ShapeDtypeStruct((16, 256, 128), F32),
             jax.ShapeDtypeStruct((16, 256, 128), F32),
             jax.ShapeDtypeStruct((128, 4096), F32),
         ),
-        in_specs=[vmem, any_, any_, any_],
-        out_specs=(vmem, any_, any_, any_),
+        in_specs=[vmem] * 7 + [any_] * 4,
+        out_specs=(vmem,) * 4 + (any_,) * 3,
         scratch_shapes=[
             vm((16, 16, 48, 512), BF16),
             vm((16, 256, 256), BF16),
@@ -351,25 +547,29 @@
             vm((16, 48, 256), BF16),
             vm((16, 256, 256), F32),
             vm((128, 4096), F32),
-            dma(3), dma(16), dma(16),
+            vm((16, 48, 256), BF16),
+            vm((16, 256, 256), BF16),
+            vm((256, 256), F32),
+            vm((256, 256), F32),
+            vm((2, 2, 8, 256), F32),
+            vm((16, 256, 256), BF16),
+            vm((16, 2, 128, 256), BF16),
+            vm((16, 2, 128, 256), BF16),
+            vm((2, 128, 256), F32),
+            dma(4), dma(16), dma(16),
             dma(4, 4), dma(4, 4), dma(4, 4), dma(4, 4), dma(8, 4), dma(8, 4),
             dma(8, 4), dma(8, 4), dma(4, 4), dma(4, 4), dma(4, 4), dma(4, 4),
             dma(16), dma(16), dma(3, 16),
+            dma(2, 2), dma(2, 2), dma(16), dma(16),
+            dma(4, 2), dma(4, 2), dma(4, 2), dma(4, 2), dma(8, 2), dma(8, 2),
+            dma(16), dma(16), dma(16), dma(16),
         ],
         compiler_params=pltpu.CompilerParams(
             collective_id=1, has_side_effects=True, vmem_limit_bytes=60 * 1024 * 1024
         ),
         cost_estimate=pl.CostEstimate(flops=8_000_000_000, bytes_accessed=20_000_000, transcendentals=100_000),
-        name="moe",
-    )(send, wg, wu, wd)
-
-
-def padded(array):
-    size = 16
-    up = [(i, i + 1) for i in range(size - 1)]
-    before = lax.ppermute(array[-1:], "sp", up)
-    after = lax.ppermute(array[:1], "sp", [(j, i) for i, j in up])
-    return jnp.concatenate([before, array, after], axis=0)
+        name="mixer_and_experts",
+    )(*operands)
 
 
 def body(moe_input, out_gate, in_gate, values, conv_taps, out_proj, route_ids, route_gates, expert_gate, expert_up, expert_down, cotangent):
@@ -388,34 +588,14 @@
     scale = slot_weight.reshape(768, 1)
     send = jnp.concatenate([both[:, :256], both[:, 256:] * scale], axis=1).astype(BF16).reshape(16, 48, 512)
 
-    ret, gg, gu, gd = moe(
-        send,
+    gog, gig, gval, gop, gg, gu, gd = mixer_and_experts(
+        send, pick, cotangent, out_gate, in_gate, values, conv_taps,
         expert_gate.reshape(16, 256, 128),
         expert_up.reshape(16, 256, 128),
         expert_down.reshape(128, 4096),
+        out_proj.reshape(16, 256, 256),
     )
-    grad_expert_gate = gg.reshape(1, 4096, 128)
-    grad_expert_up = gu.reshape(1, 4096, 128)
-    grad_expert_down = gd.reshape(1, 128, 4096)
-    moe_grad = lax.dot_general(pick, ret.reshape(768, 256), TN, preferred_element_type=F32)
-    mixer_cot = (cotangent.astype(F32) + moe_grad).astype(BF16)
-
-    conv_in = in_gate.astype(F32) * values.astype(F32)
-    rimmed = padded(conv_in)
-    conv_out = rimmed[:-2] * conv_taps[0] + rimmed[1:-1] * conv_taps[1] + rimmed[2:] * conv_taps[2]
-    mixed = (out_gate.astype(F32) * conv_out).astype(BF16)
-    all_mixed = lax.all_gather(mixed, "sp", axis=0, tiled=True)
-    full_mixer_cot = lax.all_gather(mixer_cot, "tp", axis=1, tiled=True)
-    grad_mixed = jnp.dot(full_mixer_cot, out_proj, preferred_element_type=F32)
-    grad_out_gate = (grad_mixed * conv_out).astype(BF16)
-    grad_conv_out = grad_mixed * out_gate.astype(F32)
-    rim_grad = padded(grad_conv_out)
-    grad_conv_in = rim_grad[2:] * conv_taps[0] + rim_grad[1:-1] * conv_taps[1] + rim_grad[:-2] * conv_taps[2]
-    grad_in_gate = (grad_conv_in * values.astype(F32)).astype(BF16)
-    grad_values = (grad_conv_in * in_gate.astype(F32)).astype(BF16)
-    columns = lax.all_to_all(full_mixer_cot, "sp", split_axis=1, concat_axis=0, tiled=True)
-    grad_out_proj = lax.dot_general(columns, all_mixed, TN, preferred_element_type=F32)
-    return (grad_out_gate, grad_in_gate, grad_values, grad_out_proj, grad_expert_gate, grad_expert_up, grad_expert_down)
+    return (gog, gig, gval, gop, gg.reshape(1, 4096, 128), gu.reshape(1, 4096, 128), gd.reshape(1, 128, 4096))
 
 
 def solution(mesh):

time: 261 us -> 180 us (0.69); the launches traced: 257 us -> 180 us
  waiting for transfers between devices: 75.9 us -> 0 us
  Pallas kernels: 124 us -> 161 us
  starting transfers between devices: 20.4 us -> 0 us
  between operations: 14.2 us -> 0.69 us
  matrix products: 10.5 us -> 1.5 us
  local copies, waits for them, and re-layouts: 9.4 us -> 13.4 us
    all_gather x2 -> x0, waiting for transfers between devices: 47.8 us -> none  [the longest x1 29 us: body(): full_mixer_cot = lax.all_gather(mixer_cot, 'tp', axis=1, tiled=True)]
    pallas_call x1, Pallas kernels: 124 us -> 161 us  [mixer_and_experts(): pl.pallas_call(moe_kernel, out_shape=(tile, tile, tile, jax.ShapeDtypeStr...]
    ppermute x4 -> x0, waiting for transfers between devices: 26.9 us -> none  [the longest x2 24.7 us: padded(): before = lax.ppermute(array[-1:], 'sp', up)]
    ppermute x4 -> x0, starting transfers between devices: 13.7 us -> none  [the longest x2 8.66 us: padded(): after = lax.ppermute(array[:1], 'sp', [(j, i) for i, j in up])]
    dot_general x3 -> x0, matrix products: 8.98 us -> none  [the longest x1 3.81 us: body(): lax.dot_general(columns, all_mixed, TN, preferred_element_type=F32)]
    unnamed x21 -> x11, local copies, waits for them, and re-layouts: 6.05 us -> 13.2 us
    all_to_all x1 -> x0, starting transfers between devices: 6.68 us -> none  [body(): lax.all_to_all(full_mixer_cot, 'sp', split_axis=1, concat_axis=0, tiled=T...]
    all_to_all x1 -> x0, local copies, waits for them, and re-layouts: 3.12 us -> none  [body(): lax.all_to_all(full_mixer_cot, 'sp', split_axis=1, concat_axis=0, tiled=T...]
  transfers between devices with their start and end apart: 7 -> 0, of which waited for: 6 -> 0; matrix products, arithmetic and copies ran while one was open for 2% -> 0% of each run, Pallas kernels for 0% -> 0%
where the time goes in v2:
time: 180 us
  Pallas kernels  161 us (89%)
  local copies, waits for them, and re-layouts  13.4 us (7%)
  other arithmetic  3.02 us (2%)
    pallas_call x1, Pallas kernels, mixer_and_experts(): pl.pallas_call(moe_kernel, out_shape=(tile, tile, tile, jax.ShapeDtypeStr...  161 us
    unnamed x11, local copies, waits for them, and re-layouts  13.2 us

profile of v2, /device:TPU:17, one launch (start us, length us, event | category | flops | bytes accessed | tf_op | source)
XLA Modules:
  0.0 180.0 jit_solution(511938889169133875)
XLA Ops:
  0.6 0.1 eq.44
  0.7 0.7 select_reduce_fusion.1
  1.4 0.2 convolution_select_fusion
  1.6 0.2 select_reduce_fusion
  1.8 0.1 mul.10
  1.9 1.0 fusion.7
  2.9 1.3 fusion.1
  4.2 0.2 fusion
  4.4 0.1 slice.15
  4.4 1.0 pad_maximum_fusion.send_ref
  5.4 161.4 %mixer_and_experts.1 = (bf16[256,256]{1,0:T(8,128)(2,1)}, bf16[256,256]{1,0:T(8,128)(2,1)}, bf16[256,256]{1,0:T(8,128)(2,1)}, f32[256,256]{1,0:T(8,128)}, f32[16...) custom-call(bf16[16,48,512]{2,1,0:T(8,128)(2,1)} %pad_maximum_fusion.send_ref, ...), custom_call_target="tpu_custom_call" | custom-call | flops 8000000000 | bytes 20000000 | tf_op jit(solution)/shard_map/mixer_and_experts/pallas_call | solution.py:523
  166.8 1.6 copy.30
  168.4 1.6 copy.31
  169.9 1.6 copy.32
  171.5 1.7 copy.33
  173.2 0.0 copy-start.1
  173.2 3.2 %copy.34 = f32[1,4096,128]{2,1,0:T(8,128)} copy(f32[1,4096,128]{2,1,0:T(8,128)} %bitcast.19) | data formatting | bytes 4194304
  176.4 0.0 copy-done.1
  176.4 0.0 copy-start
  176.4 1.3 copy.35
  177.7 1.0 copy-done
  178.7 1.3 copy.36
  (1 shorter events, 0.0 us)
Async XLA Ops:
  173.2 3.2 %copy-start.1 = (f32[16,256,128]{2,1,0:T(8,128)S(1)}, f32[16,256,128]{2,1,0:T(8,128)}, u32[]{:S(2)}) copy-start(f32[16,256,128]{2,1,0:T(8,128)} %get-tuple-element.19) | copy-start | bytes 6291460
  176.4 2.3 %copy-start = (f32[128,4096]{1,0:T(8,128)S(1)}, f32[128,4096]{1,0:T(8,128)}, u32[]{:S(2)}) copy-start(f32[128,4096]{1,0:T(8,128)} %get-tuple-element.20) | copy-start | bytes 6291460

commit v3 on v2

--- a/solution.py
+++ b/solution.py
@@ -11,6 +11,7 @@
 MESH = pl.DeviceIdType.MESH
 NT = (((1,), (1,)), ((), ()))
 TN = (((0,), (0,)), ((), ()))
+NN = (((1,), (0,)), ((), ()))
 
 
 def dot(a, b, dims):
@@ -18,9 +19,9 @@
 
 
 def moe_kernel(
-    send_ref, pick_ref, cot_ref, og_ref, ig_ref, val_ref, taps_ref, wg_ref, wu_ref, wd_ref, op_ref,
+    ids_ref, gates_ref, x_ref, cot_ref, og_ref, ig_ref, val_ref, taps_ref, wg_ref, wu_ref, wd_ref, op_ref,
     gog_ref, gig_ref, gval_ref, gop_ref, gg_ref, gu_ref, gd_ref,
-    rows, wgu, wd, acc, g2, hid, q, r, in_f, in_b, out_f, out_b, fin, grad_gu, grad_d,
+    pick_ref, scale, tokens, x_send, cot_send, rows, cots, wgu, wd, acc, acc_h, g2, hid, q, r, in_f, in_b, out_f, out_b, fin, grad_gu, grad_d,
     ret_ref, op, cin, cout, halo, mix, mcf, col, acc2,
     w_sem, disp_send, disp_recv,
     af_send, af_recv, ab_send, ab_recv, ap_send, ap_recv,
@@ -29,12 +30,22 @@
     halo_send, halo_recv, mix_send, mix_recv,
     mf_send, mf_recv, mb_send, mb_recv, mp_send, mp_recv,
     col_send, col_recv, colp_send, colp_recv,
+    tf_send, tf_recv, tb_send, tb_recv, cot_sent, cot_recv, cp_send, cp_recv,
 ):
     s = lax.axis_index("sp")
     t = lax.axis_index("tp")
     z, c = t // 2, t % 2
     y = s // 4
     up, down, mate = ((z + 1) % 8) * 2 + c, ((z + 7) % 8) * 2 + c, z * 2 + (1 - c)
+
+    barrier = pltpu.get_barrier_semaphore()
+
+    @pl.loop(1, 16)
+    def _(i):
+        pl.semaphore_signal(barrier, inc=1, device_id={"sp": (s + i) % 16}, device_id_type=MESH)
+
+    for other in (up, down, mate):
+        pl.semaphore_signal(barrier, inc=1, device_id={"tp": other}, device_id_type=MESH)
 
     weights = [
         pltpu.make_async_copy(wg_ref, wgu.at[:, :, pl.ds(0, 128)], w_sem.at[0]),
@@ -47,14 +58,23 @@
 
     cin[...] = ig_ref[...].astype(F32) * val_ref[...].astype(F32)
 
-    barrier = pltpu.get_barrier_semaphore()
-
-    @pl.loop(1, 16)
-    def _(i):
-        pl.semaphore_signal(barrier, inc=1, device_id={"sp": (s + i) % 16}, device_id_type=MESH)
-
-    for other in (up, down, mate):
-        pl.semaphore_signal(barrier, inc=1, device_id={"tp": other}, device_id_type=MESH)
+    expert = lax.broadcasted_iota(jnp.int32, (16, 256), 0)
+    named = [ids_ref[i : i + 1, :] == expert for i in range(2)]
+    member = jnp.where(named[0] | named[1], 1.0, 0.0)
+    weight = jnp.where(named[0], gates_ref[0:1, :], 0.0) + jnp.where(named[1], gates_ref[1:2, :], 0.0)
+    row = lax.broadcasted_iota(jnp.int32, (256, 256), 0)
+    earlier = jnp.where(row < lax.broadcasted_iota(jnp.int32, (256, 256), 1), 1.0, 0.0).astype(BF16)
+    place = jnp.where(member > 0, dot(member.astype(BF16), earlier, NN), -1.0)
+    position = lax.broadcasted_iota(jnp.int32, (48, 256), 0).astype(F32)
+    for e in range(16):
+        hit = place[e : e + 1, :] == position
+        pick_ref[e] = jnp.where(hit, 1.0, 0.0).astype(BF16)
+        slot_weight = jnp.sum(jnp.where(hit, weight[e : e + 1, :], 0.0), axis=1, keepdims=True)
+        scale[e] = jnp.broadcast_to(slot_weight, (48, 128))
+    tokens[z] = cot_ref[...].reshape(2, 128, 256)
+    acc[...] = jnp.zeros_like(acc)
+    acc_h[...] = jnp.zeros_like(acc_h)
+
     pl.semaphore_wait(barrier, 18)
 
     def remote(src, dst, send_sem, recv_sem, **where):
@@ -63,21 +83,43 @@
             device_id=where, device_id_type=MESH,
         )
 
+    def part(k):
+        return pl.ds(4 * ((y + 4 - k) % 4), 4)
+
+    def token_f(d, k):
+        at = tokens.at[(z + 8 - d) % 8, k]
+        return remote(at, at, tf_send.at[d, k], tf_recv.at[d, k], tp=up)
+
+    def token_b(d, k):
+        at = tokens.at[(z + d) % 8, k]
+        return remote(at, at, tb_send.at[d, k], tb_recv.at[d, k], tp=down)
+
+    for k in range(2):
+        from_cot = cot_ref.at[pl.ds(128 * k, 128)]
+        remote(from_cot, tokens.at[z, k], tf_send.at[0, k], tf_recv.at[0, k], tp=up).start()
+        remote(from_cot, tokens.at[z, k], tb_send.at[0, k], tb_recv.at[0, k], tp=down).start()
+
     def dispatch(peer, source):
         return remote(
-            send_ref.at[peer], rows.at[t, source], disp_send.at[peer], disp_recv.at[source], sp=peer
+            x_send.at[peer], rows.at[t, source], disp_send.at[peer], disp_recv.at[source], sp=peer
         )
 
-    own = pltpu.make_async_copy(send_ref.at[s], rows.at[t, s], disp_recv.at[s])
-    own.start()
+    own = pltpu.make_async_copy(x_send.at[s], rows.at[t, s], disp_recv.at[s])
+
+    def dispatch_cot(zz, peer, source):
+        return remote(
+            cot_send.at[zz, peer], cots.at[zz * 2 + c, source],
+            cot_sent.at[zz, peer], cot_recv.at[zz, source], sp=peer,
+        )
+
+    def own_cot(zz):
+        return pltpu.make_async_copy(cot_send.at[zz, s], cots.at[zz * 2 + c, s], cot_recv.at[zz, s])
 
     def halo_copies(h):
         return [
             remote(cin.at[pl.ds(248, 8)], halo.at[h, 0], halo_send.at[h, 0], halo_recv.at[h, 0], sp=(s + 1) % 16),
             remote(cin.at[pl.ds(0, 8)], halo.at[h, 1], halo_send.at[h, 1], halo_recv.at[h, 1], sp=(s + 15) % 16),
         ]
-
-    row = lax.broadcasted_iota(jnp.int32, (256, 256), 0)
 
     def neighbours(h):
         for copy in halo_copies(h):
@@ -92,9 +134,42 @@
     for copy in halo_copies(0):
         copy.start()
 
-    @pl.loop(1, 16)
-    def _(i):
-        dispatch((s + i) % 16, s).start()
+    def selected(k, table):
+        return dot(pick_ref[part(k)].reshape(192, 256), table, NN)
+
+    @pl.loop(0, 4)
+    def _(k):
+        x_send[part(k)] = selected(k, x_ref[...]).astype(BF16).reshape(4, 48, 256)
+        for x in range(4):
+            peer = 4 * ((y + 4 - k) % 4) + x
+
+            @pl.when(peer == s)
+            def _():
+                own.start()
+
+            @pl.when(peer != s)
+            def _():
+                dispatch(peer, s).start()
+
+    def send_cot(zz):
+        @pl.loop(0, 4)
+        def _(k):
+            value = selected(k, tokens[zz].reshape(256, 256))
+            factor = scale[part(k)].reshape(192, 128)
+            cot_send[zz, part(k), :, pl.ds(0, 128)] = (value[:, :128] * factor).astype(BF16).reshape(4, 48, 128)
+            cot_send[zz, part(k), :, pl.ds(128, 128)] = (value[:, 128:] * factor).astype(BF16).reshape(4, 48, 128)
+            for x in range(4):
+                peer = 4 * ((y + 4 - k) % 4) + x
+
+                @pl.when(peer == s)
+                def _():
+                    own_cot(zz).start()
+
+                @pl.when(peer != s)
+                def _():
+                    dispatch_cot(zz, peer, s).start()
+
+    send_cot(z)
 
     before, here, after = neighbours(0)
     conv = before * taps_ref[0:1, :] + here * taps_ref[1:2, :] + after * taps_ref[2:3, :]
@@ -104,12 +179,8 @@
     def mix_copy(peer, source):
         return remote(mix.at[source], mix.at[source], mix_send.at[peer], mix_recv.at[source], sp=peer)
 
-    acc[...] = jnp.zeros_like(acc)
     for w in weights:
         w.wait()
-
-    def part(k):
-        return pl.ds(4 * ((y + 4 - k) % 4), 4)
 
     def slice_of(zz, core, k):
         return rows.at[zz * 2 + core, part(k)]
@@ -127,15 +198,10 @@
         return remote(at, at, ap_send.at[zz, k], ap_recv.at[zz, k], tp=mate)
 
     def multiply(tt, k):
-        block = rows[tt, part(k)].reshape(192, 512)
-        pre = dot(block[:, :256], wgu[tt], (((1,), (0,)), ((), ())))
-        columns = pl.ds(pl.multiple_of(tt * 256, 256), 256)
-        hidden = dot(block[:, 256:], wd[:, columns], NT)
-        acc[part(k), :, pl.ds(0, 256)] += pre.reshape(4, 48, 256)
-        acc[part(k), :, pl.ds(256, 128)] += hidden.reshape(4, 48, 128)
-
-    @pl.loop(0, 4)
-    def _(k):
+        pre = dot(rows[tt, part(k)].reshape(192, 256), wgu[tt], NN)
+        acc[part(k)] += pre.reshape(4, 48, 256)
+
+    def ring_start(k):
         for x in range(4):
             source = 4 * ((y + 4 - k) % 4) + x
 
@@ -152,9 +218,66 @@
         to_mate(z, c, k).start()
         multiply(t, k)
 
-    @pl.loop(1, 16)
-    def _(i):
-        mix_copy((s + i) % 16, s).start()
+    @pl.loop(1, 5)
+    def _(d):
+        zf, zb = (z + 8 - d) % 8, (z + d) % 8
+        for k in range(2):
+            @pl.when((d < 4) | (k == 0))
+            def _():
+                at = tokens.at[zf, k]
+                remote(at, at, tf_send.at[d - 1, k], tf_recv.at[d - 1, k], tp=up).wait_recv()
+
+                @pl.when((d < 3) | ((d == 3) & (k == 0)))
+                def _():
+                    token_f(d, k).start()
+
+            @pl.when((d < 4) | (k == 1))
+            def _():
+                at = tokens.at[zb, k]
+                remote(at, at, tb_send.at[d - 1, k], tb_recv.at[d - 1, k], tp=down).wait_recv()
+
+                @pl.when((d < 3) | ((d == 3) & (k == 1)))
+                def _():
+                    token_b(d, k).start()
+
+        send_cot(zf)
+
+        @pl.when(d < 4)
+        def _():
+            send_cot(zb)
+
+        @pl.when((d == 2) | (d == 3))
+        def _():
+            @pl.loop(0, 2)
+            def _(k):
+                ring_start(2 * d - 4 + k)
+
+    def cot_mate(zz, core):
+        at = cots.at[zz * 2 + core]
+        return remote(at, at, cp_send.at[zz], cp_recv.at[zz], tp=mate)
+
+    def multiply_cot(tt):
+        columns = pl.ds(pl.multiple_of(tt * 256, 256), 256)
+        acc_h[...] += dot(cots[tt].reshape(768, 256), wd[:, columns], NT).reshape(16, 48, 128)
+
+    def nth(n):
+        return (z + 8 + (1 - 2 * (n % 2)) * ((n + 1) // 2)) % 8
+
+    def cot_own_part(n):
+        zz = nth(n)
+        own_cot(zz).wait()
+
+        @pl.loop(1, 16)
+        def _(i):
+            dispatch_cot(zz, (s + i) % 16, (s + i) % 16).wait_recv()
+
+        cot_mate(zz, c).start()
+        multiply_cot(zz * 2 + c)
+
+    def cot_mate_part(n):
+        zz = nth(n)
+        cot_mate(zz, 1 - c).wait_recv()
+        multiply_cot(zz * 2 + 1 - c)
 
     def mate_part(zz, k):
         to_mate(zz, 1 - c, k).wait_recv()
@@ -209,9 +332,27 @@
             mate_part((z + 8 - e) % 8, k)
             mate_part((z + e) % 8, k)
 
+        @pl.when((i >= 3) & (i % 2 == 1))
+        def _():
+            cot_own_part((i - 3) // 2)
+
+        @pl.when((i >= 4) & (i % 2 == 0))
+        def _():
+            cot_mate_part((i - 4) // 2)
+
     @pl.loop(0, 4)
     def _(k):
         mate_part((z + 4) % 8, k)
+
+    cot_own_part(7)
+
+    @pl.loop(6, 8)
+    def _(n):
+        cot_mate_part(n)
+
+    @pl.loop(1, 16)
+    def _(i):
+        mix_copy((s + i) % 16, s).start()
 
     def dots_of(tt, k):
         return dot(g2[part(k)].reshape(192, 256), wgu[tt], NT)
@@ -225,8 +366,9 @@
 
     @pl.loop(0, 4)
     def _(k):
-        block = acc[part(k)].reshape(192, 384)
-        pre_gate, pre_up, grad_hidden = block[:, :128], block[:, 128:256], block[:, 256:]
+        block = acc[part(k)].reshape(192, 256)
+        pre_gate, pre_up = block[:, :128], block[:, 128:]
+        grad_hidden = acc_h[part(k)].reshape(192, 128)
         sig = jax.nn.sigmoid(pre_gate)
         activated = pre_gate * sig
         hid[part(k)] = (activated * pre_up).astype(BF16).reshape(4, 48, 128)
@@ -261,8 +403,8 @@
         ).start()
 
     def grads(tt):
-        x = rows[tt, :, :, pl.ds(0, 256)].reshape(768, 256)
-        cot = rows[tt, :, :, pl.ds(256, 256)].reshape(768, 256)
+        x = rows[tt].reshape(768, 256)
+        cot = cots[tt].reshape(768, 256)
         grad_gu[tt] = dot(x, g2[...].reshape(768, 256), TN)
         columns = pl.ds(pl.multiple_of(tt * 256, 256), 256)
         grad_d[:, columns] = dot(hid[...].reshape(768, 128), cot, TN)
@@ -329,7 +471,7 @@
 
     mine.wait()
 
-    moe_grad = dot(pick_ref[...], ret_ref[...].reshape(768, 256), TN)
+    moe_grad = dot(pick_ref[...].reshape(768, 256), ret_ref[...].reshape(768, 256), TN)
     mixer = (cot_ref[...].astype(F32) + moe_grad).astype(BF16)
     mcf[t] = mixer.reshape(2, 128, 256)
     acc2[...] = jnp.zeros_like(acc2)
@@ -355,83 +497,70 @@
 
     kept = pltpu.make_async_copy(mcf.at[s, c], col.at[s, c], col_recv.at[s])
 
-    def use(tt, k):
-        @pl.when((k == c) & (tt == s))
+    def use(tt):
+        @pl.when(tt == s)
         def _():
             kept.start()
 
-        @pl.when((k == c) & (tt != s))
+        @pl.when(tt != s)
         def _():
             column(tt, s).start()
 
-        acc2[k] += dot(mcf[tt, k], op[tt], (((1,), (0,)), ((), ())))
+        acc2[...] += dot(mcf[tt].reshape(256, 256), op[tt], NN)
 
     for k in range(2):
         mc_f(0, k).start()
         mc_b(0, k).start()
         mc_mate(z, c, k).start()
-    for k in range(2):
-        use(t, k)
-
-    def mc_mate_part(zz, k):
-        mc_mate(zz, 1 - c, k).wait_recv()
-        use(zz * 2 + 1 - c, k)
-
-    @pl.loop(0, 8)
-    def _(i):
-        d, k = i // 2 + 1, i % 2
+    use(t)
+
+    def mc_mate_part(zz):
+        for k in range(2):
+            mc_mate(zz, 1 - c, k).wait_recv()
+        use(zz * 2 + 1 - c)
+
+    @pl.loop(1, 5)
+    def _(d):
         zf, zb = (z + 8 - d) % 8, (z + d) % 8
-        goes_f = (d < 4) | (k == 0)
-        goes_b = (d < 4) | (k == 1)
-
-        @pl.when(goes_f)
-        def _():
-            at = mcf.at[zf * 2 + c, k]
-            remote(at, at, mf_send.at[d - 1, k], mf_recv.at[d - 1, k], tp=up).wait_recv()
-
-            @pl.when((d < 3) | ((d == 3) & (k == 0)))
-            def _():
-                mc_f(d, k).start()
-
-            mc_mate(zf, c, k).start()
-
-        @pl.when(goes_b)
-        def _():
-            at = mcf.at[zb * 2 + c, k]
-            remote(at, at, mb_send.at[d - 1, k], mb_recv.at[d - 1, k], tp=down).wait_recv()
-
-            @pl.when((d < 3) | ((d == 3) & (k == 1)))
-            def _():
-                mc_b(d, k).start()
-
-        @pl.when(goes_b)
-        def _():
-            mc_mate(zb, c, k).start()
-
-        @pl.when(goes_f)
-        def _():
-            use(zf * 2 + c, k)
-
-        @pl.when(goes_b)
-        def _():
-            use(zb * 2 + c, k)
-
-        e = i // 2
-
-        @pl.when(e == 0)
-        def _():
-            mc_mate_part(z, k)
-
-        @pl.when(e > 0)
-        def _():
-            mc_mate_part((z + 8 - e) % 8, k)
-            mc_mate_part((z + e) % 8, k)
-
-    @pl.loop(0, 2)
-    def _(k):
-        mc_mate_part((z + 4) % 8, k)
-
-    grad_mixed = acc2[...].reshape(256, 256)
+        for k in range(2):
+            @pl.when((d < 4) | (k == 0))
+            def _():
+                at = mcf.at[zf * 2 + c, k]
+                remote(at, at, mf_send.at[d - 1, k], mf_recv.at[d - 1, k], tp=up).wait_recv()
+
+                @pl.when((d < 3) | ((d == 3) & (k == 0)))
+                def _():
+                    mc_f(d, k).start()
+
+                mc_mate(zf, c, k).start()
+
+            @pl.when((d < 4) | (k == 1))
+            def _():
+                at = mcf.at[zb * 2 + c, k]
+                remote(at, at, mb_send.at[d - 1, k], mb_recv.at[d - 1, k], tp=down).wait_recv()
+
+                @pl.when((d < 3) | ((d == 3) & (k == 1)))
+                def _():
+                    mc_b(d, k).start()
+
+            @pl.when((d < 4) | (k == 1))
+            def _():
+                mc_mate(zb, c, k).start()
+
+        use(zf * 2 + c)
+        mc_mate_part((z + 9 - d) % 8)
+
+        @pl.when(d < 4)
+        def _():
+            use(zb * 2 + c)
+
+        @pl.when(d > 1)
+        def _():
+            mc_mate_part((z + d - 1) % 8)
+
+    mc_mate_part((z + 4) % 8)
+
+    grad_mixed = acc2[...]
     gog_ref[...] = (grad_mixed * cout[...]).astype(BF16)
     cin[...] = grad_mixed * og_ref[...].astype(F32)
     for copy in halo_copies(1):
@@ -471,9 +600,18 @@
         mix_copy((s + i) % 16, s).wait_send()
         column((s + i) % 16, s).wait_send()
 
+        @pl.loop(0, 8)
+        def _(zz):
+            dispatch_cot(zz, (s + i) % 16, s).wait_send()
+
     @pl.loop(0, 16)
     def _(i):
         column_mate(i, c).wait_send()
+
+        @pl.when(i < 8)
+        def _():
+            cot_mate(i, c).wait_send()
+
         mc_mate(i // 2, c, i % 2).wait_send()
 
     @pl.loop(0, 8)
@@ -482,10 +620,12 @@
 
         @pl.when((d < 3) | (k == 0))
         def _():
+            token_f(d, k).wait_send()
             mc_f(d, k).wait_send()
 
         @pl.when((d < 3) | (k == 1))
         def _():
+            token_b(d, k).wait_send()
             mc_b(d, k).wait_send()
 
     @pl.loop(0, 16)
@@ -529,13 +669,20 @@
             jax.ShapeDtypeStruct((16, 256, 128), F32),
             jax.ShapeDtypeStruct((128, 4096), F32),
         ),
-        in_specs=[vmem] * 7 + [any_] * 4,
+        in_specs=[vmem] * 8 + [any_] * 4,
         out_specs=(vmem,) * 4 + (any_,) * 3,
         scratch_shapes=[
-            vm((16, 16, 48, 512), BF16),
+            vm((16, 48, 256), BF16),
+            vm((16, 48, 128), F32),
+            vm((8, 2, 128, 256), BF16),
+            vm((16, 48, 256), BF16),
+            vm((8, 16, 48, 256), BF16),
+            vm((16, 16, 48, 256), BF16),
+            vm((16, 16, 48, 256), BF16),
             vm((16, 256, 256), BF16),
             vm((128, 4096), BF16),
-            vm((16, 48, 384), F32),
+            vm((16, 48, 256), F32),
+            vm((16, 48, 128), F32),
             vm((16, 48, 256), BF16),
             vm((16, 48, 128), BF16),
             vm((8, 16, 48, 256), BF16),
@@ -555,7 +702,7 @@
             vm((16, 256, 256), BF16),
             vm((16, 2, 128, 256), BF16),
             vm((16, 2, 128, 256), BF16),
-            vm((2, 128, 256), F32),
+            vm((256, 256), F32),
             dma(4), dma(16), dma(16),
             dma(4, 4), dma(4, 4), dma(4, 4), dma(4, 4), dma(8, 4), dma(8, 4),
             dma(8, 4), dma(8, 4), dma(4, 4), dma(4, 4), dma(4, 4), dma(4, 4),
@@ -563,37 +710,65 @@
             dma(2, 2), dma(2, 2), dma(16), dma(16),
             dma(4, 2), dma(4, 2), dma(4, 2), dma(4, 2), dma(8, 2), dma(8, 2),
             dma(16), dma(16), dma(16), dma(16),
+            dma(4, 2), dma(4, 2), dma(4, 2), dma(4, 2), dma(8, 16), dma(8, 16), dma(8), dma(8),
         ],
         compiler_params=pltpu.CompilerParams(
-            collective_id=1, has_side_effects=True, vmem_limit_bytes=60 * 1024 * 1024
+            collective_id=1, has_side_effects=True, vmem_limit_bytes=67043328
         ),
         cost_estimate=pl.CostEstimate(flops=8_000_000_000, bytes_accessed=20_000_000, transcendentals=100_000),
         name="mixer_and_experts",
     )(*operands)
 
 
+def write_out(*refs):
+    count = len(refs) // 3
+    sources, targets, held = refs[:count], refs[count : 2 * count], refs[2 * count : 3 * count]
+    in_sem, out_sem = refs[3 * count :]
+    steps = []
+    for i, ref in enumerate(sources):
+        pieces = 4 if i < 3 else 1
+        size = ref.shape[0] // pieces
+        for p in range(pieces):
+            at = pl.ds(p * size, size)
+            n = len(steps)
+            steps.append((
+                pltpu.make_async_copy(ref.at[at], held[i].at[at], in_sem.at[n]),
+                pltpu.make_async_copy(held[i].at[at], targets[i].at[at], out_sem.at[n]),
+            ))
+    for fetch, _ in steps:
+        fetch.start()
+    for fetch, store in steps:
+        fetch.wait()
+        store.start()
+    for _, store in steps:
+        store.wait()
+
+
+def written(*arrays):
+    any_ = pl.BlockSpec(memory_space=pl.ANY)
+    shapes = [jax.ShapeDtypeStruct(a.shape, a.dtype) for a in arrays]
+    return pl.pallas_call(
+        write_out,
+        out_shape=tuple(shapes),
+        in_specs=[any_] * len(shapes),
+        out_specs=(any_,) * len(shapes),
+        scratch_shapes=[pltpu.VMEM(a.shape, a.dtype) for a in shapes]
+        + [pltpu.SemaphoreType.DMA((16,)), pltpu.SemaphoreType.DMA((16,))],
+        compiler_params=pltpu.CompilerParams(vmem_limit_bytes=16 * 1024 * 1024),
+        name="write_out",
+    )(*arrays)
+
+
 def body(moe_input, out_gate, in_gate, values, conv_taps, out_proj, route_ids, route_gates, expert_gate, expert_up, expert_down, cotangent):
-    experts = jnp.arange(16, dtype=jnp.int32)
-    chosen = route_ids[:, :, None] == experts[None, None, :]
-    member = jnp.sum(chosen.astype(F32), axis=1)
-    weight = jnp.sum(jnp.where(chosen, route_gates[:, :, None], 0.0), axis=1)
-    tokens = jnp.arange(256, dtype=jnp.int32)
-    earlier = (tokens[:, None] > tokens[None, :]).astype(BF16)
-    place = jnp.dot(earlier, member.astype(BF16), preferred_element_type=F32)
-    place = jnp.where(member > 0, place, -1.0)
-    pick = place.T[:, None, :] == jnp.arange(48, dtype=F32)[None, :, None]
-    slot_weight = jnp.sum(jnp.where(pick, weight.T[:, None, :], 0.0), axis=2)
-    pick = pick.astype(BF16).reshape(768, 256)
-    both = jnp.dot(pick, jnp.concatenate([moe_input, cotangent], axis=1), preferred_element_type=F32)
-    scale = slot_weight.reshape(768, 1)
-    send = jnp.concatenate([both[:, :256], both[:, 256:] * scale], axis=1).astype(BF16).reshape(16, 48, 512)
-
     gog, gig, gval, gop, gg, gu, gd = mixer_and_experts(
-        send, pick, cotangent, out_gate, in_gate, values, conv_taps,
+        route_ids.T, route_gates.T, moe_input, cotangent, out_gate, in_gate, values, conv_taps,
         expert_gate.reshape(16, 256, 128),
         expert_up.reshape(16, 256, 128),
         expert_down.reshape(128, 4096),
         out_proj.reshape(16, 256, 256),
+    )
+    gg, gu, gd, gop, gog, gig, gval = written(
+        gg.reshape(4096, 128), gu.reshape(4096, 128), gd, gop, gog, gig, gval
     )
     return (gog, gig, gval, gop, gg.reshape(1, 4096, 128), gu.reshape(1, 4096, 128), gd.reshape(1, 128, 4096))
 

time: 180 us -> 157 us (0.87)
  Pallas kernels: 161 us -> 147 us
  local copies, waits for them, and re-layouts: 13.4 us -> 8.43 us
  other arithmetic: 3.02 us -> 0 us
    pallas_call x1, Pallas kernels: 161 us -> 143 us  [mixer_and_experts(): pl.pallas_call(moe_kernel, out_shape=(tile, tile, tile, jax.ShapeDtypeStr...]
    unnamed x11 -> x14, local copies, waits for them, and re-layouts: 13.2 us -> 8.43 us
    pallas_call x0 -> x1, Pallas kernels: none -> 4.05 us  [written(): pl.pallas_call(write_out, out_shape=tuple(shapes), in_specs=[any_] * len(...]
where the time goes in v3:
time: 157 us; the launch traced here: 156 us
  Pallas kernels  147 us (94%)
  local copies, waits for them, and re-layouts  8.43 us (5%)
    pallas_call x1, Pallas kernels, mixer_and_experts(): pl.pallas_call(moe_kernel, out_shape=(tile, tile, tile, jax.ShapeDtypeStr...  143 us
    unnamed x14, local copies, waits for them, and re-layouts  8.43 us
    pallas_call x1, Pallas kernels, written(): pl.pallas_call(write_out, out_shape=tuple(shapes), in_specs=[any_] * len(...  4.05 us

profile of v3, /device:TPU:17, one launch (start us, length us, event | category | flops | bytes accessed | tf_op | source)
XLA Modules:
  0.0 156.2 jit_solution(11548518423960955186)
XLA Ops:
  0.6 143.1 %mixer_and_experts.1 = (bf16[256,256]{1,0:T(8,128)(2,1)}, bf16[256,256]{1,0:T(8,128)(2,1)}, bf16[256,256]{1,0:T(8,128)(2,1)}, f32[256,256]{1,0:T(8,128)}, f32[16...) custom-call(s32[2,256]{1,0:T(2,128)} %bitcast.20, f32[2,256]{1,0:T(2,128)} %bitcast.21, ...), custom_call_target="tpu_custom_call" | custom-call | flops 8000000000 | bytes 20000000 | tf_op jit(solution)/shard_map/mixer_and_experts/pallas_call | solution.py:663
  143.7 0.0 copy-start
  143.7 1.6 %copy-done = f32[16,256,128]{2,1,0:T(8,128)S(1)} copy-done((f32[16,256,128]{2,1,0:T(8,128)S(1)}, f32[16,256,128]{2,1,0:T(8,128)}, u32[]{:S(2)}) %copy-start) | copy-done | bytes 2097176
  145.3 0.0 copy-start.1
  145.3 1.6 %copy-done.1 = f32[16,256,128]{2,1,0:T(8,128)S(1)} copy-done((f32[16,256,128]{2,1,0:T(8,128)S(1)}, f32[16,256,128]{2,1,0:T(8,128)}, u32[]{:S(2)}) %copy-start.1) | copy-done | bytes 2097176
  146.9 0.0 copy-start.2
  146.9 1.6 %copy-done.2 = f32[128,4096]{1,0:T(8,128)S(1)} copy-done((f32[128,4096]{1,0:T(8,128)S(1)}, f32[128,4096]{1,0:T(8,128)}, u32[]{:S(2)}) %copy-start.2) | copy-done | bytes 2097176
  148.5 0.0 copy-start.3
  148.5 0.9 copy-done.3
  149.5 0.0 copy-start.4
  149.5 0.9 copy-done.4
  150.4 0.0 copy-start.5
  150.4 0.9 copy-done.5
  151.3 0.0 copy-start.6
  151.3 0.9 copy-done.6
  152.2 4.1 %write_out.1 = (f32[4096,128]{1,0:T(8,128)}, f32[4096,128]{1,0:T(8,128)}, f32[128,4096]{1,0:T(8,128)}, f32[256,256]{1,0:T(8,128)}, bf16[256,256]{1,0:T(8,128)(2,...) custom-call(f32[4096,128]{1,0:T(8,128)S(1)} %bitcast.11, f32[4096,128]{1,0:T(8,128)S(1)} %bitcast.12, ...), custom_call_target="tpu_custom_call" | custom-call | tf_op jit(solution)/shard_map/write_out/pallas_call | solution.py:750
Async XLA Ops:
  143.7 1.6 %copy-start = (f32[16,256,128]{2,1,0:T(8,128)S(1)}, f32[16,256,128]{2,1,0:T(8,128)}, u32[]{:S(2)}) copy-start(f32[16,256,128]{2,1,0:T(8,128)} %get-tuple-element.21) | copy-start | bytes 6291460
  145.3 1.6 %copy-start.1 = (f32[16,256,128]{2,1,0:T(8,128)S(1)}, f32[16,256,128]{2,1,0:T(8,128)}, u32[]{:S(2)}) copy-start(f32[16,256,128]{2,1,0:T(8,128)} %get-tuple-element.22) | copy-start | bytes 6291460
  146.9 1.6 %copy-start.2 = (f32[128,4096]{1,0:T(8,128)S(1)}, f32[128,4096]{1,0:T(8,128)}, u32[]{:S(2)}) copy-start(f32[128,4096]{1,0:T(8,128)} %get-tuple-element.23.refs_2_) | copy-start | bytes 6291460
  148.5 0.9 copy-start.3
  149.5 0.9 copy-start.4
  150.4 0.9 copy-start.5
  151.3 0.9 copy-start.6

commit v4 on v3

--- a/solution.py
+++ b/solution.py
@@ -18,19 +18,19 @@
     return lax.dot_general(a, b, dims, preferred_element_type=F32)
 
 
+(DISPATCH, ROWS, COT, COT_MATE, TOKEN_RING, HALO, HALO_BACK, MIXED, MATE_SUMS, SUMS, RETURNED,
+ MIXER, COLUMN, COLUMN_MATE) = range(14)
+
+
 def moe_kernel(
     ids_ref, gates_ref, x_ref, cot_ref, og_ref, ig_ref, val_ref, taps_ref, wg_ref, wu_ref, wd_ref, op_ref,
     gog_ref, gig_ref, gval_ref, gop_ref, gg_ref, gu_ref, gd_ref,
     pick_ref, scale, tokens, x_send, cot_send, rows, cots, wgu, wd, acc, acc_h, g2, hid, q, r, in_f, in_b, out_f, out_b, fin, grad_gu, grad_d,
-    ret_ref, op, cin, cout, halo, mix, mcf, col, acc2,
-    w_sem, disp_send, disp_recv,
-    af_send, af_recv, ab_send, ab_recv, ap_send, ap_recv,
-    rp_send, rp_recv, rf_send, rf_recv, rb_send, rb_recv,
-    ret_send, ret_recv, out_sem,
-    halo_send, halo_recv, mix_send, mix_recv,
-    mf_send, mf_recv, mb_send, mb_recv, mp_send, mp_recv,
-    col_send, col_recv, colp_send, colp_recv,
-    tf_send, tf_recv, tb_send, tb_recv, cot_sent, cot_recv, cp_send, cp_recv,
+    ret_ref, op, cin, cout, halo, mix_t, mcf, col, acc2,
+    w_sem, out_sem, sent,
+    disp_recv, af_recv, ab_recv, ap_recv, rp_recv, rf_recv, rb_recv, ret_recv,
+    halo_recv, mix_recv, mf_recv, mb_recv, mp_recv, col_recv, colp_recv,
+    tf_recv, tb_recv, cot_recv, cp_recv,
 ):
     s = lax.axis_index("sp")
     t = lax.axis_index("tp")
@@ -88,42 +88,46 @@
 
     def token_f(d, k):
         at = tokens.at[(z + 8 - d) % 8, k]
-        return remote(at, at, tf_send.at[d, k], tf_recv.at[d, k], tp=up)
+        return remote(at, at, sent.at[TOKEN_RING], tf_recv.at[d, k], tp=up)
 
     def token_b(d, k):
         at = tokens.at[(z + d) % 8, k]
-        return remote(at, at, tb_send.at[d, k], tb_recv.at[d, k], tp=down)
+        return remote(at, at, sent.at[TOKEN_RING], tb_recv.at[d, k], tp=down)
 
     for k in range(2):
         from_cot = cot_ref.at[pl.ds(128 * k, 128)]
-        remote(from_cot, tokens.at[z, k], tf_send.at[0, k], tf_recv.at[0, k], tp=up).start()
-        remote(from_cot, tokens.at[z, k], tb_send.at[0, k], tb_recv.at[0, k], tp=down).start()
-
-    def dispatch(peer, source):
+        remote(from_cot, tokens.at[z, k], sent.at[TOKEN_RING], tf_recv.at[0, k], tp=up).start()
+        remote(from_cot, tokens.at[z, k], sent.at[TOKEN_RING], tb_recv.at[0, k], tp=down).start()
+
+    def dispatch(peer):
+        return remote(x_send.at[peer], rows.at[t, s], sent.at[DISPATCH], disp_recv.at[y], sp=peer)
+
+    own = pltpu.make_async_copy(x_send.at[s], rows.at[t, s], disp_recv.at[y])
+
+    def dispatch_cot(zz, peer):
         return remote(
-            x_send.at[peer], rows.at[t, source], disp_send.at[peer], disp_recv.at[source], sp=peer
+            cot_send.at[zz, peer], cots.at[zz * 2 + c, s], sent.at[COT], cot_recv.at[zz], sp=peer
         )
 
-    own = pltpu.make_async_copy(x_send.at[s], rows.at[t, s], disp_recv.at[s])
-
-    def dispatch_cot(zz, peer, source):
-        return remote(
-            cot_send.at[zz, peer], cots.at[zz * 2 + c, source],
-            cot_sent.at[zz, peer], cot_recv.at[zz, source], sp=peer,
-        )
-
     def own_cot(zz):
-        return pltpu.make_async_copy(cot_send.at[zz, s], cots.at[zz * 2 + c, s], cot_recv.at[zz, s])
+        return pltpu.make_async_copy(cot_send.at[zz, s], cots.at[zz * 2 + c, s], cot_recv.at[zz])
+
+    def arrived(at, recv_sem):
+        remote(at, at, recv_sem, recv_sem, tp=mate).wait_recv()
+
+    def sent_all(at, index):
+        remote(at, at, sent.at[index], sent.at[index], tp=mate).wait_send()
 
     def halo_copies(h):
         return [
-            remote(cin.at[pl.ds(248, 8)], halo.at[h, 0], halo_send.at[h, 0], halo_recv.at[h, 0], sp=(s + 1) % 16),
-            remote(cin.at[pl.ds(0, 8)], halo.at[h, 1], halo_send.at[h, 1], halo_recv.at[h, 1], sp=(s + 15) % 16),
+            remote(cin.at[pl.ds(248, 8)], halo.at[h, 0], sent.at[HALO + h], halo_recv.at[h, 0], sp=(s + 1) % 16),
+            remote(cin.at[pl.ds(0, 8)], halo.at[h, 1], sent.at[HALO + h], halo_recv.at[h, 1], sp=(s + 15) % 16),
         ]
 
     def neighbours(h):
         for copy in halo_copies(h):
-            copy.wait()
+            copy.wait_recv()
+        sent_all(halo.at[h], HALO + h)
         array = cin[...]
         first = jnp.where(s > 0, halo[h, 0, 7:8, :], 0.0)
         last = jnp.where(s < 15, halo[h, 1, 0:1, :], 0.0)
@@ -149,7 +153,7 @@
 
             @pl.when(peer != s)
             def _():
-                dispatch(peer, s).start()
+                dispatch(peer).start()
 
     def send_cot(zz):
         @pl.loop(0, 4)
@@ -167,17 +171,9 @@
 
                 @pl.when(peer != s)
                 def _():
-                    dispatch_cot(zz, peer, s).start()
+                    dispatch_cot(zz, peer).start()
 
     send_cot(z)
-
-    before, here, after = neighbours(0)
-    conv = before * taps_ref[0:1, :] + here * taps_ref[1:2, :] + after * taps_ref[2:3, :]
-    cout[...] = conv
-    mix[s] = (og_ref[...].astype(F32) * conv).astype(BF16)
-
-    def mix_copy(peer, source):
-        return remote(mix.at[source], mix.at[source], mix_send.at[peer], mix_recv.at[source], sp=peer)
 
     for w in weights:
         w.wait()
@@ -187,32 +183,22 @@
 
     def along_f(d, k):
         at = slice_of((z + 8 - d) % 8, c, k)
-        return remote(at, at, af_send.at[d, k], af_recv.at[d, k], tp=up)
+        return remote(at, at, sent.at[ROWS], af_recv.at[d, k], tp=up)
 
     def along_b(d, k):
         at = slice_of((z + d) % 8, c, k)
-        return remote(at, at, ab_send.at[d, k], ab_recv.at[d, k], tp=down)
+        return remote(at, at, sent.at[ROWS], ab_recv.at[d, k], tp=down)
 
     def to_mate(zz, core, k):
         at = slice_of(zz, core, k)
-        return remote(at, at, ap_send.at[zz, k], ap_recv.at[zz, k], tp=mate)
+        return remote(at, at, sent.at[ROWS], ap_recv.at[zz, k], tp=mate)
 
     def multiply(tt, k):
         pre = dot(rows[tt, part(k)].reshape(192, 256), wgu[tt], NN)
         acc[part(k)] += pre.reshape(4, 48, 256)
 
     def ring_start(k):
-        for x in range(4):
-            source = 4 * ((y + 4 - k) % 4) + x
-
-            @pl.when(source == s)
-            def _():
-                own.wait()
-
-            @pl.when(source != s)
-            def _():
-                dispatch(source, source).wait_recv()
-
+        arrived(slice_of(z, c, k), disp_recv.at[(y + 4 - k) % 4])
         along_f(0, k).start()
         along_b(0, k).start()
         to_mate(z, c, k).start()
@@ -225,7 +211,7 @@
             @pl.when((d < 4) | (k == 0))
             def _():
                 at = tokens.at[zf, k]
-                remote(at, at, tf_send.at[d - 1, k], tf_recv.at[d - 1, k], tp=up).wait_recv()
+                remote(at, at, sent.at[TOKEN_RING], tf_recv.at[d - 1, k], tp=up).wait_recv()
 
                 @pl.when((d < 3) | ((d == 3) & (k == 0)))
                 def _():
@@ -234,27 +220,22 @@
             @pl.when((d < 4) | (k == 1))
             def _():
                 at = tokens.at[zb, k]
-                remote(at, at, tb_send.at[d - 1, k], tb_recv.at[d - 1, k], tp=down).wait_recv()
+                remote(at, at, sent.at[TOKEN_RING], tb_recv.at[d - 1, k], tp=down).wait_recv()
 
                 @pl.when((d < 3) | ((d == 3) & (k == 1)))
                 def _():
                     token_b(d, k).start()
 
+        ring_start(d - 1)
         send_cot(zf)
 
         @pl.when(d < 4)
         def _():
             send_cot(zb)
-
-        @pl.when((d == 2) | (d == 3))
-        def _():
-            @pl.loop(0, 2)
-            def _(k):
-                ring_start(2 * d - 4 + k)
 
     def cot_mate(zz, core):
         at = cots.at[zz * 2 + core]
-        return remote(at, at, cp_send.at[zz], cp_recv.at[zz], tp=mate)
+        return remote(at, at, sent.at[COT_MATE], cp_recv.at[zz], tp=mate)
 
     def multiply_cot(tt):
         columns = pl.ds(pl.multiple_of(tt * 256, 256), 256)
@@ -265,12 +246,7 @@
 
     def cot_own_part(n):
         zz = nth(n)
-        own_cot(zz).wait()
-
-        @pl.loop(1, 16)
-        def _(i):
-            dispatch_cot(zz, (s + i) % 16, (s + i) % 16).wait_recv()
-
+        arrived(cots.at[zz * 2 + c], cot_recv.at[zz])
         cot_mate(zz, c).start()
         multiply_cot(zz * 2 + c)
 
@@ -292,7 +268,7 @@
         @pl.when((d < 4) | even)
         def _():
             at = slice_of(zf, c, k)
-            remote(at, at, af_send.at[d - 1, k], af_recv.at[d - 1, k], tp=up).wait_recv()
+            remote(at, at, sent.at[ROWS], af_recv.at[d - 1, k], tp=up).wait_recv()
 
             @pl.when((d < 3) | ((d == 3) & even))
             def _():
@@ -303,7 +279,7 @@
         @pl.when((d < 4) | (~even))
         def _():
             at = slice_of(zb, c, k)
-            remote(at, at, ab_send.at[d - 1, k], ab_recv.at[d - 1, k], tp=down).wait_recv()
+            remote(at, at, sent.at[ROWS], ab_recv.at[d - 1, k], tp=down).wait_recv()
 
             @pl.when((d < 3) | ((d == 3) & (~even)))
             def _():
@@ -350,9 +326,17 @@
     def _(n):
         cot_mate_part(n)
 
+    before, here, after = neighbours(0)
+    conv = before * taps_ref[0:1, :] + here * taps_ref[1:2, :] + after * taps_ref[2:3, :]
+    cout[...] = conv
+    mine_t = pl.ds(pl.multiple_of(s * 256, 256), 256)
+    mix_t[:, mine_t] = (og_ref[...].astype(F32) * conv).T.astype(BF16)
+
     @pl.loop(1, 16)
     def _(i):
-        mix_copy((s + i) % 16, s).start()
+        remote(
+            mix_t.at[:, mine_t], mix_t.at[:, mine_t], sent.at[MIXED], mix_recv.at[0], sp=(s + i) % 16
+        ).start()
 
     def dots_of(tt, k):
         return dot(g2[part(k)].reshape(192, 256), wgu[tt], NT)
@@ -361,7 +345,7 @@
         value = dots_of(zz * 2 + 1 - c, k)
         q[zz, part(k)] = value.astype(BF16).reshape(4, 48, 256)
         remote(
-            q.at[zz, part(k)], r.at[zz, part(k)], rp_send.at[zz, k], rp_recv.at[zz, k], tp=mate
+            q.at[zz, part(k)], r.at[zz, part(k)], sent.at[MATE_SUMS], rp_recv.at[zz, k], tp=mate
         ).start()
 
     @pl.loop(0, 4)
@@ -380,10 +364,10 @@
 
     def summed(zz, k):
         at = r.at[zz, part(k)]
-        remote(at, at, rp_send.at[zz, k], rp_recv.at[zz, k], tp=mate).wait_recv()
+        remote(at, at, sent.at[MATE_SUMS], rp_recv.at[zz, k], tp=mate).wait_recv()
         return dots_of(zz * 2 + c, k) + r[zz, part(k)].reshape(192, 256).astype(F32)
 
-    def ring_step(d, k, zz, incoming, outgoing, send_sem, recv_sem, to, starts):
+    def ring_step(d, k, zz, incoming, outgoing, recv_sem, to, starts):
         value = summed(zz, k)
 
         @pl.when(starts)
@@ -393,13 +377,13 @@
         @pl.when(jnp.logical_not(starts))
         def _():
             at = incoming.at[d, part(k)]
-            remote(at, at, send_sem.at[d, k], recv_sem.at[d, k], tp=to).wait_recv()
+            arrived(at, recv_sem.at[d, k])
             both = value + incoming[d, part(k)].reshape(192, 256).astype(F32)
             outgoing[d - 1, part(k)] = both.astype(BF16).reshape(4, 48, 256)
 
         remote(
             outgoing.at[d - 1, part(k)], incoming.at[d - 1, part(k)],
-            send_sem.at[d - 1, k], recv_sem.at[d - 1, k], tp=to,
+            sent.at[SUMS], recv_sem.at[d - 1, k], tp=to,
         ).start()
 
     def grads(tt):
@@ -414,9 +398,9 @@
     def outputs(tt):
         columns = pl.ds(pl.multiple_of(tt * 256, 256), 256)
         return [
-            pltpu.make_async_copy(grad_gu.at[tt, :, pl.ds(0, 128)], gg_ref.at[tt], out_sem.at[0, tt]),
-            pltpu.make_async_copy(grad_gu.at[tt, :, pl.ds(128, 128)], gu_ref.at[tt], out_sem.at[1, tt]),
-            pltpu.make_async_copy(grad_d.at[:, columns], gd_ref.at[:, columns], out_sem.at[2, tt]),
+            pltpu.make_async_copy(grad_gu.at[tt, :, pl.ds(0, 128)], gg_ref.at[tt], out_sem.at[0]),
+            pltpu.make_async_copy(grad_gu.at[tt, :, pl.ds(128, 128)], gu_ref.at[tt], out_sem.at[1]),
+            pltpu.make_async_copy(grad_d.at[:, columns], gd_ref.at[:, columns], out_sem.at[2]),
         ]
 
     @pl.loop(0, 16)
@@ -427,11 +411,11 @@
 
         @pl.when((d < 4) | even)
         def _():
-            ring_step(d, k, zf, in_f, out_f, rf_send, rf_recv, up, (d == 4) | ((d == 3) & (~even)))
+            ring_step(d, k, zf, in_f, out_f, rf_recv, up, (d == 4) | ((d == 3) & (~even)))
 
         @pl.when((d < 4) | (~even))
         def _():
-            ring_step(d, k, zb, in_b, out_b, rb_send, rb_recv, down, (d == 4) | ((d == 3) & even))
+            ring_step(d, k, zb, in_b, out_b, rb_recv, down, (d == 4) | ((d == 3) & even))
 
         prepare((z + d - 1) % 8, k)
 
@@ -441,17 +425,16 @@
 
         grads(i)
 
-    def giving_back(peer, source):
-        return remote(fin.at[peer], ret_ref.at[source], ret_send.at[peer], ret_recv.at[source], sp=peer)
-
-    mine = pltpu.make_async_copy(fin.at[s], ret_ref.at[s], ret_recv.at[s])
+    def giving_back(peer):
+        return remote(fin.at[peer], ret_ref.at[s], sent.at[RETURNED], ret_recv.at[0], sp=peer)
+
+    mine = pltpu.make_async_copy(fin.at[s], ret_ref.at[s], ret_recv.at[0])
 
     @pl.loop(0, 4)
     def _(k):
         value = summed(z, k)
-        for incoming, send_sem, recv_sem, to in ((in_f, rf_send, rf_recv, up), (in_b, rb_send, rb_recv, down)):
-            at = incoming.at[0, part(k)]
-            remote(at, at, send_sem.at[0, k], recv_sem.at[0, k], tp=to).wait_recv()
+        for incoming, recv_sem in ((in_f, rf_recv), (in_b, rb_recv)):
+            arrived(incoming.at[0, part(k)], recv_sem.at[0, k])
             value = value + incoming[0, part(k)].reshape(192, 256).astype(F32)
         fin[part(k)] = value.astype(BF16).reshape(4, 48, 256)
         for x in range(4):
@@ -463,39 +446,32 @@
 
             @pl.when(peer != s)
             def _():
-                giving_back(peer, s).start()
-
-    @pl.loop(1, 16)
-    def _(i):
-        giving_back((s + i) % 16, (s + i) % 16).wait_recv()
-
-    mine.wait()
-
+                giving_back(peer).start()
+
+    arrived(ret_ref, ret_recv.at[0])
     moe_grad = dot(pick_ref[...].reshape(768, 256), ret_ref[...].reshape(768, 256), TN)
     mixer = (cot_ref[...].astype(F32) + moe_grad).astype(BF16)
-    mcf[t] = mixer.reshape(2, 128, 256)
+    mcf[t] = mixer.reshape(4, 64, 256)
     acc2[...] = jnp.zeros_like(acc2)
 
     def mc_f(d, k):
         at = mcf.at[((z + 8 - d) % 8) * 2 + c, k]
-        return remote(at, at, mf_send.at[d, k], mf_recv.at[d, k], tp=up)
+        return remote(at, at, sent.at[MIXER], mf_recv.at[d, k], tp=up)
 
     def mc_b(d, k):
         at = mcf.at[((z + d) % 8) * 2 + c, k]
-        return remote(at, at, mb_send.at[d, k], mb_recv.at[d, k], tp=down)
-
-    def mc_mate(zz, core, k):
-        at = mcf.at[zz * 2 + core, k]
-        return remote(at, at, mp_send.at[zz, k], mp_recv.at[zz, k], tp=mate)
-
-    def column(peer, source):
-        return remote(mcf.at[peer, c], col.at[source, c], col_send.at[peer], col_recv.at[source], sp=peer)
-
-    def column_mate(source, core):
-        at = col.at[source, core]
-        return remote(at, at, colp_send.at[source], colp_recv.at[source], tp=mate)
-
-    kept = pltpu.make_async_copy(mcf.at[s, c], col.at[s, c], col_recv.at[s])
+        return remote(at, at, sent.at[MIXER], mb_recv.at[d, k], tp=down)
+
+    def mc_mate(zz, core):
+        at = mcf.at[zz * 2 + core]
+        return remote(at, at, sent.at[MIXER], mp_recv.at[zz], tp=mate)
+
+    half = pl.ds(2 * c, 2)
+
+    def column(peer):
+        return remote(mcf.at[peer, half], col.at[s, half], sent.at[COLUMN], col_recv.at[y], sp=peer)
+
+    kept = pltpu.make_async_copy(mcf.at[s, half], col.at[s, half], col_recv.at[y])
 
     def use(tt):
         @pl.when(tt == s)
@@ -504,48 +480,45 @@
 
         @pl.when(tt != s)
         def _():
-            column(tt, s).start()
+            column(tt).start()
 
         acc2[...] += dot(mcf[tt].reshape(256, 256), op[tt], NN)
 
-    for k in range(2):
+    for k in range(4):
         mc_f(0, k).start()
         mc_b(0, k).start()
-        mc_mate(z, c, k).start()
+    mc_mate(z, c).start()
     use(t)
 
     def mc_mate_part(zz):
-        for k in range(2):
-            mc_mate(zz, 1 - c, k).wait_recv()
+        mc_mate(zz, 1 - c).wait_recv()
         use(zz * 2 + 1 - c)
 
     @pl.loop(1, 5)
     def _(d):
         zf, zb = (z + 8 - d) % 8, (z + d) % 8
-        for k in range(2):
-            @pl.when((d < 4) | (k == 0))
-            def _():
-                at = mcf.at[zf * 2 + c, k]
-                remote(at, at, mf_send.at[d - 1, k], mf_recv.at[d - 1, k], tp=up).wait_recv()
-
-                @pl.when((d < 3) | ((d == 3) & (k == 0)))
+        for k in range(4):
+            @pl.when((d < 4) | (k < 2))
+            def _():
+                arrived(mcf.at[zf * 2 + c, k], mf_recv.at[d - 1, k])
+
+                @pl.when((d < 3) | ((d == 3) & (k < 2)))
                 def _():
                     mc_f(d, k).start()
 
-                mc_mate(zf, c, k).start()
-
-            @pl.when((d < 4) | (k == 1))
-            def _():
-                at = mcf.at[zb * 2 + c, k]
-                remote(at, at, mb_send.at[d - 1, k], mb_recv.at[d - 1, k], tp=down).wait_recv()
-
-                @pl.when((d < 3) | ((d == 3) & (k == 1)))
+            @pl.when((d < 4) | (k >= 2))
+            def _():
+                arrived(mcf.at[zb * 2 + c, k], mb_recv.at[d - 1, k])
+
+                @pl.when((d < 3) | ((d == 3) & (k >= 2)))
                 def _():
                     mc_b(d, k).start()
 
-            @pl.when((d < 4) | (k == 1))
-            def _():
-                mc_mate(zb, c, k).start()
+        mc_mate(zf, c).start()
+
+        @pl.when(d < 4)
+        def _():
+            mc_mate(zb, c).start()
 
         use(zf * 2 + c)
         mc_mate_part((z + 9 - d) % 8)
@@ -566,92 +539,38 @@
     for copy in halo_copies(1):
         copy.start()
 
-    kept.wait()
-    column_mate(s, c).start()
-
-    @pl.loop(1, 16)
-    def _(i):
-        source = (s + i) % 16
-        column(source, source).wait_recv()
-        column_mate(source, c).start()
-
-    gop_ref[...] = jnp.zeros_like(gop_ref)
-
-    @pl.loop(0, 16)
-    def _(i):
-        source = (s + i) % 16
-
-        @pl.when(i > 0)
-        def _():
-            mix_copy(source, source).wait_recv()
-
-        column_mate(source, 1 - c).wait_recv()
-        gop_ref[...] += dot(col[source].reshape(256, 256), mix[source], TN)
+    def column_mate(k, core):
+        at = col.at[part(k), pl.ds(2 * core, 2)]
+        return remote(at, at, sent.at[COLUMN_MATE], colp_recv.at[(y + 4 - k) % 4], tp=mate)
+
+    for k in range(4):
+        arrived(col.at[part(k), half], col_recv.at[(y + 4 - k) % 4])
+        column_mate(k, c).start()
+    arrived(mix_t.at[:, pl.ds(0, 15 * 256)], mix_recv.at[0])
+    for k in range(4):
+        column_mate(k, 1 - c).wait_recv()
+    gop_ref[...] = dot(mix_t[...], col[...].reshape(4096, 256), NN).T
 
     before, here, after = neighbours(1)
     grad_in = after * taps_ref[0:1, :] + here * taps_ref[1:2, :] + before * taps_ref[2:3, :]
     gig_ref[...] = (grad_in * val_ref[...].astype(F32)).astype(BF16)
     gval_ref[...] = (grad_in * ig_ref[...].astype(F32)).astype(BF16)
 
-    @pl.loop(1, 16)
-    def _(i):
-        dispatch((s + i) % 16, s).wait_send()
-        giving_back((s + i) % 16, s).wait_send()
-        mix_copy((s + i) % 16, s).wait_send()
-        column((s + i) % 16, s).wait_send()
-
-        @pl.loop(0, 8)
-        def _(zz):
-            dispatch_cot(zz, (s + i) % 16, s).wait_send()
-
-    @pl.loop(0, 16)
-    def _(i):
-        column_mate(i, c).wait_send()
-
-        @pl.when(i < 8)
-        def _():
-            cot_mate(i, c).wait_send()
-
-        mc_mate(i // 2, c, i % 2).wait_send()
-
-    @pl.loop(0, 8)
-    def _(i):
-        d, k = i // 2, i % 2
-
-        @pl.when((d < 3) | (k == 0))
-        def _():
-            token_f(d, k).wait_send()
-            mc_f(d, k).wait_send()
-
-        @pl.when((d < 3) | (k == 1))
-        def _():
-            token_b(d, k).wait_send()
-            mc_b(d, k).wait_send()
-
-    @pl.loop(0, 16)
-    def _(i):
-        d, k = i // 4, i % 4
-        even = (k % 2) == 0
-
-        @pl.when((d < 3) | even)
-        def _():
-            along_f(d, k).wait_send()
-            at = out_f.at[d, part(k)]
-            remote(at, at, rf_send.at[d, k], rf_recv.at[d, k], tp=up).wait_send()
-
-        @pl.when((d < 3) | (~even))
-        def _():
-            along_b(d, k).wait_send()
-            at = out_b.at[d, part(k)]
-            remote(at, at, rb_send.at[d, k], rb_recv.at[d, k], tp=down).wait_send()
-
-        for half in range(2):
-            zz = d * 2 + half
-            to_mate(zz, c, k).wait_send()
-            at = q.at[zz, part(k)]
-            remote(at, at, rp_send.at[zz, k], rp_recv.at[zz, k], tp=mate).wait_send()
-        for copy in outputs(i):
-            copy.wait()
+    sent_all(rows.at[0, pl.ds(0, 15)], DISPATCH)
+    sent_all(rows.at[pl.ds(0, 15)], ROWS)
+    sent_all(cots.at[pl.ds(0, 8), pl.ds(0, 15)], COT)
+    sent_all(cots.at[pl.ds(0, 8)], COT_MATE)
+    sent_all(tokens.at[pl.ds(0, 7)], TOKEN_RING)
+    sent_all(mix_t.at[:, pl.ds(0, 15 * 256)], MIXED)
+    sent_all(q, MATE_SUMS)
+    sent_all(q.at[pl.ds(0, 7)], SUMS)
+    sent_all(fin.at[pl.ds(0, 15)], RETURNED)
+    sent_all(mcf.at[pl.ds(0, 15)], MIXER)
+    sent_all(mcf.at[pl.ds(0, 15), pl.ds(0, 2)], COLUMN)
+    sent_all(col.at[:, pl.ds(0, 2)], COLUMN_MATE)
+    pltpu.make_async_copy(grad_gu.at[:, :, pl.ds(0, 128)], gg_ref, out_sem.at[0]).wait()
+    pltpu.make_async_copy(grad_gu.at[:, :, pl.ds(128, 128)], gu_ref, out_sem.at[1]).wait()
+    pltpu.make_async_copy(grad_d, gd_ref, out_sem.at[2]).wait()
 
 
 def mixer_and_experts(*operands):
@@ -699,18 +618,14 @@
             vm((256, 256), F32),
             vm((256, 256), F32),
             vm((2, 2, 8, 256), F32),
-            vm((16, 256, 256), BF16),
-            vm((16, 2, 128, 256), BF16),
-            vm((16, 2, 128, 256), BF16),
+            vm((256, 4096), BF16),
+            vm((16, 4, 64, 256), BF16),
+            vm((16, 4, 64, 256), BF16),
             vm((256, 256), F32),
-            dma(4), dma(16), dma(16),
-            dma(4, 4), dma(4, 4), dma(4, 4), dma(4, 4), dma(8, 4), dma(8, 4),
-            dma(8, 4), dma(8, 4), dma(4, 4), dma(4, 4), dma(4, 4), dma(4, 4),
-            dma(16), dma(16), dma(3, 16),
-            dma(2, 2), dma(2, 2), dma(16), dma(16),
-            dma(4, 2), dma(4, 2), dma(4, 2), dma(4, 2), dma(8, 2), dma(8, 2),
-            dma(16), dma(16), dma(16), dma(16),
-            dma(4, 2), dma(4, 2), dma(4, 2), dma(4, 2), dma(8, 16), dma(8, 16), dma(8), dma(8),
+            dma(4), dma(3), dma(14),
+            dma(4), dma(4, 4), dma(4, 4), dma(8, 4), dma(8, 4), dma(4, 4), dma(4, 4), dma(1),
+            dma(2, 2), dma(1), dma(4, 4), dma(4, 4), dma(8), dma(4), dma(4),
+            dma(4, 2), dma(4, 2), dma(8), dma(8),
         ],
         compiler_params=pltpu.CompilerParams(
             collective_id=1, has_side_effects=True, vmem_limit_bytes=67043328
@@ -754,7 +669,7 @@
         out_specs=(any_,) * len(shapes),
         scratch_shapes=[pltpu.VMEM(a.shape, a.dtype) for a in shapes]
         + [pltpu.SemaphoreType.DMA((16,)), pltpu.SemaphoreType.DMA((16,))],
-        compiler_params=pltpu.CompilerParams(vmem_limit_bytes=16 * 1024 * 1024),
+        compiler_params=pltpu.CompilerParams(vmem_limit_bytes=67043328),
         name="write_out",
     )(*arrays)
 

time: 157 us -> 139 us (0.89)
  Pallas kernels: 147 us -> 138 us
  local copies, waits for them, and re-layouts: 8.43 us -> 0 us
    pallas_call x1, Pallas kernels: 143 us -> 132 us  [mixer_and_experts(): pl.pallas_call(moe_kernel, out_shape=(tile, tile, tile, jax.ShapeDtypeStr...]
    unnamed x14 -> x0, local copies, waits for them, and re-layouts: 8.43 us -> none
    pallas_call x1, Pallas kernels: 4.05 us -> 5.71 us  [written(): pl.pallas_call(write_out, out_shape=tuple(shapes), in_specs=[any_] * len(...]
where the time goes in v4:
time: 139 us
  Pallas kernels  138 us (99%)
    pallas_call x1, Pallas kernels, mixer_and_experts(): pl.pallas_call(moe_kernel, out_shape=(tile, tile, tile, jax.ShapeDtypeStr...  132 us
    pallas_call x1, Pallas kernels, written(): pl.pallas_call(write_out, out_shape=tuple(shapes), in_specs=[any_] * len(...  5.71 us

profile of v4, /device:TPU:17, one launch (start us, length us, event | category | flops | bytes accessed | tf_op | source)
XLA Modules:
  0.0 138.6 jit_solution(15860124850853031068)
XLA Ops:
  0.6 132.3 %mixer_and_experts.1 = (bf16[256,256]{1,0:T(8,128)(2,1)}, bf16[256,256]{1,0:T(8,128)(2,1)}, bf16[256,256]{1,0:T(8,128)(2,1)}, f32[256,256]{1,0:T(8,128)}, f32[16...) custom-call(s32[2,256]{1,0:T(2,128)} %bitcast.20, f32[2,256]{1,0:T(2,128)} %bitcast.21, ...), custom_call_target="tpu_custom_call" | custom-call | flops 8000000000 | bytes 20000000 | tf_op jit(solution)/shard_map/mixer_and_experts/pallas_call | solution.py:582
  132.9 5.7 %write_out.1 = (f32[4096,128]{1,0:T(8,128)}, f32[4096,128]{1,0:T(8,128)}, f32[128,4096]{1,0:T(8,128)}, f32[256,256]{1,0:T(8,128)}, bf16[256,256]{1,0:T(8,128)(2,...) custom-call(f32[4096,128]{1,0:T(8,128)} %bitcast.11, f32[4096,128]{1,0:T(8,128)} %bitcast.12, ...), custom_call_target="tpu_custom_call" | custom-call | tf_op jit(solution)/shard_map/write_out/pallas_call | solution.py:665

commit v5 on v4

--- a/solution.py
+++ b/solution.py
@@ -23,8 +23,9 @@
 
 
 def moe_kernel(
-    ids_ref, gates_ref, x_ref, cot_ref, og_ref, ig_ref, val_ref, taps_ref, wg_ref, wu_ref, wd_ref, op_ref,
+    ids_ref, gates_ref, taps_ref, x_hbm, cot_hbm, og_hbm, ig_hbm, val_hbm, wg_ref, wu_ref, wd_ref, op_ref,
     gog_ref, gig_ref, gval_ref, gop_ref, gg_ref, gu_ref, gd_ref,
+    x_ref, cot_ref, og_ref, ig_ref, val_ref,
     pick_ref, scale, tokens, x_send, cot_send, rows, cots, wgu, wd, acc, acc_h, g2, hid, q, r, in_f, in_b, out_f, out_b, fin, grad_gu, grad_d,
     ret_ref, op, cin, cout, halo, mix_t, mcf, col, acc2,
     w_sem, out_sem, sent,
@@ -47,6 +48,15 @@
     for other in (up, down, mate):
         pl.semaphore_signal(barrier, inc=1, device_id={"tp": other}, device_id_type=MESH)
 
+    tiles = [
+        pltpu.make_async_copy(source, held, w_sem.at[4 + i])
+        for i, (source, held) in enumerate((
+            (ig_hbm, ig_ref), (val_hbm, val_ref), (cot_hbm, cot_ref), (x_hbm, x_ref), (og_hbm, og_ref)
+        ))
+    ]
+    for tile in tiles:
+        tile.start()
+
     weights = [
         pltpu.make_async_copy(wg_ref, wgu.at[:, :, pl.ds(0, 128)], w_sem.at[0]),
         pltpu.make_async_copy(wu_ref, wgu.at[:, :, pl.ds(128, 128)], w_sem.at[1]),
@@ -55,8 +65,6 @@
     ]
     for w in weights:
         w.start()
-
-    cin[...] = ig_ref[...].astype(F32) * val_ref[...].astype(F32)
 
     expert = lax.broadcasted_iota(jnp.int32, (16, 256), 0)
     named = [ids_ref[i : i + 1, :] == expert for i in range(2)]
@@ -71,6 +79,9 @@
         pick_ref[e] = jnp.where(hit, 1.0, 0.0).astype(BF16)
         slot_weight = jnp.sum(jnp.where(hit, weight[e : e + 1, :], 0.0), axis=1, keepdims=True)
         scale[e] = jnp.broadcast_to(slot_weight, (48, 128))
+    for tile in tiles:
+        tile.wait()
+    cin[...] = ig_ref[...].astype(F32) * val_ref[...].astype(F32)
     tokens[z] = cot_ref[...].reshape(2, 128, 256)
     acc[...] = jnp.zeros_like(acc)
     acc_h[...] = jnp.zeros_like(acc_h)
@@ -338,60 +349,81 @@
             mix_t.at[:, mine_t], mix_t.at[:, mine_t], sent.at[MIXED], mix_recv.at[0], sp=(s + i) % 16
         ).start()
 
+    def eight(k):
+        return pl.ds(8 * k, 8)
+
     def dots_of(tt, k):
-        return dot(g2[part(k)].reshape(192, 256), wgu[tt], NT)
+        return dot(g2[eight(k)].reshape(384, 256), wgu[tt], NT)
 
     def prepare(zz, k):
         value = dots_of(zz * 2 + 1 - c, k)
-        q[zz, part(k)] = value.astype(BF16).reshape(4, 48, 256)
+        q[zz, eight(k)] = value.astype(BF16).reshape(8, 48, 256)
         remote(
-            q.at[zz, part(k)], r.at[zz, part(k)], sent.at[MATE_SUMS], rp_recv.at[zz, k], tp=mate
+            q.at[zz, eight(k)], r.at[zz, eight(k)], sent.at[MATE_SUMS], rp_recv.at[zz, k], tp=mate
         ).start()
 
     @pl.loop(0, 4)
     def _(k):
-        block = acc[part(k)].reshape(192, 256)
+        block = acc[pl.ds(4 * k, 4)].reshape(192, 256)
         pre_gate, pre_up = block[:, :128], block[:, 128:]
-        grad_hidden = acc_h[part(k)].reshape(192, 128)
+        grad_hidden = acc_h[pl.ds(4 * k, 4)].reshape(192, 128)
         sig = jax.nn.sigmoid(pre_gate)
         activated = pre_gate * sig
-        hid[part(k)] = (activated * pre_up).astype(BF16).reshape(4, 48, 128)
+        hid[pl.ds(4 * k, 4)] = (activated * pre_up).astype(BF16).reshape(4, 48, 128)
         grad_gate = (grad_hidden * pre_up * sig * (1.0 + pre_gate * (1.0 - sig))).astype(BF16)
         grad_up = (grad_hidden * activated).astype(BF16)
-        g2[part(k), :, pl.ds(0, 128)] = grad_gate.reshape(4, 48, 128)
-        g2[part(k), :, pl.ds(128, 128)] = grad_up.reshape(4, 48, 128)
-        prepare((z + 4) % 8, k)
+        g2[pl.ds(4 * k, 4), :, pl.ds(0, 128)] = grad_gate.reshape(4, 48, 128)
+        g2[pl.ds(4 * k, 4), :, pl.ds(128, 128)] = grad_up.reshape(4, 48, 128)
+
+        @pl.when(k % 2 == 1)
+        def _():
+            prepare((z + 4) % 8, k // 2)
 
     def summed(zz, k):
-        at = r.at[zz, part(k)]
+        at = r.at[zz, eight(k)]
         remote(at, at, sent.at[MATE_SUMS], rp_recv.at[zz, k], tp=mate).wait_recv()
-        return dots_of(zz * 2 + c, k) + r[zz, part(k)].reshape(192, 256).astype(F32)
+        return dots_of(zz * 2 + c, k) + r[zz, eight(k)].reshape(384, 256).astype(F32)
+
+    def ring_send(h, d, k, incoming, outgoing, recv_sem, to):
+        remote(
+            outgoing.at[h, d - 1, eight(k)], incoming.at[h, d - 1, eight(k)],
+            sent.at[SUMS], recv_sem.at[h, d - 1, k], tp=to,
+        ).start()
+
+    def half_of(ref, *index):
+        return ref[index].reshape(384, 128).astype(F32)
 
     def ring_step(d, k, zz, incoming, outgoing, recv_sem, to, starts):
         value = summed(zz, k)
+        outgoing[1, d - 1, eight(k)] = value[:, 128:].astype(BF16).reshape(8, 48, 128)
 
         @pl.when(starts)
         def _():
-            outgoing[d - 1, part(k)] = value.astype(BF16).reshape(4, 48, 256)
+            outgoing[0, d - 1, eight(k)] = value[:, :128].astype(BF16).reshape(8, 48, 128)
 
         @pl.when(jnp.logical_not(starts))
         def _():
-            at = incoming.at[d, part(k)]
-            arrived(at, recv_sem.at[d, k])
-            both = value + incoming[d, part(k)].reshape(192, 256).astype(F32)
-            outgoing[d - 1, part(k)] = both.astype(BF16).reshape(4, 48, 256)
-
-        remote(
-            outgoing.at[d - 1, part(k)], incoming.at[d - 1, part(k)],
-            sent.at[SUMS], recv_sem.at[d - 1, k], tp=to,
-        ).start()
+            arrived(incoming.at[0, d, eight(k)], recv_sem.at[0, d, k])
+            both = value[:, :128] + half_of(incoming, 0, d, eight(k))
+            outgoing[0, d - 1, eight(k)] = both.astype(BF16).reshape(8, 48, 128)
+
+        ring_send(0, d, k, incoming, outgoing, recv_sem, to)
+
+    def ring_step_2(d, k, incoming, outgoing, recv_sem, to, starts):
+        @pl.when(jnp.logical_not(starts))
+        def _():
+            arrived(incoming.at[1, d, eight(k)], recv_sem.at[1, d, k])
+            both = half_of(outgoing, 1, d - 1, eight(k)) + half_of(incoming, 1, d, eight(k))
+            outgoing[1, d - 1, eight(k)] = both.astype(BF16).reshape(8, 48, 128)
+
+        ring_send(1, d, k, incoming, outgoing, recv_sem, to)
 
     def grads(tt):
         x = rows[tt].reshape(768, 256)
         cot = cots[tt].reshape(768, 256)
-        grad_gu[tt] = dot(x, g2[...].reshape(768, 256), TN)
+        grad_gu[tt] = dot(x, g2[...].reshape(768, 256), TN).astype(BF16)
         columns = pl.ds(pl.multiple_of(tt * 256, 256), 256)
-        grad_d[:, columns] = dot(hid[...].reshape(768, 128), cot, TN)
+        grad_d[:, columns] = dot(hid[...].reshape(768, 128), cot, TN).astype(BF16)
         for copy in outputs(tt):
             copy.start()
 
@@ -403,9 +435,9 @@
             pltpu.make_async_copy(grad_d.at[:, columns], gd_ref.at[:, columns], out_sem.at[2]),
         ]
 
-    @pl.loop(0, 16)
+    @pl.loop(0, 8)
     def _(i):
-        d, k = 4 - i // 4, i % 4
+        d, k = 4 - i // 2, i % 2
         even = (k % 2) == 0
         zf, zb = (z + d) % 8, (z + 8 - d) % 8
 
@@ -423,115 +455,166 @@
         def _():
             prepare((z + 9 - d) % 8, k)
 
-        grads(i)
-
-    def giving_back(peer):
-        return remote(fin.at[peer], ret_ref.at[s], sent.at[RETURNED], ret_recv.at[0], sp=peer)
-
-    mine = pltpu.make_async_copy(fin.at[s], ret_ref.at[s], ret_recv.at[0])
-
-    @pl.loop(0, 4)
-    def _(k):
-        value = summed(z, k)
+    def giving_back(h, peer):
+        return remote(fin.at[h, peer], ret_ref.at[h, s], sent.at[RETURNED], ret_recv.at[h], sp=peer)
+
+    def mine(h):
+        return pltpu.make_async_copy(fin.at[h, s], ret_ref.at[h, s], ret_recv.at[h])
+
+    def finish(h, k, value):
         for incoming, recv_sem in ((in_f, rf_recv), (in_b, rb_recv)):
-            arrived(incoming.at[0, part(k)], recv_sem.at[0, k])
-            value = value + incoming[0, part(k)].reshape(192, 256).astype(F32)
-        fin[part(k)] = value.astype(BF16).reshape(4, 48, 256)
-        for x in range(4):
-            peer = 4 * ((y + 4 - k) % 4) + x
+            arrived(incoming.at[h, 0, eight(k)], recv_sem.at[h, 0, k])
+            value = value + half_of(incoming, h, 0, eight(k))
+        fin[h, eight(k)] = value.astype(BF16).reshape(8, 48, 128)
+        for x in range(8):
+            peer = 8 * k + x
 
             @pl.when(peer == s)
             def _():
-                mine.start()
+                mine(h).start()
 
             @pl.when(peer != s)
             def _():
-                giving_back(peer).start()
-
-    arrived(ret_ref, ret_recv.at[0])
-    moe_grad = dot(pick_ref[...].reshape(768, 256), ret_ref[...].reshape(768, 256), TN)
-    mixer = (cot_ref[...].astype(F32) + moe_grad).astype(BF16)
-    mcf[t] = mixer.reshape(4, 64, 256)
+                giving_back(h, peer).start()
+
+    def mc_f(h, d, k):
+        at = mcf.at[h, ((z + 8 - d) % 8) * 2 + c, pl.ds(2 * k, 2)]
+        return remote(at, at, sent.at[MIXER], mf_recv.at[h, d, k], tp=up)
+
+    def mc_b(h, d, k):
+        at = mcf.at[h, ((z + d) % 8) * 2 + c, pl.ds(2 * k, 2)]
+        return remote(at, at, sent.at[MIXER], mb_recv.at[h, d, k], tp=down)
+
+    def mc_mate(h, zz, core):
+        at = mcf.at[h, zz * 2 + core]
+        return remote(at, at, sent.at[MIXER], mp_recv.at[h, zz], tp=mate)
+
+    tokens_half = pl.ds(2 * c, 2)
+
+    def send_column(h, tt):
+        @pl.when(tt == s)
+        def _():
+            pltpu.make_async_copy(
+                mcf.at[h, s, tokens_half], col.at[h, s, tokens_half], col_recv.at[h, y]
+            ).start()
+
+        @pl.when(tt != s)
+        def _():
+            remote(
+                mcf.at[h, tt, tokens_half], col.at[h, s, tokens_half],
+                sent.at[COLUMN], col_recv.at[h, y], sp=tt,
+            ).start()
+
+    def use(tt):
+        tile = jnp.concatenate([mcf[h, tt].reshape(256, 128) for h in range(2)], axis=1)
+        acc2[...] += dot(tile, op[tt], NN)
+
+    def from_mate(h, zz):
+        mc_mate(h, zz, 1 - c).wait_recv()
+        send_column(h, zz * 2 + 1 - c)
+
+    def mixer_start(h):
+        arrived(ret_ref.at[h], ret_recv.at[h])
+        moe_grad = dot(pick_ref[...].reshape(768, 256), ret_ref[h].reshape(768, 128), TN)
+        mixer = cot_ref[:, pl.ds(128 * h, 128)].astype(F32) + moe_grad
+        mcf[h, t] = mixer.astype(BF16).reshape(4, 64, 128)
+        for k in range(2):
+            mc_f(h, 0, k).start()
+            mc_b(h, 0, k).start()
+        mc_mate(h, z, c).start()
+        send_column(h, t)
+
+    def mixer_step(h, d, compute):
+        zf, zb = (z + 8 - d) % 8, (z + d) % 8
+        for k in range(2):
+            @pl.when((d < 4) | (k == 0))
+            def _():
+                arrived(mcf.at[h, zf * 2 + c, pl.ds(2 * k, 2)], mf_recv.at[h, d - 1, k])
+
+                @pl.when((d < 3) | ((d == 3) & (k == 0)))
+                def _():
+                    mc_f(h, d, k).start()
+
+            @pl.when((d < 4) | (k == 1))
+            def _():
+                arrived(mcf.at[h, zb * 2 + c, pl.ds(2 * k, 2)], mb_recv.at[h, d - 1, k])
+
+                @pl.when((d < 3) | ((d == 3) & (k == 1)))
+                def _():
+                    mc_b(h, d, k).start()
+
+        mc_mate(h, zf, c).start()
+        send_column(h, zf * 2 + c)
+
+        @pl.when(d < 4)
+        def _():
+            mc_mate(h, zb, c).start()
+            send_column(h, zb * 2 + c)
+
+        lf, lb = (zf + 1) % 8, (zb + 7) % 8
+        from_mate(h, lf)
+        if compute:
+            for core in range(2):
+                use(lf * 2 + core)
+
+        @pl.when(d > 1)
+        def _():
+            from_mate(h, lb)
+            if compute:
+                for core in range(2):
+                    use(lb * 2 + core)
+
+    @pl.loop(0, 8)
+    def _(i):
+        d, k = 4 - i // 2, i % 2
+        even = k == 0
+
+        @pl.when((d < 4) | even)
+        def _():
+            ring_step_2(d, k, in_f, out_f, rf_recv, up, (d == 4) | ((d == 3) & (~even)))
+
+        @pl.when((d < 4) | (~even))
+        def _():
+            ring_step_2(d, k, in_b, out_b, rb_recv, down, (d == 4) | ((d == 3) & even))
+
+        @pl.when((i >= 1) & (i < 3))
+        def _():
+            value = summed(z, i - 1)
+            fin[1, eight(i - 1)] = value[:, 128:].astype(BF16).reshape(8, 48, 128)
+            finish(0, i - 1, value[:, :128])
+
+        @pl.when(i != 1)
+        def _():
+            grads(i)
+
     acc2[...] = jnp.zeros_like(acc2)
-
-    def mc_f(d, k):
-        at = mcf.at[((z + 8 - d) % 8) * 2 + c, k]
-        return remote(at, at, sent.at[MIXER], mf_recv.at[d, k], tp=up)
-
-    def mc_b(d, k):
-        at = mcf.at[((z + d) % 8) * 2 + c, k]
-        return remote(at, at, sent.at[MIXER], mb_recv.at[d, k], tp=down)
-
-    def mc_mate(zz, core):
-        at = mcf.at[zz * 2 + core]
-        return remote(at, at, sent.at[MIXER], mp_recv.at[zz], tp=mate)
-
-    half = pl.ds(2 * c, 2)
-
-    def column(peer):
-        return remote(mcf.at[peer, half], col.at[s, half], sent.at[COLUMN], col_recv.at[y], sp=peer)
-
-    kept = pltpu.make_async_copy(mcf.at[s, half], col.at[s, half], col_recv.at[y])
-
-    def use(tt):
-        @pl.when(tt == s)
-        def _():
-            kept.start()
-
-        @pl.when(tt != s)
-        def _():
-            column(tt).start()
-
-        acc2[...] += dot(mcf[tt].reshape(256, 256), op[tt], NN)
-
-    for k in range(4):
-        mc_f(0, k).start()
-        mc_b(0, k).start()
-    mc_mate(z, c).start()
-    use(t)
-
-    def mc_mate_part(zz):
-        mc_mate(zz, 1 - c).wait_recv()
-        use(zz * 2 + 1 - c)
-
-    @pl.loop(1, 5)
+    finish(1, 0, half_of(fin, 1, eight(0)))
+    mixer_start(0)
+    finish(1, 1, half_of(fin, 1, eight(1)))
+    grads(1)
+
+    @pl.loop(1, 3)
     def _(d):
-        zf, zb = (z + 8 - d) % 8, (z + d) % 8
-        for k in range(4):
-            @pl.when((d < 4) | (k < 2))
-            def _():
-                arrived(mcf.at[zf * 2 + c, k], mf_recv.at[d - 1, k])
-
-                @pl.when((d < 3) | ((d == 3) & (k < 2)))
-                def _():
-                    mc_f(d, k).start()
-
-            @pl.when((d < 4) | (k >= 2))
-            def _():
-                arrived(mcf.at[zb * 2 + c, k], mb_recv.at[d - 1, k])
-
-                @pl.when((d < 3) | ((d == 3) & (k >= 2)))
-                def _():
-                    mc_b(d, k).start()
-
-        mc_mate(zf, c).start()
-
-        @pl.when(d < 4)
-        def _():
-            mc_mate(zb, c).start()
-
-        use(zf * 2 + c)
-        mc_mate_part((z + 9 - d) % 8)
-
-        @pl.when(d < 4)
-        def _():
-            use(zb * 2 + c)
-
-        @pl.when(d > 1)
-        def _():
-            mc_mate_part((z + d - 1) % 8)
-
-    mc_mate_part((z + 4) % 8)
+        mixer_step(0, d, False)
+        grads(7 + d)
+
+    mixer_start(1)
+
+    @pl.loop(3, 5)
+    def _(d):
+        mixer_step(0, d, False)
+        mixer_step(1, d - 2, True)
+
+    from_mate(0, (z + 4) % 8)
+
+    @pl.loop(3, 5)
+    def _(d):
+        mixer_step(1, d, True)
+        grads(7 + d)
+
+    from_mate(1, (z + 4) % 8)
+    for core in range(2):
+        use(((z + 4) % 8) * 2 + core)
 
     grad_mixed = acc2[...]
     gog_ref[...] = (grad_mixed * cout[...]).astype(BF16)
@@ -539,17 +622,24 @@
     for copy in halo_copies(1):
         copy.start()
 
-    def column_mate(k, core):
-        at = col.at[part(k), pl.ds(2 * core, 2)]
-        return remote(at, at, sent.at[COLUMN_MATE], colp_recv.at[(y + 4 - k) % 4], tp=mate)
-
-    for k in range(4):
-        arrived(col.at[part(k), half], col_recv.at[(y + 4 - k) % 4])
-        column_mate(k, c).start()
+    @pl.loop(12, 16)
+    def _(i):
+        grads(i)
+
+    def column_mate(h, k, core):
+        at = col.at[h, part(k), pl.ds(2 * core, 2)]
+        return remote(at, at, sent.at[COLUMN_MATE], colp_recv.at[h, (y + 4 - k) % 4], tp=mate)
+
+    for h in range(2):
+        for k in range(4):
+            arrived(col.at[h, part(k), tokens_half], col_recv.at[h, (y + 4 - k) % 4])
+            column_mate(h, k, c).start()
     arrived(mix_t.at[:, pl.ds(0, 15 * 256)], mix_recv.at[0])
-    for k in range(4):
-        column_mate(k, 1 - c).wait_recv()
-    gop_ref[...] = dot(mix_t[...], col[...].reshape(4096, 256), NN).T
+    for h in range(2):
+        for k in range(4):
+            column_mate(h, k, 1 - c).wait_recv()
+    columns = jnp.concatenate([col[h].reshape(4096, 128) for h in range(2)], axis=1)
+    gop_ref[...] = dot(mix_t[...], columns, NN).T
 
     before, here, after = neighbours(1)
     grad_in = after * taps_ref[0:1, :] + here * taps_ref[1:2, :] + before * taps_ref[2:3, :]
@@ -564,10 +654,10 @@
     sent_all(mix_t.at[:, pl.ds(0, 15 * 256)], MIXED)
     sent_all(q, MATE_SUMS)
     sent_all(q.at[pl.ds(0, 7)], SUMS)
-    sent_all(fin.at[pl.ds(0, 15)], RETURNED)
-    sent_all(mcf.at[pl.ds(0, 15)], MIXER)
-    sent_all(mcf.at[pl.ds(0, 15), pl.ds(0, 2)], COLUMN)
-    sent_all(col.at[:, pl.ds(0, 2)], COLUMN_MATE)
+    sent_all(fin.at[:, pl.ds(0, 15)], RETURNED)
+    sent_all(mcf.at[:, pl.ds(0, 15)], MIXER)
+    sent_all(mcf.at[:, pl.ds(0, 15), pl.ds(0, 2)], COLUMN)
+    sent_all(col.at[:, :, pl.ds(0, 2)], COLUMN_MATE)
     pltpu.make_async_copy(grad_gu.at[:, :, pl.ds(0, 128)], gg_ref, out_sem.at[0]).wait()
     pltpu.make_async_copy(grad_gu.at[:, :, pl.ds(128, 128)], gu_ref, out_sem.at[1]).wait()
     pltpu.make_async_copy(grad_d, gd_ref, out_sem.at[2]).wait()
@@ -584,13 +674,18 @@
         out_shape=(
             tile, tile, tile,
             jax.ShapeDtypeStruct((256, 256), F32),
-            jax.ShapeDtypeStruct((16, 256, 128), F32),
-            jax.ShapeDtypeStruct((16, 256, 128), F32),
-            jax.ShapeDtypeStruct((128, 4096), F32),
+            jax.ShapeDtypeStruct((16, 256, 128), BF16),
+            jax.ShapeDtypeStruct((16, 256, 128), BF16),
+            jax.ShapeDtypeStruct((128, 4096), BF16),
         ),
-        in_specs=[vmem] * 8 + [any_] * 4,
+        in_specs=[vmem] * 3 + [any_] * 9,
         out_specs=(vmem,) * 4 + (any_,) * 3,
         scratch_shapes=[
+            vm((256, 256), BF16),
+            vm((256, 256), BF16),
+            vm((256, 256), BF16),
+            vm((256, 256), BF16),
+            vm((256, 256), BF16),
             vm((16, 48, 256), BF16),
             vm((16, 48, 128), F32),
             vm((8, 2, 128, 256), BF16),
@@ -606,25 +701,25 @@
             vm((16, 48, 128), BF16),
             vm((8, 16, 48, 256), BF16),
             vm((8, 16, 48, 256), BF16),
-            vm((4, 16, 48, 256), BF16),
-            vm((4, 16, 48, 256), BF16),
-            vm((4, 16, 48, 256), BF16),
-            vm((4, 16, 48, 256), BF16),
-            vm((16, 48, 256), BF16),
-            vm((16, 256, 256), F32),
-            vm((128, 4096), F32),
-            vm((16, 48, 256), BF16),
+            vm((2, 4, 16, 48, 128), BF16),
+            vm((2, 4, 16, 48, 128), BF16),
+            vm((2, 4, 16, 48, 128), BF16),
+            vm((2, 4, 16, 48, 128), BF16),
+            vm((2, 16, 48, 128), BF16),
+            vm((16, 256, 256), BF16),
+            vm((128, 4096), BF16),
+            vm((2, 16, 48, 128), BF16),
             vm((16, 256, 256), BF16),
             vm((256, 256), F32),
             vm((256, 256), F32),
             vm((2, 2, 8, 256), F32),
             vm((256, 4096), BF16),
-            vm((16, 4, 64, 256), BF16),
-            vm((16, 4, 64, 256), BF16),
+            vm((2, 16, 4, 64, 128), BF16),
+            vm((2, 16, 4, 64, 128), BF16),
             vm((256, 256), F32),
-            dma(4), dma(3), dma(14),
-            dma(4), dma(4, 4), dma(4, 4), dma(8, 4), dma(8, 4), dma(4, 4), dma(4, 4), dma(1),
-            dma(2, 2), dma(1), dma(4, 4), dma(4, 4), dma(8), dma(4), dma(4),
+            dma(9), dma(3), dma(14),
+            dma(4), dma(4, 4), dma(4, 4), dma(8, 4), dma(8, 2), dma(2, 4, 2), dma(2, 4, 2), dma(2),
+            dma(2, 2), dma(1), dma(2, 4, 2), dma(2, 4, 2), dma(2, 8), dma(2, 4), dma(2, 4),
             dma(4, 2), dma(4, 2), dma(8), dma(8),
         ],
         compiler_params=pltpu.CompilerParams(
@@ -636,38 +731,42 @@
 
 
 def write_out(*refs):
-    count = len(refs) // 3
-    sources, targets, held = refs[:count], refs[count : 2 * count], refs[2 * count : 3 * count]
-    in_sem, out_sem = refs[3 * count :]
+    sources, targets, held = refs[:7], refs[7:14], refs[14:21]
+    wide, in_sem, out_sem = refs[21:24], refs[24], refs[25]
     steps = []
     for i, ref in enumerate(sources):
         pieces = 4 if i < 3 else 1
         size = ref.shape[0] // pieces
+        staged = wide[i] if i < 3 else held[i]
         for p in range(pieces):
             at = pl.ds(p * size, size)
             n = len(steps)
             steps.append((
+                i, at,
                 pltpu.make_async_copy(ref.at[at], held[i].at[at], in_sem.at[n]),
-                pltpu.make_async_copy(held[i].at[at], targets[i].at[at], out_sem.at[n]),
+                pltpu.make_async_copy(staged.at[at], targets[i].at[at], out_sem.at[n]),
             ))
-    for fetch, _ in steps:
+    for _, _, fetch, _ in steps:
         fetch.start()
-    for fetch, store in steps:
+    for i, at, fetch, store in steps:
         fetch.wait()
+        if i < 3:
+            wide[i][at, :] = held[i][at, :].astype(F32)
         store.start()
-    for _, store in steps:
+    for _, _, _, store in steps:
         store.wait()
 
 
 def written(*arrays):
     any_ = pl.BlockSpec(memory_space=pl.ANY)
-    shapes = [jax.ShapeDtypeStruct(a.shape, a.dtype) for a in arrays]
+    shapes = [jax.ShapeDtypeStruct(a.shape, F32 if i < 3 else a.dtype) for i, a in enumerate(arrays)]
     return pl.pallas_call(
         write_out,
         out_shape=tuple(shapes),
         in_specs=[any_] * len(shapes),
         out_specs=(any_,) * len(shapes),
-        scratch_shapes=[pltpu.VMEM(a.shape, a.dtype) for a in shapes]
+        scratch_shapes=[pltpu.VMEM(a.shape, a.dtype) for a in arrays]
+        + [pltpu.VMEM(a.shape, F32) for a in arrays[:3]]
         + [pltpu.SemaphoreType.DMA((16,)), pltpu.SemaphoreType.DMA((16,))],
         compiler_params=pltpu.CompilerParams(vmem_limit_bytes=67043328),
         name="write_out",
@@ -676,7 +775,7 @@
 
 def body(moe_input, out_gate, in_gate, values, conv_taps, out_proj, route_ids, route_gates, expert_gate, expert_up, expert_down, cotangent):
     gog, gig, gval, gop, gg, gu, gd = mixer_and_experts(
-        route_ids.T, route_gates.T, moe_input, cotangent, out_gate, in_gate, values, conv_taps,
+        route_ids.T, route_gates.T, conv_taps, moe_input, cotangent, out_gate, in_gate, values,
         expert_gate.reshape(16, 256, 128),
         expert_up.reshape(16, 256, 128),
         expert_down.reshape(128, 4096),

time: 139 us -> 134 us (0.964)
  Pallas kernels: 138 us -> 134 us
    pallas_call x1, Pallas kernels: 132 us -> 129 us  [mixer_and_experts(): pl.pallas_call(moe_kernel, out_shape=(tile, tile, tile, jax.ShapeDtypeStr...]
    pallas_call x1, Pallas kernels: 5.71 us -> 4.09 us  [written(): pl.pallas_call(write_out, out_shape=tuple(shapes), in_specs=[any_] * len(...]
where the time goes in v5:
time: 134 us
  Pallas kernels  134 us (100%)
    pallas_call x1, Pallas kernels, mixer_and_experts(): pl.pallas_call(moe_kernel, out_shape=(tile, tile, tile, jax.ShapeDtypeStr...  129 us
    pallas_call x1, Pallas kernels, written(): pl.pallas_call(write_out, out_shape=tuple(shapes), in_specs=[any_] * len(...  4.09 us

profile of v5, /device:TPU:17, one launch (start us, length us, event | category | flops | bytes accessed | tf_op | source)
XLA Modules:
  0.0 134.2 jit_solution(345688129490719134)
XLA Ops:
  0.6 129.5 %mixer_and_experts.1 = (bf16[256,256]{1,0:T(8,128)(2,1)}, bf16[256,256]{1,0:T(8,128)(2,1)}, bf16[256,256]{1,0:T(8,128)(2,1)}, f32[256,256]{1,0:T(8,128)}, bf16[1...) custom-call(s32[2,256]{1,0:T(2,128)} %bitcast.20, f32[2,256]{1,0:T(2,128)} %bitcast.21, ...), custom_call_target="tpu_custom_call" | custom-call | flops 8000000000 | bytes 20000000 | tf_op jit(solution)/shard_map/mixer_and_experts/pallas_call | solution.py:672
  130.1 4.1 %write_out.1 = (f32[4096,128]{1,0:T(8,128)}, f32[4096,128]{1,0:T(8,128)}, f32[128,4096]{1,0:T(8,128)}, f32[256,256]{1,0:T(8,128)}, bf16[256,256]{1,0:T(8,128)(2,...) custom-call(bf16[4096,128]{1,0:T(8,128)(2,1)} %bitcast.11, bf16[4096,128]{1,0:T(8,128)(2,1)} %bitcast.12, ...), custom_call_target="tpu_custom_call" | custom-call | tf_op jit(solution)/shard_map/write_out/pallas_call | solution.py:763

commit v6 on v5

--- a/solution.py
+++ b/solution.py
@@ -24,10 +24,11 @@
 
 def moe_kernel(
     ids_ref, gates_ref, taps_ref, x_hbm, cot_hbm, og_hbm, ig_hbm, val_hbm, wg_ref, wu_ref, wd_ref, op_ref,
-    gog_ref, gig_ref, gval_ref, gop_ref, gg_ref, gu_ref, gd_ref,
+    gog_hbm, gig_hbm, gval_hbm, gop_hbm, gg_ref, gu_ref, gd_ref,
+    gog_ref, gig_ref, gval_ref, gop_ref,
     x_ref, cot_ref, og_ref, ig_ref, val_ref,
     pick_ref, scale, tokens, x_send, cot_send, rows, cots, wgu, wd, acc, acc_h, g2, hid, q, r, in_f, in_b, out_f, out_b, fin, grad_gu, grad_d,
-    ret_ref, op, cin, cout, halo, mix_t, mcf, col, acc2,
+    ret_ref, op, cin, cout, halo, mix_t, mcf, col,
     w_sem, out_sem, sent,
     disp_recv, af_recv, ab_recv, ap_recv, rp_recv, rf_recv, rb_recv, ret_recv,
     halo_recv, mix_recv, mf_recv, mb_recv, mp_recv, col_recv, colp_recv,
@@ -202,18 +203,16 @@
 
     def to_mate(zz, core, k):
         at = slice_of(zz, core, k)
-        return remote(at, at, sent.at[ROWS], ap_recv.at[zz, k], tp=mate)
-
-    def multiply(tt, k):
-        pre = dot(rows[tt, part(k)].reshape(192, 256), wgu[tt], NN)
-        acc[part(k)] += pre.reshape(4, 48, 256)
+        return remote(at, at, sent.at[ROWS], ap_recv.at[zz], tp=mate)
+
+    def multiply(tt):
+        acc[...] += dot(rows[tt].reshape(768, 256), wgu[tt], NN).reshape(16, 48, 256)
 
     def ring_start(k):
         arrived(slice_of(z, c, k), disp_recv.at[(y + 4 - k) % 4])
         along_f(0, k).start()
         along_b(0, k).start()
         to_mate(z, c, k).start()
-        multiply(t, k)
 
     @pl.loop(1, 5)
     def _(d):
@@ -266,9 +265,9 @@
         cot_mate(zz, 1 - c).wait_recv()
         multiply_cot(zz * 2 + 1 - c)
 
-    def mate_part(zz, k):
-        to_mate(zz, 1 - c, k).wait_recv()
-        multiply(zz * 2 + 1 - c, k)
+    def mate_part(zz):
+        arrived(rows.at[zz * 2 + 1 - c], ap_recv.at[zz])
+        multiply(zz * 2 + 1 - c)
 
     @pl.loop(0, 16)
     def _(i):
@@ -300,40 +299,37 @@
         def _():
             to_mate(zb, c, k).start()
 
-        @pl.when((d < 4) | even)
-        def _():
-            multiply(zf * 2 + c, k)
-
-        @pl.when((d < 4) | (~even))
-        def _():
-            multiply(zb * 2 + c, k)
-
-        e = i // 4
-
-        @pl.when(e == 0)
-        def _():
-            mate_part(z, k)
-
-        @pl.when(e > 0)
-        def _():
-            mate_part((z + 8 - e) % 8, k)
-            mate_part((z + e) % 8, k)
+        last_f, last_b = (zf + 1) % 8, (zb + 7) % 8
+
+        @pl.when(k == 0)
+        def _():
+            multiply(last_f * 2 + c)
+
+        @pl.when((k == 1) & (d > 1))
+        def _():
+            multiply(last_b * 2 + c)
+
+        @pl.when(k == 2)
+        def _():
+            mate_part(last_f)
+
+        @pl.when((k == 3) & (d > 1))
+        def _():
+            mate_part(last_b)
 
         @pl.when((i >= 3) & (i % 2 == 1))
         def _():
             cot_own_part((i - 3) // 2)
 
-        @pl.when((i >= 4) & (i % 2 == 0))
-        def _():
-            cot_mate_part((i - 4) // 2)
-
-    @pl.loop(0, 4)
-    def _(k):
-        mate_part((z + 4) % 8, k)
+        @pl.when((i >= 6) & (i % 2 == 0))
+        def _():
+            cot_mate_part((i - 6) // 2)
 
     cot_own_part(7)
-
-    @pl.loop(6, 8)
+    multiply(((z + 4) % 8) * 2 + c)
+    mate_part((z + 4) % 8)
+
+    @pl.loop(5, 8)
     def _(n):
         cot_mate_part(n)
 
@@ -435,26 +431,6 @@
             pltpu.make_async_copy(grad_d.at[:, columns], gd_ref.at[:, columns], out_sem.at[2]),
         ]
 
-    @pl.loop(0, 8)
-    def _(i):
-        d, k = 4 - i // 2, i % 2
-        even = (k % 2) == 0
-        zf, zb = (z + d) % 8, (z + 8 - d) % 8
-
-        @pl.when((d < 4) | even)
-        def _():
-            ring_step(d, k, zf, in_f, out_f, rf_recv, up, (d == 4) | ((d == 3) & (~even)))
-
-        @pl.when((d < 4) | (~even))
-        def _():
-            ring_step(d, k, zb, in_b, out_b, rb_recv, down, (d == 4) | ((d == 3) & even))
-
-        prepare((z + d - 1) % 8, k)
-
-        @pl.when(d > 1)
-        def _():
-            prepare((z + 9 - d) % 8, k)
-
     def giving_back(h, peer):
         return remote(fin.at[h, peer], ret_ref.at[h, s], sent.at[RETURNED], ret_recv.at[h], sp=peer)
 
@@ -504,10 +480,6 @@
                 mcf.at[h, tt, tokens_half], col.at[h, s, tokens_half],
                 sent.at[COLUMN], col_recv.at[h, y], sp=tt,
             ).start()
-
-    def use(tt):
-        tile = jnp.concatenate([mcf[h, tt].reshape(256, 128) for h in range(2)], axis=1)
-        acc2[...] += dot(tile, op[tt], NN)
 
     def from_mate(h, zz):
         mc_mate(h, zz, 1 - c).wait_recv()
@@ -524,7 +496,7 @@
         mc_mate(h, z, c).start()
         send_column(h, t)
 
-    def mixer_step(h, d, compute):
+    def mixer_step(h, d):
         zf, zb = (z + 8 - d) % 8, (z + d) % 8
         for k in range(2):
             @pl.when((d < 4) | (k == 0))
@@ -553,98 +525,110 @@
 
         lf, lb = (zf + 1) % 8, (zb + 7) % 8
         from_mate(h, lf)
-        if compute:
-            for core in range(2):
-                use(lf * 2 + core)
 
         @pl.when(d > 1)
         def _():
             from_mate(h, lb)
-            if compute:
-                for core in range(2):
-                    use(lb * 2 + core)
-
-    @pl.loop(0, 8)
+
+    @pl.loop(0, 12)
     def _(i):
-        d, k = 4 - i // 2, i % 2
+        k = i % 2
         even = k == 0
 
-        @pl.when((d < 4) | even)
-        def _():
-            ring_step_2(d, k, in_f, out_f, rf_recv, up, (d == 4) | ((d == 3) & (~even)))
-
-        @pl.when((d < 4) | (~even))
-        def _():
-            ring_step_2(d, k, in_b, out_b, rb_recv, down, (d == 4) | ((d == 3) & even))
-
-        @pl.when((i >= 1) & (i < 3))
-        def _():
-            value = summed(z, i - 1)
-            fin[1, eight(i - 1)] = value[:, 128:].astype(BF16).reshape(8, 48, 128)
-            finish(0, i - 1, value[:, :128])
-
-        @pl.when(i != 1)
-        def _():
-            grads(i)
-
-    acc2[...] = jnp.zeros_like(acc2)
+        @pl.when(i < 8)
+        def _():
+            d = 4 - i // 2
+            zf, zb = (z + d) % 8, (z + 8 - d) % 8
+
+            @pl.when((d < 4) | even)
+            def _():
+                ring_step(d, k, zf, in_f, out_f, rf_recv, up, (d == 4) | ((d == 3) & (~even)))
+
+            @pl.when((d < 4) | (~even))
+            def _():
+                ring_step(d, k, zb, in_b, out_b, rb_recv, down, (d == 4) | ((d == 3) & even))
+
+            prepare((z + d - 1) % 8, k)
+
+            @pl.when(d > 1)
+            def _():
+                prepare((z + 9 - d) % 8, k)
+
+        @pl.when(i >= 4)
+        def _():
+            d = 6 - i // 2
+
+            @pl.when((d < 4) | even)
+            def _():
+                ring_step_2(d, k, in_f, out_f, rf_recv, up, (d == 4) | ((d == 3) & (~even)))
+
+            @pl.when((d < 4) | (~even))
+            def _():
+                ring_step_2(d, k, in_b, out_b, rb_recv, down, (d == 4) | ((d == 3) & even))
+
+        @pl.when((i >= 8) & (i < 10))
+        def _():
+            value = summed(z, k)
+            fin[1, eight(k)] = value[:, 128:].astype(BF16).reshape(8, 48, 128)
+            finish(0, k, value[:, :128])
+
+        @pl.when(i < 4)
+        def _():
+            grads(12 + i)
+
+        grads(i)
+
     finish(1, 0, half_of(fin, 1, eight(0)))
+    finish(1, 1, half_of(fin, 1, eight(1)))
     mixer_start(0)
-    finish(1, 1, half_of(fin, 1, eight(1)))
-    grads(1)
-
-    @pl.loop(1, 3)
+    mixer_step(0, jnp.int32(1))
+    mixer_start(1)
+
+    @pl.loop(2, 5)
     def _(d):
-        mixer_step(0, d, False)
-        grads(7 + d)
-
-    mixer_start(1)
-
-    @pl.loop(3, 5)
-    def _(d):
-        mixer_step(0, d, False)
-        mixer_step(1, d - 2, True)
+        mixer_step(0, d)
+        mixer_step(1, d - 1)
 
     from_mate(0, (z + 4) % 8)
-
-    @pl.loop(3, 5)
-    def _(d):
-        mixer_step(1, d, True)
-        grads(7 + d)
-
+    mixer_step(1, jnp.int32(4))
     from_mate(1, (z + 4) % 8)
-    for core in range(2):
-        use(((z + 4) % 8) * 2 + core)
-
-    grad_mixed = acc2[...]
+
+    full = jnp.concatenate([mcf[h, tt].reshape(256, 128) for tt in range(16) for h in range(2)], axis=1)
+    grad_mixed = dot(full, op[...].reshape(4096, 256), NN)
     gog_ref[...] = (grad_mixed * cout[...]).astype(BF16)
     cin[...] = grad_mixed * og_ref[...].astype(F32)
     for copy in halo_copies(1):
         copy.start()
 
-    @pl.loop(12, 16)
-    def _(i):
-        grads(i)
-
     def column_mate(h, k, core):
         at = col.at[h, part(k), pl.ds(2 * core, 2)]
         return remote(at, at, sent.at[COLUMN_MATE], colp_recv.at[h, (y + 4 - k) % 4], tp=mate)
 
+    def put(i):
+        held, out = ((gog_ref, gog_hbm), (gig_ref, gig_hbm), (gval_ref, gval_hbm))[i]
+        return pltpu.make_async_copy(held, out, out_sem.at[3 + i])
+
+    put_sums = pltpu.make_async_copy(gop_ref, gop_hbm, out_sem.at[6])
+
+    put(0).start()
     for h in range(2):
         for k in range(4):
             arrived(col.at[h, part(k), tokens_half], col_recv.at[h, (y + 4 - k) % 4])
             column_mate(h, k, c).start()
-    arrived(mix_t.at[:, pl.ds(0, 15 * 256)], mix_recv.at[0])
+        if h == 0:
+            before, here, after = neighbours(1)
+            grad_in = after * taps_ref[0:1, :] + here * taps_ref[1:2, :] + before * taps_ref[2:3, :]
+            gig_ref[...] = (grad_in * val_ref[...].astype(F32)).astype(BF16)
+            gval_ref[...] = (grad_in * ig_ref[...].astype(F32)).astype(BF16)
+            put(1).start()
+            put(2).start()
+            arrived(mix_t.at[:, pl.ds(0, 15 * 256)], mix_recv.at[0])
     for h in range(2):
         for k in range(4):
             column_mate(h, k, 1 - c).wait_recv()
     columns = jnp.concatenate([col[h].reshape(4096, 128) for h in range(2)], axis=1)
     gop_ref[...] = dot(mix_t[...], columns, NN).T
-
-    before, here, after = neighbours(1)
-    grad_in = after * taps_ref[0:1, :] + here * taps_ref[1:2, :] + before * taps_ref[2:3, :]
-    gig_ref[...] = (grad_in * val_ref[...].astype(F32)).astype(BF16)
-    gval_ref[...] = (grad_in * ig_ref[...].astype(F32)).astype(BF16)
+    put_sums.start()
 
     sent_all(rows.at[0, pl.ds(0, 15)], DISPATCH)
     sent_all(rows.at[pl.ds(0, 15)], ROWS)
@@ -661,6 +645,9 @@
     pltpu.make_async_copy(grad_gu.at[:, :, pl.ds(0, 128)], gg_ref, out_sem.at[0]).wait()
     pltpu.make_async_copy(grad_gu.at[:, :, pl.ds(128, 128)], gu_ref, out_sem.at[1]).wait()
     pltpu.make_async_copy(grad_d, gd_ref, out_sem.at[2]).wait()
+    for i in range(3):
+        put(i).wait()
+    put_sums.wait()
 
 
 def mixer_and_experts(*operands):
@@ -679,8 +666,12 @@
             jax.ShapeDtypeStruct((128, 4096), BF16),
         ),
         in_specs=[vmem] * 3 + [any_] * 9,
-        out_specs=(vmem,) * 4 + (any_,) * 3,
+        out_specs=(any_,) * 7,
         scratch_shapes=[
+            vm((256, 256), BF16),
+            vm((256, 256), BF16),
+            vm((256, 256), BF16),
+            vm((256, 256), F32),
             vm((256, 256), BF16),
             vm((256, 256), BF16),
             vm((256, 256), BF16),
@@ -716,9 +707,8 @@
             vm((256, 4096), BF16),
             vm((2, 16, 4, 64, 128), BF16),
             vm((2, 16, 4, 64, 128), BF16),
-            vm((256, 256), F32),
-            dma(9), dma(3), dma(14),
-            dma(4), dma(4, 4), dma(4, 4), dma(8, 4), dma(8, 2), dma(2, 4, 2), dma(2, 4, 2), dma(2),
+            dma(9), dma(7), dma(14),
+            dma(4), dma(4, 4), dma(4, 4), dma(8), dma(8, 2), dma(2, 4, 2), dma(2, 4, 2), dma(2),
             dma(2, 2), dma(1), dma(2, 4, 2), dma(2, 4, 2), dma(2, 8), dma(2, 4), dma(2, 4),
             dma(4, 2), dma(4, 2), dma(8), dma(8),
         ],

time: 134 us -> 134 us (level); the launches traced: 134 us -> 133 us
  Pallas kernels: 134 us -> 132 us
    pallas_call x1, Pallas kernels: 129 us -> 128 us  [mixer_and_experts(): pl.pallas_call(moe_kernel, out_shape=(tile, tile, tile, jax.ShapeDtypeStr...]
where the time goes in v6:
time: 134 us; the launch traced here: 133 us
  Pallas kernels  132 us (99%)
    pallas_call x1, Pallas kernels, mixer_and_experts(): pl.pallas_call(moe_kernel, out_shape=(tile, tile, tile, jax.ShapeDtypeStr...  128 us
    pallas_call x1, Pallas kernels, written(): pl.pallas_call(write_out, out_shape=tuple(shapes), in_specs=[any_] * len(...  4.09 us

profile of v6, /device:TPU:17, one launch (start us, length us, event | category | flops | bytes accessed | tf_op | source)
XLA Modules:
  0.0 132.6 jit_solution(14014216097112468592)
XLA Ops:
  0.6 127.9 %mixer_and_experts.1 = (bf16[256,256]{1,0:T(8,128)(2,1)}, bf16[256,256]{1,0:T(8,128)(2,1)}, bf16[256,256]{1,0:T(8,128)(2,1)}, f32[256,256]{1,0:T(8,128)}, bf16[1...) custom-call(s32[2,256]{1,0:T(2,128)} %bitcast.20, f32[2,256]{1,0:T(2,128)} %bitcast.21, ...), custom_call_target="tpu_custom_call" | custom-call | flops 8000000000 | bytes 20000000 | tf_op jit(solution)/shard_map/mixer_and_experts/pallas_call | solution.py:659
  128.5 4.1 %write_out.1 = (f32[4096,128]{1,0:T(8,128)}, f32[4096,128]{1,0:T(8,128)}, f32[128,4096]{1,0:T(8,128)}, f32[256,256]{1,0:T(8,128)}, bf16[256,256]{1,0:T(8,128)(2,...) custom-call(bf16[4096,128]{1,0:T(8,128)(2,1)} %bitcast.11, bf16[4096,128]{1,0:T(8,128)(2,1)} %bitcast.12, ...), custom_call_target="tpu_custom_call" | custom-call | tf_op jit(solution)/shard_map/write_out/pallas_call | solution.py:753

commit v7 on v6

--- a/solution.py
+++ b/solution.py
@@ -467,17 +467,20 @@
 
     tokens_half = pl.ds(2 * c, 2)
 
+    def lanes(h):
+        return pl.ds(128 * h, 128)
+
     def send_column(h, tt):
         @pl.when(tt == s)
         def _():
             pltpu.make_async_copy(
-                mcf.at[h, s, tokens_half], col.at[h, s, tokens_half], col_recv.at[h, y]
+                mcf.at[h, s, tokens_half], col.at[s, tokens_half, :, lanes(h)], col_recv.at[h, y]
             ).start()
 
         @pl.when(tt != s)
         def _():
             remote(
-                mcf.at[h, tt, tokens_half], col.at[h, s, tokens_half],
+                mcf.at[h, tt, tokens_half], col.at[s, tokens_half, :, lanes(h)],
                 sent.at[COLUMN], col_recv.at[h, y], sp=tt,
             ).start()
 
@@ -601,7 +604,7 @@
         copy.start()
 
     def column_mate(h, k, core):
-        at = col.at[h, part(k), pl.ds(2 * core, 2)]
+        at = col.at[part(k), pl.ds(2 * core, 2), :, lanes(h)]
         return remote(at, at, sent.at[COLUMN_MATE], colp_recv.at[h, (y + 4 - k) % 4], tp=mate)
 
     def put(i):
@@ -613,22 +616,21 @@
     put(0).start()
     for h in range(2):
         for k in range(4):
-            arrived(col.at[h, part(k), tokens_half], col_recv.at[h, (y + 4 - k) % 4])
+            arrived(col.at[part(k), tokens_half, :, lanes(h)], col_recv.at[h, (y + 4 - k) % 4])
             column_mate(h, k, c).start()
-        if h == 0:
-            before, here, after = neighbours(1)
-            grad_in = after * taps_ref[0:1, :] + here * taps_ref[1:2, :] + before * taps_ref[2:3, :]
-            gig_ref[...] = (grad_in * val_ref[...].astype(F32)).astype(BF16)
-            gval_ref[...] = (grad_in * ig_ref[...].astype(F32)).astype(BF16)
-            put(1).start()
-            put(2).start()
-            arrived(mix_t.at[:, pl.ds(0, 15 * 256)], mix_recv.at[0])
+    arrived(mix_t.at[:, pl.ds(0, 15 * 256)], mix_recv.at[0])
     for h in range(2):
         for k in range(4):
             column_mate(h, k, 1 - c).wait_recv()
-    columns = jnp.concatenate([col[h].reshape(4096, 128) for h in range(2)], axis=1)
-    gop_ref[...] = dot(mix_t[...], columns, NN).T
+    gop_ref[...] = dot(mix_t[...], col[...].reshape(4096, 256), NN).T
     put_sums.start()
+
+    before, here, after = neighbours(1)
+    grad_in = after * taps_ref[0:1, :] + here * taps_ref[1:2, :] + before * taps_ref[2:3, :]
+    gig_ref[...] = (grad_in * val_ref[...].astype(F32)).astype(BF16)
+    gval_ref[...] = (grad_in * ig_ref[...].astype(F32)).astype(BF16)
+    put(1).start()
+    put(2).start()
 
     sent_all(rows.at[0, pl.ds(0, 15)], DISPATCH)
     sent_all(rows.at[pl.ds(0, 15)], ROWS)
@@ -641,7 +643,7 @@
     sent_all(fin.at[:, pl.ds(0, 15)], RETURNED)
     sent_all(mcf.at[:, pl.ds(0, 15)], MIXER)
     sent_all(mcf.at[:, pl.ds(0, 15), pl.ds(0, 2)], COLUMN)
-    sent_all(col.at[:, :, pl.ds(0, 2)], COLUMN_MATE)
+    sent_all(col.at[:, pl.ds(0, 2)], COLUMN_MATE)
     pltpu.make_async_copy(grad_gu.at[:, :, pl.ds(0, 128)], gg_ref, out_sem.at[0]).wait()
     pltpu.make_async_copy(grad_gu.at[:, :, pl.ds(128, 128)], gu_ref, out_sem.at[1]).wait()
     pltpu.make_async_copy(grad_d, gd_ref, out_sem.at[2]).wait()
@@ -706,7 +708,7 @@
             vm((2, 2, 8, 256), F32),
             vm((256, 4096), BF16),
             vm((2, 16, 4, 64, 128), BF16),
-            vm((2, 16, 4, 64, 128), BF16),
+            vm((16, 4, 64, 256), BF16),
             dma(9), dma(7), dma(14),
             dma(4), dma(4, 4), dma(4, 4), dma(8), dma(8, 2), dma(2, 4, 2), dma(2, 4, 2), dma(2),
             dma(2, 2), dma(1), dma(2, 4, 2), dma(2, 4, 2), dma(2, 8), dma(2, 4), dma(2, 4),

time: 134 us -> 134 us (level)
  no operation moved by 1% of the time
where the time goes in v7:
time: 134 us; the launch traced here: 133 us
  Pallas kernels  132 us (99%)
    pallas_call x1, Pallas kernels, mixer_and_experts(): pl.pallas_call(moe_kernel, out_shape=(tile, tile, tile, jax.ShapeDtypeStr...  128 us
    pallas_call x1, Pallas kernels, written(): pl.pallas_call(write_out, out_shape=tuple(shapes), in_specs=[any_] * len(...  4.09 us

profile of v7, /device:TPU:17, one launch (start us, length us, event | category | flops | bytes accessed | tf_op | source)
XLA Modules:
  0.0 132.7 jit_solution(6333544753379024991)
XLA Ops:
  0.6 128.0 %mixer_and_experts.1 = (bf16[256,256]{1,0:T(8,128)(2,1)}, bf16[256,256]{1,0:T(8,128)(2,1)}, bf16[256,256]{1,0:T(8,128)(2,1)}, f32[256,256]{1,0:T(8,128)}, bf16[1...) custom-call(s32[2,256]{1,0:T(2,128)} %bitcast.20, f32[2,256]{1,0:T(2,128)} %bitcast.21, ...), custom_call_target="tpu_custom_call" | custom-call | flops 8000000000 | bytes 20000000 | tf_op jit(solution)/shard_map/mixer_and_experts/pallas_call | solution.py:661
  128.6 4.1 %write_out.1 = (f32[4096,128]{1,0:T(8,128)}, f32[4096,128]{1,0:T(8,128)}, f32[128,4096]{1,0:T(8,128)}, f32[256,256]{1,0:T(8,128)}, bf16[256,256]{1,0:T(8,128)(2,...) custom-call(bf16[4096,128]{1,0:T(8,128)(2,1)} %bitcast.11, bf16[4096,128]{1,0:T(8,128)(2,1)} %bitcast.12, ...), custom_call_target="tpu_custom_call" | custom-call | tf_op jit(solution)/shard_map/write_out/pallas_call | solution.py:755
